TPU v7x, 128 devices: a whole 4x4x4 slice. The times are simulated.
128 devices in a mesh: ep: 32 (over z, y, core), tp: 4 (over x).
Axes of the slice: x: 4, y: 4, z: 4, core: 2. Of those that a mesh axis runs over, the one named last changes fastest.
Arguments:
- query: bfloat16 [32768, 1024], P('ep', 'tp'), may hold values from -6 to 6
- keys: bfloat16 [32768, 1024], P('ep', 'tp'), may hold values from -6 to 6
- values: bfloat16 [32768, 2048], P('ep', 'tp'), may hold values from -6 to 6
- gate_pre: bfloat16 [32768, 2048], P('ep', 'tp'), may hold values from -6 to 6
- log_decay: float32 [16, 32768], P('tp', 'ep'), may hold values from -1 to 0
- out_weight: bfloat16 [2048, 4096], P(None, 'tp'), may hold values from -0.125 to 0.125
- expert_input: bfloat16 [8192, 4096], P(('ep', 'tp')), may hold values from -6 to 6
- norm_gain: float32 [4096], replicated, may hold values from 0.1 to 1.9
- routes: int32 [8192, 2], P(('ep', 'tp')), may hold values from 0 to 31, all different within a row; in each aligned block of 64 rows (0 to 63, 64 to 127, ...) at most 6 rows name the same one
- route_weights: float32 [8192, 2], P(('ep', 'tp')), may hold values from 0.1 to 1
- w_gate: bfloat16 [32, 4096, 1536], P('ep', None, 'tp'), may hold values from -0.09375 to 0.09375
- w_up: bfloat16 [32, 4096, 1536], P('ep', None, 'tp'), may hold values from -0.09375 to 0.09375
- w_down: bfloat16 [32, 1536, 4096], P('ep', 'tp'), may hold values from -0.15625 to 0.15625
Outputs:
- mixed: bfloat16 [32768, 4096], P('ep', 'tp')
- moe_out: bfloat16 [8192, 4096], P(('ep', 'tp'))
Inputs may be any that keep to these rules, and one draw needn't show every extreme that they name: `routes`: each row names 2 different experts; among the rows of one device no expert is named by more than 6 rows, a bound that some block reaches of some device.
All inputs are finite; a program needn't handle non-finite values.
Results may differ from a plain program's by a relative error of at most 0.018.
Values may be sent and summed in bfloat16 or wider, within the bound.
No kernel may reach another device: no remote copies, remote signals or barrier semaphores. Data moves between devices by JAX's collectives and lax.ppermute only.
A program may use at most 128 MiB of HBM per device.

v0:
```python
import jax
import jax.numpy as jnp
from jax import lax
from jax.experimental import pallas as pl
from jax.experimental.pallas import tpu as pltpu
from jax.sharding import Mesh
from jax.sharding import PartitionSpec as P


EP = ("ep_0", "ep_1", "ep_2")
EP_TP = ("ep_0", "ep_1", "ep_2", "tp")
CHUNK = 256
META = 128
ROW = 8
D_B = 1280
R_B = 1024
F32 = jnp.float32
BF16 = jnp.bfloat16


def send(value, axis, step):
    n = lax.axis_size(axis)
    return lax.ppermute(value, axis, [(i, (i + step) % n) for i in range(n)])


def after(value, *earlier):
    return lax.optimization_barrier((value, earlier))[0]


def mm(a, b):
    return jnp.dot(a, b, preferred_element_type=F32)


def mm_t(a, b):
    return lax.dot_general(a, b, (((0,), (0,)), ((), ())), preferred_element_type=F32)


def turned(x, cosine, sine):
    lane = lax.broadcasted_iota(jnp.int32, x.shape, 1) % 64
    other = jnp.where(lane < 32, pltpu.roll(x, 96, 1), pltpu.roll(x, 32, 1))
    return x * cosine + other * sine


def state_kernel(k_ref, v_ref, cos_ref, sin_ref, cum_t_ref, out_ref, state_ref):
    step = pl.program_id(0)
    heads = v_ref.shape[1] // 128

    @pl.when(step == 0)
    def _():
        state_ref[...] = jnp.zeros_like(state_ref)

    cosine = cos_ref[...]
    sine = sin_ref[...]
    half = lax.broadcasted_iota(jnp.int32, (CHUNK, 128), 1) < 64
    for pair in range(heads // 2):
        lanes = slice(128 * pair, 128 * pair + 128)
        k = turned(k_ref[:, lanes].astype(F32), cosine, sine) * 0.125
        c0 = cum_t_ref[:, 2 * pair : 2 * pair + 1]
        c1 = cum_t_ref[:, 2 * pair + 1 : 2 * pair + 2]
        t0 = c0[CHUNK - 1 : CHUNK, :]
        t1 = c1[CHUNK - 1 : CHUNK, :]
        k = k * jnp.exp(jnp.where(half, t0 - c0, t1 - c1))
        v = v_ref[:, 256 * pair : 256 * pair + 256]
        new = mm_t(k.astype(BF16), v)
        for j, t in ((0, t0), (1, t1)):
            h = 2 * pair + j
            rows = slice(64 * h, 64 * h + 64)
            state_ref[rows, :] = (
                state_ref[rows, :] * jnp.exp(t) + new[64 * j : 64 * j + 64, 128 * j : 128 * j + 128]
            )

    @pl.when(step == pl.num_programs(0) - 1)
    def _():
        out_ref[...] = state_ref[...]


def output_kernel(
    q_ref, k_ref, v_ref, g_ref, cos_ref, sin_ref, cum_ref, cum_t_ref, inc_ref, out_ref, state_ref
):
    step = pl.program_id(0)
    heads = v_ref.shape[1] // 128

    @pl.when(step == 0)
    def _():
        state_ref[...] = jnp.zeros_like(state_ref)
        for h in range(heads):
            low = 64 * (h % 2)
            state_ref[h, low : low + 64, :] = inc_ref[64 * h : 64 * h + 64, :]

    cosine = cos_ref[...]
    sine = sin_ref[...]
    half = lax.broadcasted_iota(jnp.int32, (CHUNK, 128), 1) < 64
    causal = lax.broadcasted_iota(jnp.int32, (CHUNK, CHUNK), 0) >= lax.broadcasted_iota(
        jnp.int32, (CHUNK, CHUNK), 1
    )
    for pair in range(heads // 2):
        lanes = slice(128 * pair, 128 * pair + 128)
        q = turned(q_ref[:, lanes].astype(F32), cosine, sine)
        k = turned(k_ref[:, lanes].astype(F32), cosine, sine) * 0.125
        k_b = k.astype(BF16)
        for j in range(2):
            h = 2 * pair + j
            mine = half if j == 0 else jnp.logical_not(half)
            v = v_ref[:, 128 * h : 128 * h + 128]
            col = cum_t_ref[:, h : h + 1]
            row = cum_ref[0, h : h + 1, :]
            total = col[CHUNK - 1 : CHUNK, :]
            q_h = jnp.where(mine, q, 0.0)
            weights = jnp.exp(jnp.where(causal, col - row, -1e9))
            scores = (
                lax.dot_general(
                    q_h.astype(BF16), k_b, (((1,), (1,)), ((), ())), preferred_element_type=F32
                )
                * weights
            )
            state = state_ref[h]
            out = mm(scores.astype(BF16), v) + mm(
                (q_h * jnp.exp(col)).astype(BF16), state.astype(BF16)
            )
            k_h = jnp.where(mine, k * jnp.exp(total - col), 0.0)
            state_ref[h] = state * jnp.exp(total) + mm_t(k_h.astype(BF16), v)
            centered = out - jnp.mean(out, axis=1, keepdims=True)
            variance = jnp.mean(centered * centered, axis=1, keepdims=True)
            normed = centered * lax.rsqrt(variance + 1e-06)
            gate = g_ref[:, 128 * h : 128 * h + 128].astype(F32)
            out_ref[:, 128 * h : 128 * h + 128] = (gate * jax.nn.sigmoid(gate) * normed).astype(
                BF16
            )


def local_state(keys, values, cosine, sine, cum_t):
    rows, width = keys.shape
    grid = rows // CHUNK
    heads = values.shape[1] // 128
    return pl.pallas_call(
        state_kernel,
        name="local_state",
        grid=(grid,),
        in_specs=[
            pl.BlockSpec((CHUNK, width), lambda i: (i, 0)),
            pl.BlockSpec((CHUNK, values.shape[1]), lambda i: (i, 0)),
            pl.BlockSpec((CHUNK, 128), lambda i: (i, 0)),
            pl.BlockSpec((CHUNK, 128), lambda i: (i, 0)),
            pl.BlockSpec((CHUNK, heads), lambda i: (i, 0)),
        ],
        out_specs=pl.BlockSpec((64 * heads, 128), lambda i: (0, 0)),
        out_shape=jax.ShapeDtypeStruct((64 * heads, 128), F32),
        scratch_shapes=[pltpu.VMEM((64 * heads, 128), F32)],
        cost_estimate=pl.CostEstimate(
            flops=2 * rows * width * 256, bytes_accessed=3 << 20, transcendentals=1 << 18
        ),
    )(keys, values, cosine, sine, cum_t)


def gated_output(query, keys, values, gate_pre, cosine, sine, cum, cum_t, incoming):
    rows, width = keys.shape
    grid = rows // CHUNK
    vw = values.shape[1]
    heads = vw // 128
    return pl.pallas_call(
        output_kernel,
        name="gated_output",
        grid=(grid,),
        in_specs=[
            pl.BlockSpec((CHUNK, width), lambda i: (i, 0)),
            pl.BlockSpec((CHUNK, width), lambda i: (i, 0)),
            pl.BlockSpec((CHUNK, vw), lambda i: (i, 0)),
            pl.BlockSpec((CHUNK, vw), lambda i: (i, 0)),
            pl.BlockSpec((CHUNK, 128), lambda i: (i, 0)),
            pl.BlockSpec((CHUNK, 128), lambda i: (i, 0)),
            pl.BlockSpec((1, heads, CHUNK), lambda i: (i, 0, 0)),
            pl.BlockSpec((CHUNK, heads), lambda i: (i, 0)),
            pl.BlockSpec((64 * heads, 128), lambda i: (0, 0)),
        ],
        out_specs=pl.BlockSpec((CHUNK, vw), lambda i: (i, 0)),
        out_shape=jax.ShapeDtypeStruct((rows, vw), BF16),
        scratch_shapes=[pltpu.VMEM((heads, 128, 128), F32)],
        cost_estimate=pl.CostEstimate(
            flops=10 * 1000 * 1000 * 1000, bytes_accessed=5 << 20, transcendentals=1 << 20
        ),
    )(query, keys, values, gate_pre, cosine, sine, cum, cum_t, incoming)


def pack_state(state, log_total):
    high = log_total.astype(BF16)
    low = (log_total - high.astype(F32)).astype(BF16)
    extra = jnp.concatenate([high[:, None], low[:, None]], axis=0)
    extra = jnp.broadcast_to(extra, (extra.shape[0], 128))
    return jnp.concatenate([state.astype(BF16), extra], axis=0)


def unpack_state(packed, heads):
    state = packed[: 64 * heads].astype(F32)
    logs = packed[64 * heads :, 0].astype(F32)
    return state, logs[:heads] + logs[heads:]


def scaled(state, log_factor):
    return state * jnp.repeat(jnp.exp(log_factor), 64)[:, None]


def core_prefix(state, log_total):
    heads = log_total.shape[0]
    second = lax.axis_index("ep_2") == 1
    mine = pack_state(state, log_total)
    other_state, other_log = unpack_state(send(mine, "ep_2", 1), heads)
    state = unpack_state(mine, heads)[0]
    inside = (jnp.where(second, other_state, 0.0), jnp.where(second, other_log, 0.0))
    first_s = jnp.where(second, other_state, state)
    second_s = jnp.where(second, state, other_state)
    second_log = jnp.where(second, log_total, other_log)
    group = pack_state(scaled(first_s, second_log) + second_s, log_total + other_log)
    return inside, group


def ring_prefix(inside, packed, axis, heads):
    count = lax.axis_size(axis)
    position = lax.axis_index(axis)
    pieces = [unpack_state(packed, heads)] + [
        unpack_state(send(packed, axis, d), heads) for d in range(1, count)
    ]
    places = [(position - d) % count for d in range(count)]
    before = jnp.zeros_like(pieces[0][0])
    before_log = jnp.zeros_like(pieces[0][1])
    for d in range(1, count):
        ok = position >= d
        before = before + jnp.where(ok, scaled(pieces[d][0], before_log), 0.0)
        before_log = before_log + jnp.where(ok, pieces[d][1], 0.0)
    inside = (scaled(before, inside[1]) + inside[0], inside[1] + before_log)
    group_state = jnp.zeros_like(before)
    for d in range(count):
        later = jnp.zeros_like(before_log)
        for k in range(count):
            if k != d:
                later = later + jnp.where(places[k] > places[d], pieces[k][1], 0.0)
        group_state = group_state + scaled(pieces[d][0], later)
    return inside, pack_state(group_state, sum(piece[1] for piece in pieces))


def tables(rows):
    offset = lax.axis_index(EP) * rows
    position = (offset + jnp.arange(rows, dtype=jnp.int32)).astype(F32)
    inverse = 1.0 / 10000.0 ** jnp.linspace(0.0, 1.0, 32, dtype=F32)
    angles = position[:, None] * jnp.tile(inverse, 4)[None, :]
    sign = jnp.where(jnp.arange(128) % 64 < 32, -1.0, 1.0).astype(F32)
    return jnp.cos(angles), jnp.sin(angles) * sign[None, :]


def running(log_decay):
    heads, rows = log_decay.shape
    chunks = rows // CHUNK
    upper = (jnp.arange(CHUNK)[:, None] <= jnp.arange(CHUNK)[None, :]).astype(F32)
    cum = jnp.dot(
        log_decay.reshape(heads * chunks, CHUNK), upper, precision=lax.Precision.HIGHEST
    ).reshape(heads, chunks, CHUNK)
    return cum.transpose(1, 0, 2), cum.transpose(1, 2, 0).reshape(rows, heads)


def ring_first(value):
    return send(value, "tp", 1), send(value, "tp", -1)


def ring_second(left, right, *earlier):
    half = left.shape[0] // 2
    top, bottom = after(left[:half], *earlier), after(right[half:], *earlier)
    top = send(top, "tp", 1)
    bottom = send(bottom, "tp", -1)
    return [top, bottom]


def project_kernel(place_ref, own, left, top, bottom, right, w_ref, out_ref):
    height = own.shape[1]
    step = pl.program_id(0)
    cross = jnp.where(step < pl.num_programs(0) // 2, top[...], bottom[...])
    total = None
    for d, piece in enumerate((own[...], left[...], cross, right[...])):
        start = pl.multiple_of(((place_ref[0] - d) & 3) * height, height)
        product = mm(piece, w_ref[pl.ds(start, height), :])
        total = product if total is None else total + product
    out_ref[...] = total.astype(BF16)


def projected(place, own, left, top, bottom, right, out_weight):
    rows, width = own.shape
    cols = out_weight.shape[1]
    step = rows // 4
    whole = pl.BlockSpec((step, width), lambda i: (i, 0))
    return pl.pallas_call(
        project_kernel,
        name="projected",
        grid=(4,),
        in_specs=[
            pl.BlockSpec(memory_space=pltpu.SMEM),
            whole,
            whole,
            pl.BlockSpec((step, width), lambda i: (jnp.minimum(i, 1), 0)),
            pl.BlockSpec((step, width), lambda i: (jnp.maximum(i - 2, 0), 0)),
            whole,
            pl.BlockSpec(out_weight.shape, lambda i: (0, 0)),
        ],
        out_specs=pl.BlockSpec((step, cols), lambda i: (i, 0)),
        out_shape=jax.ShapeDtypeStruct((rows, cols), BF16),
        cost_estimate=pl.CostEstimate(
            flops=8 * rows * width * cols, bytes_accessed=10 << 20, transcendentals=0
        ),
    )(place, own, left, top, bottom, right, out_weight)


def token_kernel(x_ref, gain_ref, routes_ref, weights_ref, a_ref, b_ref, meta_ref, *, capacity):
    tokens, width = x_ref.shape
    x = x_ref[...].astype(F32)
    centered = x - jnp.mean(x, axis=1, keepdims=True)
    variance = jnp.mean(centered * centered, axis=1, keepdims=True)
    normed = (centered * lax.rsqrt(variance + 1e-05) * gain_ref[...]).astype(BF16)
    first = routes_ref[0:1, :]
    second = routes_ref[1:2, :]
    expert = lax.broadcasted_iota(jnp.int32, (32, tokens), 0)
    hit_0 = (expert == first).astype(F32)
    hit_1 = (expert == second).astype(F32)
    sooner = lax.broadcasted_iota(jnp.int32, (tokens, tokens), 0) < lax.broadcasted_iota(
        jnp.int32, (tokens, tokens), 1
    )
    earlier = mm((hit_0 + hit_1).astype(BF16), sooner.astype(F32).astype(BF16))
    slot_0 = jnp.sum(earlier * hit_0, axis=0, keepdims=True)
    slot_1 = jnp.sum(earlier * hit_1, axis=0, keepdims=True)
    first_f = first.astype(F32)
    second_f = second.astype(F32)
    row_0 = first_f * ROW + slot_0
    row_1 = second_f * ROW + slot_1
    line = lax.broadcasted_iota(jnp.int32, (8, tokens), 0)
    facts = jnp.zeros((8, tokens), F32)
    for index, row in enumerate(
        (
            first_f * capacity + slot_0,
            second_f * capacity + slot_1,
            weights_ref[0:1, :],
            weights_ref[1:2, :],
            row_0,
            row_1,
        )
    ):
        facts = jnp.where(line == index, row, facts)
    spot = lax.broadcasted_iota(jnp.int32, (8, META), 0) == lax.broadcasted_iota(
        jnp.int32, (8, META), 1
    )
    meta = mm_t(facts.astype(BF16), spot.astype(F32).astype(BF16))
    meta_ref[...] = meta
    place = lax.broadcasted_iota(jnp.int32, (a_ref.shape[0], tokens), 0)
    chosen = jnp.logical_or(
        place == row_0.astype(jnp.int32), place == row_1.astype(jnp.int32)
    )
    a_width = a_ref.shape[1]
    a_ref[...] = mm(chosen.astype(F32).astype(BF16), normed[:, :a_width]).astype(BF16)
    b_ref[:, : width - a_width] = normed[:, a_width:]
    b_ref[:, width - a_width :] = meta.astype(BF16)


def token_rows(expert_input, norm_gain, routes, route_weights, capacity, b_width):
    tokens, width = expert_input.shape
    kernel = lambda *refs: token_kernel(*refs, capacity=float(capacity))
    return pl.pallas_call(
        kernel,
        name="token_rows",
        out_shape=(
            jax.ShapeDtypeStruct((32 * ROW, width - b_width), BF16),
            jax.ShapeDtypeStruct((tokens, b_width + META), BF16),
            jax.ShapeDtypeStruct((tokens, META), F32),
        ),
        cost_estimate=pl.CostEstimate(
            flops=1 << 24, bytes_accessed=1 << 20, transcendentals=tokens
        ),
    )(expert_input, norm_gain[None, :], routes.T, route_weights.T)


def slot_row(target, source_x, source_core, here, capacity):
    expert = (target * 10923) >> 16
    slot = target - expert * capacity
    far = ((expert >> 3) - here[0]) & 3
    near = (((expert >> 1) & 3) - here[1]) & 3
    other = (expert - here[2]) & 1
    row = (far * 4 + near) * 8 * capacity + source_x * 2 * capacity + source_core * capacity + slot
    return jnp.where(other == 0, row, -1)


def place_kernel(here_ref, p0, p1, p2, p3, sw, o0, o1, o2, o3, meta_ref, all_ref, *, capacity):
    tokens = p0.shape[0]
    width = o0.shape[1]
    for d, p in enumerate((p0, p1, p2, p3)):
        all_ref[tokens * d : tokens * d + tokens, :] = p[...]
    all_ref[4 * tokens :, :] = sw[...]
    meta = all_ref[:, width:]
    meta_ref[...] = meta
    here = (here_ref[0], here_ref[1], here_ref[2])
    spot = lax.broadcasted_iota(jnp.int32, (8, META), 0) == lax.broadcasted_iota(
        jnp.int32, (8, META), 1
    )
    facts = lax.dot_general(
        spot.astype(F32).astype(BF16), meta, (((1,), (1,)), ((), ())), preferred_element_type=F32
    )
    token = lax.broadcasted_iota(jnp.int32, (1, 8 * tokens), 1)
    source_core = token // (4 * tokens)
    source_x = token // tokens - 4 * source_core
    rows = [
        slot_row(facts[r : r + 1, :].astype(jnp.int32), source_x, source_core, here, capacity)
        for r in range(2)
    ]
    count = o0.shape[0]
    values = all_ref[:, :width]
    for d, out in enumerate((o0, o1, o2, o3)):
        place = lax.broadcasted_iota(jnp.int32, (count, 8 * tokens), 0) + d * count
        chosen = jnp.logical_or(place == rows[0], place == rows[1])
        out[...] = mm(chosen.astype(F32).astype(BF16), values).astype(BF16)


def placed_rows(here, pieces, swapped, width, capacity):
    tokens = pieces[0].shape[0]
    count = 32 * capacity
    vmem = pl.BlockSpec(memory_space=pltpu.VMEM)
    kernel = lambda *refs: place_kernel(*refs, capacity=capacity)
    result = pl.pallas_call(
        kernel,
        name="placed_rows",
        in_specs=[pl.BlockSpec(memory_space=pltpu.SMEM)] + [vmem] * 5,
        out_specs=(vmem,) * 5,
        out_shape=(jax.ShapeDtypeStruct((count, width), BF16),) * 4
        + (jax.ShapeDtypeStruct((8 * tokens, META), BF16),),
        scratch_shapes=[pltpu.VMEM((8 * tokens, width + META), BF16)],
        cost_estimate=pl.CostEstimate(flops=1 << 30, bytes_accessed=4 << 20, transcendentals=0),
    )(here, *pieces, swapped)
    return list(result[:4]), result[4]


def regroup_kernel(i0, i1, i2, i3, o0, o1, o2, o3):
    count = i0.shape[0] // 4
    for d, out in enumerate((o0, o1, o2, o3)):
        for j, source in enumerate((i0, i1, i2, i3)):
            out[count * j : count * j + count, :] = source[count * d : count * d + count, :]


def regrouped(blocks):
    vmem = pl.BlockSpec(memory_space=pltpu.VMEM)
    shape = jax.ShapeDtypeStruct(blocks[0].shape, BF16)
    return list(
        pl.pallas_call(
            regroup_kernel,
            name="regrouped",
            in_specs=[vmem] * 4,
            out_specs=(vmem,) * 4,
            out_shape=(shape,) * 4,
            cost_estimate=pl.CostEstimate(flops=1 << 20, bytes_accessed=4 << 20, transcendentals=0),
        )(*blocks)
    )


def swap_matrix(side, unit):
    row = lax.broadcasted_iota(jnp.int32, (side, side), 0)
    lane = lax.broadcasted_iota(jnp.int32, (side, side), 1)
    block = 4 * unit
    outer = row // block
    middle = (row - outer * block) // unit
    inside = row - outer * block - middle * unit
    return (lane == middle * block + outer * unit + inside).astype(F32).astype(BF16)


def turn_kernel(i0, i1, i2, i3, out_ref, *, unit):
    side = i0.shape[0]
    block = 4 * unit
    swap = swap_matrix(side, unit)
    for z in range(4):
        part = jnp.concatenate(
            [piece[block * z : block * z + block, :] for piece in (i0, i1, i2, i3)], axis=0
        )
        turned_part = mm(swap, part).astype(BF16)
        for x in range(4):
            out_ref[side * x + block * z : side * x + block * z + block, :] = turned_part[
                block * x : block * x + block, :
            ]


def turned_rows(pieces, unit):
    rows, width = pieces[0].shape
    vmem = pl.BlockSpec(memory_space=pltpu.VMEM)
    return pl.pallas_call(
        lambda *refs: turn_kernel(*refs, unit=unit),
        name="turned_rows",
        in_specs=[vmem] * 4,
        out_specs=vmem,
        out_shape=jax.ShapeDtypeStruct((4 * rows, width), BF16),
        cost_estimate=pl.CostEstimate(flops=1 << 29, bytes_accessed=4 << 20, transcendentals=0),
    )(*pieces)


def back_b_kernel(hidden_ref, w_ref, o0, o1, o2, o3, swapped_ref, *, unit):
    side = hidden_ref.shape[0] // 4
    block = 4 * unit
    swap = swap_matrix(side, unit)
    for z in range(4):
        part = jnp.concatenate(
            [hidden_ref[side * x + block * z : side * x + block * z + block, :] for x in range(4)],
            axis=0,
        )
        turned_part = mm(swap, part).astype(BF16)
        for y in range(4):
            swapped_ref[side * y + block * z : side * y + block * z + block, :] = turned_part[
                block * y : block * y + block, :
            ]
    for y, out in enumerate((o0, o1, o2, o3)):
        out[...] = mm(swapped_ref[side * y : side * y + side, :], w_ref[...]).astype(BF16)


def back_b_rows(hidden, weight, unit):
    rows, inner = hidden.shape
    vmem = pl.BlockSpec(memory_space=pltpu.VMEM)
    shape = jax.ShapeDtypeStruct((rows // 4, R_B), BF16)
    first = (weight.shape[1] - R_B) // R_B
    return list(
        pl.pallas_call(
            lambda *refs: back_b_kernel(*refs, unit=unit),
            name="back_b_rows",
            grid=(1,),
            in_specs=[
                pl.BlockSpec((rows, inner), lambda i: (0, 0)),
                pl.BlockSpec((inner, R_B), lambda i: (0, first)),
            ],
            out_specs=(pl.BlockSpec((rows // 4, R_B), lambda i: (0, 0)),) * 4,
            out_shape=(shape,) * 4,
            scratch_shapes=[pltpu.VMEM((rows, inner), BF16)],
            cost_estimate=pl.CostEstimate(
                flops=1 << 30, bytes_accessed=3 << 20, transcendentals=0
            ),
        )(hidden, weight)
    )


def back_a_rows(hidden, weight, width, spans):
    rows, inner = hidden.shape

    def kernel(hidden_ref, w_ref, *out_refs):
        for (low, high), out in zip(spans, out_refs):
            out[...] = mm(hidden_ref[low:high, :], w_ref[...]).astype(BF16)

    return pl.pallas_call(
        kernel,
        grid=(width // 512,),
        in_specs=[
            pl.BlockSpec((rows, inner), lambda i: (0, 0)),
            pl.BlockSpec((inner, 512), lambda i: (0, i)),
        ],
        out_specs=tuple(pl.BlockSpec((h - l, 512), lambda i: (0, i)) for l, h in spans),
        out_shape=tuple(jax.ShapeDtypeStruct((h - l, width), BF16) for l, h in spans),
        cost_estimate=pl.CostEstimate(flops=2 << 30, bytes_accessed=6 << 20, transcendentals=0),
    )(hidden, weight)


def combine_kernel(here_ref, h0, h1, h2, h3, meta_ref, own_ref, other_ref, *, capacity):
    here = (here_ref[0], here_ref[1], here_ref[2])
    source_core = pl.program_id(0)
    total = meta_ref.shape[0]
    source_x = lax.broadcasted_iota(jnp.int32, (total, 1), 0) // (total // 4)
    meta = meta_ref[...].astype(F32)
    rows = [
        slot_row(meta[:, r : r + 1].astype(jnp.int32), source_x, source_core, here, capacity)
        for r in range(2)
    ]
    count = h0.shape[0]
    result = None
    for d, h in enumerate((h0, h1, h2, h3)):
        place = lax.broadcasted_iota(jnp.int32, (total, count), 1) + d * count
        shares = jnp.where(place == rows[0], meta[:, 2:3], 0.0) + jnp.where(
            place == rows[1], meta[:, 3:4], 0.0
        )
        product = mm(shares.astype(BF16), h[...])
        result = product if result is None else result + product

    @pl.when(source_core == 0)
    def _():
        own_ref[...] = result.astype(BF16)

    @pl.when(source_core == 1)
    def _():
        other_ref[...] = result.astype(BF16)


def combined_rows(here, pieces, meta, capacity):
    half = meta.shape[0] // 2
    rows, width = pieces[0].shape
    kernel = lambda *refs: combine_kernel(*refs, capacity=capacity)
    shape = jax.ShapeDtypeStruct((half, width), BF16)
    piece = pl.BlockSpec((rows, width), lambda i: (0, 0))
    whole = pl.BlockSpec((half, width), lambda i: (0, 0))
    return pl.pallas_call(
        kernel,
        name="combined_rows",
        grid=(2,),
        in_specs=[pl.BlockSpec(memory_space=pltpu.SMEM)]
        + [piece] * 4
        + [pl.BlockSpec((half, META), lambda i: (i, 0))],
        out_specs=(whole, whole),
        out_shape=(shape, shape),
        cost_estimate=pl.CostEstimate(flops=1 << 30, bytes_accessed=4 << 20, transcendentals=0),
    )(here, *pieces, meta)


def exchange(blocks, axis, sign):
    return [blocks[0]] + [send(blocks[d], axis, sign * d) for d in range(1, len(blocks))]


def rows_of(value, count):
    height = value.shape[0] // count
    return [value[height * d : height * (d + 1)] for d in range(count)]


def compaction(capacity):
    place = [lax.axis_index(name) for name in EP]
    index = jnp.arange(32 * capacity, dtype=jnp.int32)
    slot = index % capacity
    digits = index // capacity
    far = (place[0] - digits // 8) % 4
    near = (place[1] - digits // 2) % 4
    core = (place[2] - digits) % 2
    source = ((far * 4 + near) * 2 + core) * ROW + slot
    lanes = jnp.arange(32 * ROW, dtype=jnp.int32)
    return (source[:, None] == lanes[None, :]).astype(BF16)


def per_device(
    query,
    keys,
    values,
    gate_pre,
    log_decay,
    out_weight,
    expert_input,
    norm_gain,
    routes,
    route_weights,
    w_gate,
    w_up,
    w_down,
):
    heads = log_decay.shape[0]
    tokens, width = expert_input.shape
    top = routes.shape[1]
    capacity = 3 * tokens * top // (2 * lax.axis_size(EP))
    unit = 2 * capacity
    block = 4 * unit
    a_width = width - D_B
    gate_w, up_w, down_w = (w_gate[0], w_up[0], w_down[0])

    placed_a, payload_b, meta_a = token_rows(
        expert_input, norm_gain, routes, route_weights, capacity, D_B
    )
    here = jnp.stack([lax.axis_index(name) for name in EP]).astype(jnp.int32)
    got_b = exchange([payload_b] * 4, "tp", 1)
    got_a = lax.all_to_all(placed_a.reshape(32, ROW, a_width), EP, 0, 0, tiled=False)

    held_b = jnp.concatenate(got_b, axis=0)
    other_b = send(held_b, "ep_2", 1)
    decay = after(log_decay, placed_a)
    cosine, sine = tables(query.shape[0])
    cum_c, cum_t = running(decay)
    blocks_b, meta_b = placed_rows(here, got_b, after(other_b, sine), D_B, capacity)
    got_b = exchange(blocks_b, "ep_0", 1)

    state = local_state(after(keys, blocks_b[0]), values, cosine, sine, cum_t)
    inside, group = core_prefix(state, jnp.sum(decay, axis=1))
    inside, group_z = ring_prefix(inside, group, "ep_1", heads)

    compact = compaction(capacity)
    slots_a = mm(compact, after(got_a, group).reshape(32 * ROW, a_width)).astype(BF16)
    left_a, right_a = ring_first(slots_a)
    inside, _ = ring_prefix(inside, after(group_z, slots_a), "ep_0", heads)

    turn_b = regrouped(after(got_b, slots_a))
    got_b = exchange(turn_b, "ep_1", 1)
    gated = gated_output(
        query, keys, values, gate_pre, cosine, sine, cum_c, cum_t, after(inside[0], turn_b[0])
    )
    cross_a = ring_second(left_a, right_a, gated)
    left_g, right_g = ring_first(gated)

    turned_b = turned_rows(after(got_b, gated), unit)
    gate_h = mm(turned_b, gate_w[a_width:])
    up_h = mm(turned_b, up_w[a_width:])
    all_a = jnp.concatenate(after([slots_a, left_a, *cross_a, right_a], gate_h), axis=0)
    gate_h = gate_h + mm(all_a, gate_w[:a_width])
    up_h = up_h + mm(all_a, up_w[:a_width])
    hidden = lax.optimization_barrier((jax.nn.silu(gate_h) * up_h).astype(BF16))

    ra = width - R_B
    half = 2 * block
    upper, lower = back_a_rows(
        hidden, down_w, ra, ((8 * block, 10 * block), (10 * block, 12 * block))
    )
    upper = send(upper, "tp", -1)
    lower = send(lower, "tp", 1)
    back_b = back_b_rows(hidden, down_w, unit)
    got_b = exchange(back_b, "ep_1", -1)
    b0, b1, b3 = back_a_rows(
        after(hidden, back_b[0]),
        down_w,
        ra,
        ((0, 4 * block), (4 * block, 8 * block), (12 * block, 16 * block)),
    )
    b1 = jnp.concatenate([b1[:half] + upper, b1[half:]], axis=0)
    b3 = jnp.concatenate([b3[:half], b3[half:] + lower], axis=0)
    up_a, down_a = send(b1, "tp", -1), send(b3, "tp", 1)
    turn_b = regrouped(after(got_b, b1, b3))
    home_b = exchange(turn_b, "ep_0", -1)
    cross_g = ring_second(left_g, right_g, turn_b[0])
    own_b, other_b = combined_rows(here, home_b, meta_b, capacity)
    other_b = send(other_b, "ep_2", 1)
    summed_a = (after(b0, own_b).astype(F32) + up_a.astype(F32) + down_a.astype(F32)).astype(BF16)
    spread_a = mm_t(compact, summed_a).astype(BF16)
    home_a = lax.all_to_all(
        spread_a.reshape(32, ROW, ra), EP, 0, 0, tiled=False
    ).reshape(32 * ROW, ra)
    mixed_b = own_b + after(other_b, spread_a)
    got_b = exchange(rows_of(mixed_b, 4), "tp", -1)
    place = lax.axis_index("tp").astype(jnp.int32)[None]
    mixed = projected(
        place, gated, left_g, *after(cross_g, mixed_b), right_g, out_weight
    )
    final_b = sum(p.astype(F32) for p in got_b)
    slot_lane = jnp.arange(32 * ROW, dtype=jnp.int32)[None, :]
    shares = sum(
        jnp.where(meta_a[:, 4 + r : 5 + r].astype(jnp.int32) == slot_lane, meta_a[:, 2 + r : 3 + r], 0.0)
        for r in range(top)
    ).astype(BF16)
    final_a = mm(shares, after(home_a, mixed))
    moe_out = jnp.concatenate([final_a, final_b], axis=1).astype(BF16)
    return (mixed, moe_out)


def solution(mesh):
    torus = Mesh(mesh.devices.reshape(4, 4, 2, mesh.shape["tp"]), ("ep_0", "ep_1", "ep_2", "tp"))
    return jax.shard_map(
        per_device,
        mesh=torus,
        in_specs=(
            P(EP, "tp"),
            P(EP, "tp"),
            P(EP, "tp"),
            P(EP, "tp"),
            P("tp", EP),
            P(None, "tp"),
            P(EP_TP, None),
            P(),
            P(EP_TP, None),
            P(EP_TP, None),
            P(EP, None, "tp"),
            P(EP, None, "tp"),
            P(EP, "tp", None),
        ),
        out_specs=(P(EP, "tp"), P(EP_TP, None)),
        check_vma=False,
    )
```

profile of v0, /device:TPU:1, one launch (start us, length us, event | category | flops | bytes accessed | tf_op | source)
XLA Modules:
  0.0 250.9 jit_solution(2327119335764398179)
XLA Ops:
  0.6 3.1 %token_rows.1 = (bf16[256,2816]{1,0:T(8,128)(2,1)}, bf16[64,1408]{1,0:T(8,128)(2,1)}, f32[64,128]{1,0:T(8,128)}) custom-call(bf16[64,4096]{1,0:T(8,128)(2,1)} %refs_0_.1, f32[1,4096]{1,0:T(1,128)} %bitcast.68, s32[2,64]{1,0:T(2,128)} %bitcast.70, f32[2,64]{1,0:T(2,128)} %bitcast.71), custom_call_target="tpu_custom_call" | custom-call | flops 16777216 | bytes 1048576 | tf_op jit(solution)/shard_map/token_rows/pallas_call | solution.py:361
  3.7 2.0 collective-permute-start
  5.7 2.5 collective-permute-start.1
  8.2 1.2 collective-permute-start.2
  11.1 5.1 %collective-permute-done.1.refs_3_ = bf16[64,1408]{1,0:T(8,128)(2,1)S(1)} collective-permute-done((bf16[64,1408]{1,0:T(8,128)(2,1)}, bf16[64,1408]{1,0:T(8,128)(2,1)S(1)}, u32[]{:S(2)}, u32[]{:S(2)}) %collective-permute-start.1) | collective-permute-done | bytes 180256 | tf_op jit(solution)/shard_map/ppermute | solution.py:23
  16.2 1.1 pad_maximum_fusion.2
  17.3 1.6 collective-permute-start.3
  19.1 1.0 copy.18
  20.9 3.0 %fusion.17 = (f32[1024,128]{1,0:T(8,128)}, f32[1024,128]{1,0:T(8,128)}) fusion(f32[128]{0:T(128)S(1)} %compare_select_fusion.6, f32[128]{0:T(128)S(1)} %mul.201, f32[1024]{0:T(1024)S(1)} %add_convert_fusion.5), kind=kLoop, calls=%fused_computation.27 | loop fusion | flops 262144 | bytes 1053696 | tf_op jit(solution)/shard_map/mul | solution.py:246
  24.8 3.7 %placed_rows.1 = (bf16[192,1280]{1,0:T(8,128)(2,1)}, bf16[192,1280]{1,0:T(8,128)(2,1)}, bf16[192,1280]{1,0:T(8,128)(2,1)}, bf16[192,1280]{1,0:T(8,128)(2,1)}, bf16[512,128]{1,0:T(8,128)(2,1)}) custom-call(s32[3]{0:T(128)} %pad_add_fusion.refs_0_, bf16[64,1408]{1,0:T(8,128)(2,1)} %get-tuple-element.64.refs_1_, bf16[64,1408]{1,0:T(8,128)(2,1)} %copy-done.19, ...), custom_call_target="tpu_custom_call" | custom-call | flops 1073741824 | bytes 4194304 | tf_op jit(solution)/shard_map/placed_rows/pallas_call | solution.py:420
  28.5 4.9 %local_state.1 = f32[256,128]{1,0:T(8,128)} custom-call(bf16[1024,256]{1,0:T(8,128)(2,1)} %k_ref.2, bf16[1024,512]{1,0:T(8,128)(2,1)} %v_ref.3, f32[1024,128]{1,0:T(8,128)} %get-tuple-element.143.cos_ref, f32[1024,128]{1,0:T(8,128)} %get-tuple-element.142.sin_ref, f32[1024,4]{1,0:T(8,128)} %bitcast.65), custom_call_target="tpu_custom_call" | custom-call | flops 134217728 | bytes 3145728 | tf_op jit(solution)/shard_map/local_state/pallas_call | solution.py:135
  33.3 0.9 convert_element_type.168
  34.4 8.6 %all-to-all-start = ((bf16[32,8,2816]{2,1,0:T(8,128)(2,1)}), bf16[32,8,2816]{2,1,0:T(8,128)(2,1)S(1)}, u32[]{:S(2)}, u32[]{:S(2)}) async-start(bf16[32,8,2816]{2,1,0:T(8,128)(2,1)} %bitcast.19), calls=%async_computation | async-start | bytes 2883584 | tf_op jit(solution)/shard_map/all_to_all | solution.py:655
  43.8 2.6 %collective-permute-start.7 = (bf16[264,128]{1,0:T(8,128)(2,1)S(1)}, bf16[264,128]{1,0:T(8,128)(2,1)S(1)}, u32[]{:S(2)}, u32[]{:S(2)}) collective-permute-start(bf16[264,128]{1,0:T(8,128)(2,1)S(1)} %pad_maximum_fusion.5), channel_id=1, source_target_pairs={{0,24},{8,0},{16,8},{24,16},{1,25},{9,1},{17,9},{25,17},{2,26},{10... | collective-permute-start | bytes 202760 | tf_op jit(solution)/shard_map/ppermute | solution.py:23
  46.4 1.3 collective-permute-start.11
  47.7 2.5 collective-permute-start.12
  50.2 1.1 collective-permute-start.13
  51.8 10.4 %collective-permute-done.7 = bf16[264,128]{1,0:T(8,128)(2,1)S(1)} collective-permute-done((bf16[264,128]{1,0:T(8,128)(2,1)S(1)}, bf16[264,128]{1,0:T(8,128)(2,1)S(1)}, u32[]{:S(2)}, u32[]{:S(2)}) %collective-permute-start.7) | collective-permute-done | bytes 67616 | tf_op jit(solution)/shard_map/ppermute | solution.py:23
  63.1 1.1 collective-permute-done.6
  64.3 2.6 %collective-permute-done.5 = bf16[264,128]{1,0:T(8,128)(2,1)S(1)} collective-permute-done((bf16[264,128]{1,0:T(8,128)(2,1)S(1)}, bf16[264,128]{1,0:T(8,128)(2,1)S(1)}, u32[]{:S(2)}, u32[]{:S(2)}) %collective-permute-start.5) | collective-permute-done | bytes 67616 | tf_op jit(solution)/shard_map/ppermute | solution.py:23
  69.5 2.5 collective-permute-start.9
  75.5 2.0 collective-permute-start.10
  77.6 5.7 %collective-permute-done.12.i2 = bf16[192,1280]{1,0:T(8,128)(2,1)S(1)} collective-permute-done((bf16[192,1280]{1,0:T(8,128)(2,1)}, bf16[192,1280]{1,0:T(8,128)(2,1)S(1)}, u32[]{:S(2)}, u32[]{:S(2)}) %collective-permute-start.12) | collective-permute-done | bytes 491552 | tf_op jit(solution)/shard_map/ppermute | solution.py:23
  83.2 1.9 collective-permute-start.20
  85.2 2.8 %regrouped.2 = (bf16[192,1280]{1,0:T(8,128)(2,1)}, bf16[192,1280]{1,0:T(8,128)(2,1)}, bf16[192,1280]{1,0:T(8,128)(2,1)}, bf16[192,1280]{1,0:T(8,128)(2,1)}) custom-call(bf16[192,1280]{1,0:T(8,128)(2,1)} %get-tuple-element.73.i0, bf16[192,1280]{1,0:T(8,128)(2,1)} %copy-done.6, bf16[192,1280]{1,0:T(8,128)(2,1)} %copy-done.7, ...), custom_call_target="tpu_custom_call" | custom-call | flops 1048576 | bytes 4194304 | tf_op jit(solution)/shard_map/regrouped/pallas_call | solution.py:444
  88.0 1.2 collective-permute-start.15
  89.2 2.4 collective-permute-start.16
  92.8 1.8 collective-permute-start.17
  94.6 1.8 fusion.29.inc_ref
  96.4 14.0 %gated_output.1.own = bf16[1024,512]{1,0:T(8,128)(2,1)} custom-call(bf16[1024,256]{1,0:T(8,128)(2,1)} %q_ref.1, bf16[1024,256]{1,0:T(8,128)(2,1)} %k_ref.2, bf16[1024,512]{1,0:T(8,128)(2,1)} %v_ref.3, bf16[1024,512]{1,0:T(8,128)(2,1)} %g_ref.1, f32[1024,128]{1,0:T(8,128)} %get-tuple-element.143.cos_ref, f32[1024,128]{1,0:T(8,128)} %get-tuple-element.142.sin_ref, ...), custom_call_target="tpu_custom_call" | custom-call | flops 10000000000 | bytes 5242880 | tf_op jit(solution)/shard_map/gated_output/pallas_call | solution.py:160
  111.3 2.7 %collective-permute-start.21 = (bf16[96,2816]{1,0:T(8,128)(2,1)}, bf16[96,2816]{1,0:T(8,128)(2,1)S(1)}, u32[]{:S(2)}, u32[]{:S(2)}) collective-permute-start(bf16[96,2816]{1,0:T(8,128)(2,1)} %slice.232), channel_id=1, source_target_pairs={{0,3},{1,0},{2,1},{3,2},{4,7},{5,4},{6,5},{7,6},{8,11},{9,8},{10,9... | collective-permute-start | bytes 1622024 | tf_op jit(solution)/shard_map/ppermute | solution.py:23
  114.0 1.9 slice.231
  116.7 3.5 %turned_rows.1 = bf16[768,1280]{1,0:T(8,128)(2,1)} custom-call(bf16[192,1280]{1,0:T(8,128)(2,1)} %get-tuple-element.82.refs_0_, bf16[192,1280]{1,0:T(8,128)(2,1)} %copy-done.5, bf16[192,1280]{1,0:T(8,128)(2,1)} %collective-permute-done.16.refs_2_, bf16[192,1280]{1,0:T(8,128)(2,1)} %collective-permute-done.17.refs_3_), custom_call_target="tpu_custom_call" | custom-call | flops 536870912 | bytes 4194304 | tf_op jit(solution)/shard_map/turned_rows/pallas_call | solution.py:483
  120.2 3.0 %fusion.13 = f32[768,384]{1,0:T(8,128)S(1)} fusion(bf16[768,1280]{1,0:T(8,128)(2,1)} %turned_rows.1, bf16[1,4096,384]{2,1,0:T(8,128)(2,1)} %param.23), kind=kOutput, calls=%fused_computation.18 | convolution fusion | flops 754974720 | bytes 4128768 | tf_op jit(solution)/shard_map/dot_general | solution.py:31
  124.0 5.0 %collective-permute-done.19 = bf16[96,2816]{1,0:T(8,128)(2,1)} collective-permute-done((bf16[96,2816]{1,0:T(8,128)(2,1)}, bf16[96,2816]{1,0:T(8,128)(2,1)}, u32[]{:S(2)}, u32[]{:S(2)}) %collective-permute-start.19) | collective-permute-done | bytes 540704 | tf_op jit(solution)/shard_map/ppermute | solution.py:23
  129.1 1.3 constant_dynamic-update-slice_fusion.3
  130.4 1.1 constant_dynamic-update-slice_fusion.2
  131.6 1.8 copy-done.24
  133.4 2.4 fusion.8
  135.8 2.4 fusion
  138.2 2.2 fusion.11.refs_0_.hidden_ref
  140.4 5.5 %shard_map.141 = (bf16[96,3072]{1,0:T(8,128)(2,1)}, bf16[96,3072]{1,0:T(8,128)(2,1)}) custom-call(bf16[768,384]{1,0:T(8,128)(2,1)} %fusion.11.refs_0_.hidden_ref, bf16[384,4096]{1,0:T(8,128)(2,1)} %bitcast.72), custom_call_target="tpu_custom_call" | custom-call | flops 2147483648 | bytes 6291456 | tf_op jit(solution)/shard_map/pallas_call | solution.py:542
  145.9 1.5 collective-permute-start.26
  147.3 3.4 %back_b_rows.1 = (bf16[192,1024]{1,0:T(8,128)(2,1)}, bf16[192,1024]{1,0:T(8,128)(2,1)}, bf16[192,1024]{1,0:T(8,128)(2,1)}, bf16[192,1024]{1,0:T(8,128)(2,1)}) custom-call(bf16[768,384]{1,0:T(8,128)(2,1)} %fusion.11.refs_0_.hidden_ref, bf16[384,4096]{1,0:T(8,128)(2,1)} %bitcast.73), custom_call_target="tpu_custom_call" | custom-call | flops 1073741824 | bytes 3145728 | tf_op jit(solution)/shard_map/back_b_rows/pallas_call | solution.py:517
  150.7 1.8 collective-permute-start.23
  153.3 6.2 %shard_map.140 = (bf16[192,3072]{1,0:T(8,128)(2,1)}, bf16[192,3072]{1,0:T(8,128)(2,1)}, bf16[192,3072]{1,0:T(8,128)(2,1)}) custom-call(bf16[768,384]{1,0:T(8,128)(2,1)} %fusion.11.refs_0_.hidden_ref, bf16[384,4096]{1,0:T(8,128)(2,1)} %bitcast.74), custom_call_target="tpu_custom_call" | custom-call | flops 2147483648 | bytes 6291456 | tf_op jit(solution)/shard_map/pallas_call | solution.py:542
  159.5 1.8 slice_add_fusion.1
  161.6 2.7 %collective-permute-start.34 = (bf16[192,3072]{1,0:T(8,128)(2,1)S(1)}, bf16[192,3072]{1,0:T(8,128)(2,1)}, u32[]{:S(2)}, u32[]{:S(2)}) collective-permute-start(bf16[192,3072]{1,0:T(8,128)(2,1)S(1)} %pad_maximum_fusion), channel_id=1, source_target_pairs={{0,3},{1,0},{2,1},{3,2},{4,7},{5,4},{6,5},{7,6},{8,11},{9,8},{10,9... | collective-permute-start | bytes 3538952 | tf_op jit(solution)/shard_map/ppermute | solution.py:23
  164.3 6.8 %collective-permute-done.24.i3 = bf16[192,1024]{1,0:T(8,128)(2,1)S(1)} collective-permute-done((bf16[192,1024]{1,0:T(8,128)(2,1)}, bf16[192,1024]{1,0:T(8,128)(2,1)S(1)}, u32[]{:S(2)}, u32[]{:S(2)}) %collective-permute-start.24) | collective-permute-done | bytes 393248 | tf_op jit(solution)/shard_map/ppermute | solution.py:23
  171.8 2.6 %regrouped.3 = (bf16[192,1024]{1,0:T(8,128)(2,1)}, bf16[192,1024]{1,0:T(8,128)(2,1)}, bf16[192,1024]{1,0:T(8,128)(2,1)}, bf16[192,1024]{1,0:T(8,128)(2,1)}) custom-call(bf16[192,1024]{1,0:T(8,128)(2,1)} %get-tuple-element.102.i0, bf16[192,1024]{1,0:T(8,128)(2,1)} %copy-done.8, bf16[192,1024]{1,0:T(8,128)(2,1)} %copy-done.9, bf16[192,1024]{1,0:T(8,128)(2,1)} %copy-done.10), custom_call_target="tpu_custom_call" | custom-call | flops 1048576 | bytes 4194304 | tf_op jit(solution)/shard_map/regrouped/pallas_call | solution.py:444
  174.4 1.5 collective-permute-start.28
  175.9 8.2 %collective-permute-done.30.refs_2_ = bf16[192,1024]{1,0:T(8,128)(2,1)S(1)} collective-permute-done((bf16[192,1024]{1,0:T(8,128)(2,1)}, bf16[192,1024]{1,0:T(8,128)(2,1)S(1)}, u32[]{:S(2)}, u32[]{:S(2)}) %collective-permute-start.30) | collective-permute-done | bytes 393248 | tf_op jit(solution)/shard_map/ppermute | solution.py:23
  184.5 1.0 collective-permute-done.31.refs_3_
  185.5 6.3 %collective-permute-start.32 = (bf16[192,1024]{1,0:T(8,128)(2,1)}, bf16[192,1024]{1,0:T(8,128)(2,1)S(1)}, u32[]{:S(2)}, u32[]{:S(2)}) collective-permute-start(bf16[192,1024]{1,0:T(8,128)(2,1)} %get-tuple-element.111), channel_id=1, source_target_pairs={{0,32},{32,64},{64,96},{96,0},{1,33},{33,65},{65,97},{97,1},{2,34}... | collective-permute-start | bytes 1179656 | tf_op jit(solution)/shard_map/ppermute | solution.py:23
  191.8 10.7 %collective-permute-done.32.refs_4_ = bf16[192,1024]{1,0:T(8,128)(2,1)S(1)} collective-permute-done((bf16[192,1024]{1,0:T(8,128)(2,1)}, bf16[192,1024]{1,0:T(8,128)(2,1)S(1)}, u32[]{:S(2)}, u32[]{:S(2)}) %collective-permute-start.32) | collective-permute-done | bytes 393248 | tf_op jit(solution)/shard_map/ppermute | solution.py:23
  203.3 4.4 %combined_rows.1 = (bf16[256,1024]{1,0:T(8,128)(2,1)}, bf16[256,1024]{1,0:T(8,128)(2,1)}) custom-call(s32[3]{0:T(128)} %pad_add_fusion.refs_0_, bf16[192,1024]{1,0:T(8,128)(2,1)} %get-tuple-element.106.refs_1_, bf16[192,1024]{1,0:T(8,128)(2,1)} %copy-done.27, bf16[192,1024]{1,0:T(8,128)(2,1)} %copy-done.28, bf16[192,1024]{1,0:T(8,128)(2,1)} %copy-done.29, ...), custom_call_target="tpu_custom_call" | custom-call | flops 1073741824 | bytes 4194304 | tf_op jit(solution)/shard_map/combined_rows/pallas_call | solution.py:591
  207.8 3.5 %convolution_convert_fusion = bf16[256,3072]{1,0:T(8,128)(2,1)} fusion(bf16[192,3072]{1,0:T(8,128)(2,1)} %collective-permute-done.35, bf16[192,3072]{1,0:T(8,128)(2,1)} %collective-permute-done.34, bf16[192,3072]{1,0:T(8,128)(2,1)S(1)} %copy-done.2, s32[192]{0:T(256)S(1)} %copy-done.23), kind=kOutput, calls=%fused_computation | convolution fusion | flops 306364416 | bytes 5112576 | tf_op jit(solution)/shard_map/dot_general | solution.py:35
  211.3 8.1 %all-to-all-start.1 = ((bf16[32,8,3072]{2,1,0:T(8,128)(2,1)}), bf16[32,8,3072]{2,1,0:T(8,128)(2,1)S(1)}, u32[]{:S(2)}, u32[]{:S(2)}) async-start(bf16[32,8,3072]{2,1,0:T(8,128)(2,1)} %bitcast.26), calls=%async_computation.1 | async-start | bytes 3145728 | tf_op jit(solution)/shard_map/all_to_all | solution.py:715
  219.5 1.9 slice.233
  221.4 1.9 slice.230
  223.5 1.2 collective-permute-start.29
  225.6 11.4 %collective-permute-done.29.bottom = bf16[512,512]{1,0:T(8,128)(2,1)} collective-permute-done((bf16[512,512]{1,0:T(8,128)(2,1)}, bf16[512,512]{1,0:T(8,128)(2,1)}, u32[]{:S(2)}, u32[]{:S(2)}) %collective-permute-start.29) | collective-permute-done | bytes 524320 | tf_op jit(solution)/shard_map/ppermute | solution.py:23
  237.0 2.2 collective-permute-done.27.top
  240.8 8.8 %projected.1 = bf16[1024,1024]{1,0:T(8,128)(2,1)} custom-call(s32[1]{0:T(128)} %bitcast.place_ref, bf16[1024,512]{1,0:T(8,128)(2,1)} %gated_output.1.own, bf16[1024,512]{1,0:T(8,128)(2,1)} %collective-permute-done.14.left, bf16[512,512]{1,0:T(8,128)(2,1)} %collective-permute-done.27.top, bf16[512,512]{1,0:T(8,128)(2,1)} %collective-permute-done.29.bottom, ...), custom_call_target="tpu_custom_call" | custom-call | flops 4294967296 | bytes 10485760 | tf_op jit(solution)/shard_map/projected/pallas_call | solution.py:288
  (183 shorter events, 22.8 us)
Async XLA Ops:
  3.7 7.4 %collective-permute-start = (bf16[64,1408]{1,0:T(8,128)(2,1)}, bf16[64,1408]{1,0:T(8,128)(2,1)S(1)}, u32[]{:S(2)}, u32[]{:S(2)}) collective-permute-start(bf16[64,1408]{1,0:T(8,128)(2,1)} %get-tuple-element.64.refs_1_), channel_id=1, source_target_pairs={{0,1},{1,2},{2,3},{3,0},{4,5},{5,6},{6,7},{7,4},{8,9},{9,10},{10,1... | collective-permute-start | bytes 540680 | tf_op jit(solution)/shard_map/ppermute | solution.py:23
  5.7 10.5 %collective-permute-start.1 = (bf16[64,1408]{1,0:T(8,128)(2,1)}, bf16[64,1408]{1,0:T(8,128)(2,1)S(1)}, u32[]{:S(2)}, u32[]{:S(2)}) collective-permute-start(bf16[64,1408]{1,0:T(8,128)(2,1)} %get-tuple-element.64.refs_1_), channel_id=1, source_target_pairs={{0,2},{1,3},{2,0},{3,1},{4,6},{5,7},{6,4},{7,5},{8,10},{9,11},{10,... | collective-permute-start | bytes 540680 | tf_op jit(solution)/shard_map/ppermute | solution.py:23
  8.2 8.0 %collective-permute-start.2 = (bf16[64,1408]{1,0:T(8,128)(2,1)}, bf16[64,1408]{1,0:T(8,128)(2,1)S(1)}, u32[]{:S(2)}, u32[]{:S(2)}) collective-permute-start(bf16[64,1408]{1,0:T(8,128)(2,1)} %get-tuple-element.64.refs_1_), channel_id=1, source_target_pairs={{0,3},{1,0},{2,1},{3,2},{4,7},{5,4},{6,5},{7,6},{8,11},{9,8},{10,9... | collective-permute-start | bytes 540680 | tf_op jit(solution)/shard_map/ppermute | solution.py:23
  11.1 12.8 %copy-start.19 = (bf16[64,1408]{1,0:T(8,128)(2,1)}, bf16[64,1408]{1,0:T(8,128)(2,1)S(1)}, u32[]{:S(2)}) copy-start(bf16[64,1408]{1,0:T(8,128)(2,1)S(1)} %collective-permute-done.refs_2_) | copy-start | bytes 540676
  16.2 7.7 %copy-start.20 = (bf16[64,1408]{1,0:T(8,128)(2,1)}, bf16[64,1408]{1,0:T(8,128)(2,1)S(1)}, u32[]{:S(2)}) copy-start(bf16[64,1408]{1,0:T(8,128)(2,1)S(1)} %collective-permute-done.1.refs_3_) | copy-start | bytes 540676
  16.2 7.8 %copy-start.21 = (bf16[64,1408]{1,0:T(8,128)(2,1)}, bf16[64,1408]{1,0:T(8,128)(2,1)S(1)}, u32[]{:S(2)}) copy-start(bf16[64,1408]{1,0:T(8,128)(2,1)S(1)} %collective-permute-done.2.refs_4_) | copy-start | bytes 540676
  17.3 6.6 %collective-permute-start.3 = (bf16[256,1408]{1,0:T(8,128)(2,1)S(1)}, bf16[256,1408]{1,0:T(8,128)(2,1)S(1)}, u32[]{:S(2)}, u32[]{:S(2)}) collective-permute-start(bf16[256,1408]{1,0:T(8,128)(2,1)S(1)} %pad_maximum_fusion.2), channel_id=1, source_target_pairs={{0,4},{4,0},{1,5},{5,1},{2,6},{6,2},{3,7},{7,3},{8,12},{12,8},{9,1... | collective-permute-start | bytes 2162696 | tf_op jit(solution)/shard_map/ppermute | solution.py:23
  34.2 9.3 %copy-start.1 = (f32[256,128]{1,0:T(8,128)S(1)}, f32[256,128]{1,0:T(8,128)}, u32[]{:S(2)}) copy-start(f32[256,128]{1,0:T(8,128)} %local_state.1) | copy-start | bytes 393220
  34.4 8.8 %collective-permute-start.4 = (bf16[264,128]{1,0:T(8,128)(2,1)S(1)}, bf16[264,128]{1,0:T(8,128)(2,1)S(1)}, u32[]{:S(2)}, u32[]{:S(2)}) collective-permute-start(bf16[264,128]{1,0:T(8,128)(2,1)S(1)} %pad_maximum_fusion.4), channel_id=1, source_target_pairs={{0,4},{4,0},{1,5},{5,1},{2,6},{6,2},{3,7},{7,3},{8,12},{12,8},{9,1... | collective-permute-start | bytes 202760 | tf_op jit(solution)/shard_map/ppermute | solution.py:23
  34.4 34.5 %all-to-all-start = ((bf16[32,8,2816]{2,1,0:T(8,128)(2,1)}), bf16[32,8,2816]{2,1,0:T(8,128)(2,1)S(1)}, u32[]{:S(2)}, u32[]{:S(2)}) async-start(bf16[32,8,2816]{2,1,0:T(8,128)(2,1)} %bitcast.19), calls=%async_computation | async-start | bytes 2883584 | tf_op jit(solution)/shard_map/all_to_all | solution.py:655
  43.1 25.8 %copy-start.11 = (bf16[264,128]{1,0:T(8,128)(2,1)}, bf16[264,128]{1,0:T(8,128)(2,1)S(1)}, u32[]{:S(2)}) copy-start(bf16[264,128]{1,0:T(8,128)(2,1)S(1)} %collective-permute-done.4) | copy-start | bytes 202756
  43.8 18.5 %collective-permute-start.7 = (bf16[264,128]{1,0:T(8,128)(2,1)S(1)}, bf16[264,128]{1,0:T(8,128)(2,1)S(1)}, u32[]{:S(2)}, u32[]{:S(2)}) collective-permute-start(bf16[264,128]{1,0:T(8,128)(2,1)S(1)} %pad_maximum_fusion.5), channel_id=1, source_target_pairs={{0,24},{8,0},{16,8},{24,16},{1,25},{9,1},{17,9},{25,17},{2,26},{10... | collective-permute-start | bytes 202760 | tf_op jit(solution)/shard_map/ppermute | solution.py:23
  46.4 27.0 %copy-start.22 = (s32[192]{0:T(256)}, s32[192]{0:T(256)S(1)}, u32[]{:S(2)}) copy-start(s32[192]{0:T(256)S(1)} %fusion.44) | copy-start | bytes 2308
  46.4 29.1 %collective-permute-start.11 = (bf16[192,1280]{1,0:T(8,128)(2,1)}, bf16[192,1280]{1,0:T(8,128)(2,1)S(1)}, u32[]{:S(2)}, u32[]{:S(2)}) collective-permute-start(bf16[192,1280]{1,0:T(8,128)(2,1)} %get-tuple-element.70), channel_id=1, source_target_pairs={{0,32},{32,64},{64,96},{96,0},{1,33},{33,65},{65,97},{97,1},{2,34}... | collective-permute-start | bytes 1474568 | tf_op jit(solution)/shard_map/ppermute | solution.py:23
  47.7 35.6 %collective-permute-start.12 = (bf16[192,1280]{1,0:T(8,128)(2,1)}, bf16[192,1280]{1,0:T(8,128)(2,1)S(1)}, u32[]{:S(2)}, u32[]{:S(2)}) collective-permute-start(bf16[192,1280]{1,0:T(8,128)(2,1)} %get-tuple-element.71), channel_id=1, source_target_pairs={{0,64},{32,96},{64,0},{96,32},{1,65},{33,97},{65,1},{97,33},{2,66}... | collective-permute-start | bytes 1474568 | tf_op jit(solution)/shard_map/ppermute | solution.py:23
  50.2 35.0 %collective-permute-start.13 = (bf16[192,1280]{1,0:T(8,128)(2,1)}, bf16[192,1280]{1,0:T(8,128)(2,1)}, u32[]{:S(2)}, u32[]{:S(2)}) collective-permute-start(bf16[192,1280]{1,0:T(8,128)(2,1)} %get-tuple-element.72), channel_id=1, source_target_pairs={{0,96},{32,0},{64,32},{96,64},{1,97},{33,1},{65,33},{97,65},{2,98}... | collective-permute-start | bytes 1474568 | tf_op jit(solution)/shard_map/ppermute | solution.py:23
  51.3 12.9 %collective-permute-start.6 = (bf16[264,128]{1,0:T(8,128)(2,1)S(1)}, bf16[264,128]{1,0:T(8,128)(2,1)S(1)}, u32[]{:S(2)}, u32[]{:S(2)}) collective-permute-start(bf16[264,128]{1,0:T(8,128)(2,1)S(1)} %pad_maximum_fusion.5), channel_id=1, source_target_pairs={{0,16},{8,24},{16,0},{24,8},{1,17},{9,25},{17,1},{25,9},{2,18},{10... | collective-permute-start | bytes 202760 | tf_op jit(solution)/shard_map/ppermute | solution.py:23
  62.3 6.7 %copy-start.13 = (bf16[264,128]{1,0:T(8,128)(2,1)}, bf16[264,128]{1,0:T(8,128)(2,1)S(1)}, u32[]{:S(2)}) copy-start(bf16[264,128]{1,0:T(8,128)(2,1)S(1)} %collective-permute-done.7) | copy-start | bytes 202756
  62.3 4.6 %collective-permute-start.5 = (bf16[264,128]{1,0:T(8,128)(2,1)S(1)}, bf16[264,128]{1,0:T(8,128)(2,1)S(1)}, u32[]{:S(2)}, u32[]{:S(2)}) collective-permute-start(bf16[264,128]{1,0:T(8,128)(2,1)S(1)} %pad_maximum_fusion.5), channel_id=1, source_target_pairs={{0,8},{8,16},{16,24},{24,0},{1,9},{9,17},{17,25},{25,1},{2,10},{10... | collective-permute-start | bytes 202760 | tf_op jit(solution)/shard_map/ppermute | solution.py:23
  64.2 4.7 %copy-start.15 = (bf16[264,128]{1,0:T(8,128)(2,1)}, bf16[264,128]{1,0:T(8,128)(2,1)S(1)}, u32[]{:S(2)}) copy-start(bf16[264,128]{1,0:T(8,128)(2,1)S(1)} %collective-permute-done.6) | copy-start | bytes 202756
  69.4 25.2 %copy-start.12 = (bf16[264,128]{1,0:T(8,128)(2,1)S(1)}, bf16[264,128]{1,0:T(8,128)(2,1)}, u32[]{:S(2)}) copy-start(bf16[264,128]{1,0:T(8,128)(2,1)} %copy-done.11) | copy-start | bytes 202756
  69.4 25.2 %copy-start.14 = (bf16[264,128]{1,0:T(8,128)(2,1)S(1)}, bf16[264,128]{1,0:T(8,128)(2,1)}, u32[]{:S(2)}) copy-start(bf16[264,128]{1,0:T(8,128)(2,1)} %copy-done.13) | copy-start | bytes 202756
  69.4 25.2 %copy-start.16 = (bf16[264,128]{1,0:T(8,128)(2,1)S(1)}, bf16[264,128]{1,0:T(8,128)(2,1)}, u32[]{:S(2)}) copy-start(bf16[264,128]{1,0:T(8,128)(2,1)} %copy-done.15) | copy-start | bytes 202756
  69.4 25.2 %copy-start.18 = (bf16[264,128]{1,0:T(8,128)(2,1)S(1)}, bf16[264,128]{1,0:T(8,128)(2,1)}, u32[]{:S(2)}) copy-start(bf16[264,128]{1,0:T(8,128)(2,1)} %copy-done.17) | copy-start | bytes 202756
  69.5 18.5 %collective-permute-start.9 = (bf16[264,128]{1,0:T(8,128)(2,1)}, bf16[264,128]{1,0:T(8,128)(2,1)S(1)}, u32[]{:S(2)}, u32[]{:S(2)}) collective-permute-start(bf16[264,128]{1,0:T(8,128)(2,1)} %pad_maximum_fusion.6), channel_id=1, source_target_pairs={{0,64},{32,96},{64,0},{96,32},{1,65},{33,97},{65,1},{97,33},{2,66}... | collective-permute-start | bytes 202760 | tf_op jit(solution)/shard_map/ppermute | solution.py:23
  74.9 14.3 %collective-permute-start.8 = (bf16[264,128]{1,0:T(8,128)(2,1)}, bf16[264,128]{1,0:T(8,128)(2,1)}, u32[]{:S(2)}, u32[]{:S(2)}) collective-permute-start(bf16[264,128]{1,0:T(8,128)(2,1)} %pad_maximum_fusion.6), channel_id=1, source_target_pairs={{0,32},{32,64},{64,96},{96,0},{1,33},{33,65},{65,97},{97,1},{2,34}... | collective-permute-start | bytes 202760 | tf_op jit(solution)/shard_map/ppermute | solution.py:23
  75.5 9.6 %copy-start.6 = (bf16[192,1280]{1,0:T(8,128)(2,1)}, bf16[192,1280]{1,0:T(8,128)(2,1)S(1)}, u32[]{:S(2)}) copy-start(bf16[192,1280]{1,0:T(8,128)(2,1)S(1)} %collective-permute-done.11.i1) | copy-start | bytes 1474564
  75.5 17.2 %collective-permute-start.10 = (bf16[264,128]{1,0:T(8,128)(2,1)}, bf16[264,128]{1,0:T(8,128)(2,1)}, u32[]{:S(2)}, u32[]{:S(2)}) collective-permute-start(bf16[264,128]{1,0:T(8,128)(2,1)} %pad_maximum_fusion.6), channel_id=1, source_target_pairs={{0,96},{32,0},{64,32},{96,64},{1,97},{33,1},{65,33},{97,65},{2,98}... | collective-permute-start | bytes 202760 | tf_op jit(solution)/shard_map/ppermute | solution.py:23
  83.2 27.2 %collective-permute-start.20 = (bf16[192,2816]{1,0:T(8,128)(2,1)S(1)}, bf16[192,2816]{1,0:T(8,128)(2,1)S(1)}, u32[]{:S(2)}, u32[]{:S(2)}) collective-permute-start(bf16[192,2816]{1,0:T(8,128)(2,1)S(1)} %convolution_convert_fusion.1), channel_id=1, source_target_pairs={{0,3},{1,0},{2,1},{3,2},{4,7},{5,4},{6,5},{7,6},{8,11},{9,8},{10,9... | collective-permute-start | bytes 3244040 | tf_op jit(solution)/shard_map/ppermute | solution.py:23
  85.2 28.8 %collective-permute-start.18 = (bf16[192,2816]{1,0:T(8,128)(2,1)S(1)}, bf16[192,2816]{1,0:T(8,128)(2,1)}, u32[]{:S(2)}, u32[]{:S(2)}) collective-permute-start(bf16[192,2816]{1,0:T(8,128)(2,1)S(1)} %convolution_convert_fusion.1), channel_id=1, source_target_pairs={{0,1},{1,2},{2,3},{3,0},{4,5},{5,6},{6,7},{7,4},{8,9},{9,10},{10,1... | collective-permute-start | bytes 3244040 | tf_op jit(solution)/shard_map/ppermute | solution.py:23
  88.0 27.9 %collective-permute-start.15 = (bf16[192,1280]{1,0:T(8,128)(2,1)}, bf16[192,1280]{1,0:T(8,128)(2,1)S(1)}, u32[]{:S(2)}, u32[]{:S(2)}) collective-permute-start(bf16[192,1280]{1,0:T(8,128)(2,1)} %get-tuple-element.79), channel_id=1, source_target_pairs={{0,8},{8,16},{16,24},{24,0},{1,9},{9,17},{17,25},{25,1},{2,10},{10... | collective-permute-start | bytes 1474568 | tf_op jit(solution)/shard_map/ppermute | solution.py:23
  89.2 26.7 %collective-permute-start.16 = (bf16[192,1280]{1,0:T(8,128)(2,1)}, bf16[192,1280]{1,0:T(8,128)(2,1)}, u32[]{:S(2)}, u32[]{:S(2)}) collective-permute-start(bf16[192,1280]{1,0:T(8,128)(2,1)} %get-tuple-element.80), channel_id=1, source_target_pairs={{0,16},{8,24},{16,0},{24,8},{1,17},{9,25},{17,1},{25,9},{2,18},{10... | collective-permute-start | bytes 1474568 | tf_op jit(solution)/shard_map/ppermute | solution.py:23
  92.8 23.1 %collective-permute-start.17 = (bf16[192,1280]{1,0:T(8,128)(2,1)}, bf16[192,1280]{1,0:T(8,128)(2,1)}, u32[]{:S(2)}, u32[]{:S(2)}) collective-permute-start(bf16[192,1280]{1,0:T(8,128)(2,1)} %get-tuple-element.81), channel_id=1, source_target_pairs={{0,24},{8,0},{16,8},{24,16},{1,25},{9,1},{17,9},{25,17},{2,26},{10... | collective-permute-start | bytes 1474568 | tf_op jit(solution)/shard_map/ppermute | solution.py:23
  111.3 12.7 %collective-permute-start.21 = (bf16[96,2816]{1,0:T(8,128)(2,1)}, bf16[96,2816]{1,0:T(8,128)(2,1)S(1)}, u32[]{:S(2)}, u32[]{:S(2)}) collective-permute-start(bf16[96,2816]{1,0:T(8,128)(2,1)} %slice.232), channel_id=1, source_target_pairs={{0,3},{1,0},{2,1},{3,2},{4,7},{5,4},{6,5},{7,6},{8,11},{9,8},{10,9... | collective-permute-start | bytes 1622024 | tf_op jit(solution)/shard_map/ppermute | solution.py:23
  115.9 13.1 %collective-permute-start.19 = (bf16[96,2816]{1,0:T(8,128)(2,1)}, bf16[96,2816]{1,0:T(8,128)(2,1)}, u32[]{:S(2)}, u32[]{:S(2)}) collective-permute-start(bf16[96,2816]{1,0:T(8,128)(2,1)} %slice.231), channel_id=1, source_target_pairs={{0,1},{1,2},{2,3},{3,0},{4,5},{5,6},{6,7},{7,4},{8,9},{9,10},{10,1... | collective-permute-start | bytes 1622024 | tf_op jit(solution)/shard_map/ppermute | solution.py:23
  133.4 2.4 copy-start.25
  135.8 2.4 copy-start
  145.9 13.6 %collective-permute-start.25 = (bf16[96,3072]{1,0:T(8,128)(2,1)}, bf16[96,3072]{1,0:T(8,128)(2,1)S(1)}, u32[]{:S(2)}, u32[]{:S(2)}) collective-permute-start(bf16[96,3072]{1,0:T(8,128)(2,1)} %get-tuple-element.99), channel_id=1, source_target_pairs={{0,3},{1,0},{2,1},{3,2},{4,7},{5,4},{6,5},{7,6},{8,11},{9,8},{10,9... | collective-permute-start | bytes 1769480 | tf_op jit(solution)/shard_map/ppermute | solution.py:23
  145.9 13.6 %collective-permute-start.26 = (bf16[96,3072]{1,0:T(8,128)(2,1)}, bf16[96,3072]{1,0:T(8,128)(2,1)S(1)}, u32[]{:S(2)}, u32[]{:S(2)}) collective-permute-start(bf16[96,3072]{1,0:T(8,128)(2,1)} %get-tuple-element.101), channel_id=1, source_target_pairs={{0,1},{1,2},{2,3},{3,0},{4,5},{5,6},{6,7},{7,4},{8,9},{9,10},{10,1... | collective-permute-start | bytes 1769480 | tf_op jit(solution)/shard_map/ppermute | solution.py:23
  150.7 13.6 %collective-permute-start.22 = (bf16[192,1024]{1,0:T(8,128)(2,1)}, bf16[192,1024]{1,0:T(8,128)(2,1)S(1)}, u32[]{:S(2)}, u32[]{:S(2)}) collective-permute-start(bf16[192,1024]{1,0:T(8,128)(2,1)} %get-tuple-element.94), channel_id=1, source_target_pairs={{0,24},{8,0},{16,8},{24,16},{1,25},{9,1},{17,9},{25,17},{2,26},{10... | collective-permute-start | bytes 1179656 | tf_op jit(solution)/shard_map/ppermute | solution.py:23
  150.7 13.6 %collective-permute-start.23 = (bf16[192,1024]{1,0:T(8,128)(2,1)}, bf16[192,1024]{1,0:T(8,128)(2,1)S(1)}, u32[]{:S(2)}, u32[]{:S(2)}) collective-permute-start(bf16[192,1024]{1,0:T(8,128)(2,1)} %get-tuple-element.95), channel_id=1, source_target_pairs={{0,16},{8,24},{16,0},{24,8},{1,17},{9,25},{17,1},{25,9},{2,18},{10... | collective-permute-start | bytes 1179656 | tf_op jit(solution)/shard_map/ppermute | solution.py:23
  152.5 18.6 %collective-permute-start.24 = (bf16[192,1024]{1,0:T(8,128)(2,1)}, bf16[192,1024]{1,0:T(8,128)(2,1)S(1)}, u32[]{:S(2)}, u32[]{:S(2)}) collective-permute-start(bf16[192,1024]{1,0:T(8,128)(2,1)} %get-tuple-element.96), channel_id=1, source_target_pairs={{0,8},{8,16},{16,24},{24,0},{1,9},{9,17},{17,25},{25,1},{2,10},{10... | collective-permute-start | bytes 1179656 | tf_op jit(solution)/shard_map/ppermute | solution.py:23
  161.4 46.4 %collective-permute-start.35 = (bf16[192,3072]{1,0:T(8,128)(2,1)S(1)}, bf16[192,3072]{1,0:T(8,128)(2,1)}, u32[]{:S(2)}, u32[]{:S(2)}) collective-permute-start(bf16[192,3072]{1,0:T(8,128)(2,1)S(1)} %pad_maximum_fusion.1), channel_id=1, source_target_pairs={{0,1},{1,2},{2,3},{3,0},{4,5},{5,6},{6,7},{7,4},{8,9},{9,10},{10,1... | collective-permute-start | bytes 3538952 | tf_op jit(solution)/shard_map/ppermute | solution.py:23
  161.6 46.2 %collective-permute-start.34 = (bf16[192,3072]{1,0:T(8,128)(2,1)S(1)}, bf16[192,3072]{1,0:T(8,128)(2,1)}, u32[]{:S(2)}, u32[]{:S(2)}) collective-permute-start(bf16[192,3072]{1,0:T(8,128)(2,1)S(1)} %pad_maximum_fusion), channel_id=1, source_target_pairs={{0,3},{1,0},{2,1},{3,2},{4,7},{5,4},{6,5},{7,6},{8,11},{9,8},{10,9... | collective-permute-start | bytes 3538952 | tf_op jit(solution)/shard_map/ppermute | solution.py:23
  164.3 6.8 %copy-start.8 = (bf16[192,1024]{1,0:T(8,128)(2,1)}, bf16[192,1024]{1,0:T(8,128)(2,1)S(1)}, u32[]{:S(2)}) copy-start(bf16[192,1024]{1,0:T(8,128)(2,1)S(1)} %collective-permute-done.22.i1) | copy-start | bytes 1179652
  164.3 6.8 %copy-start.9 = (bf16[192,1024]{1,0:T(8,128)(2,1)}, bf16[192,1024]{1,0:T(8,128)(2,1)S(1)}, u32[]{:S(2)}) copy-start(bf16[192,1024]{1,0:T(8,128)(2,1)S(1)} %collective-permute-done.23.i2) | copy-start | bytes 1179652
  174.4 9.7 %collective-permute-start.30 = (bf16[192,1024]{1,0:T(8,128)(2,1)}, bf16[192,1024]{1,0:T(8,128)(2,1)S(1)}, u32[]{:S(2)}, u32[]{:S(2)}) collective-permute-start(bf16[192,1024]{1,0:T(8,128)(2,1)} %get-tuple-element.109), channel_id=1, source_target_pairs={{0,96},{32,0},{64,32},{96,64},{1,97},{33,1},{65,33},{97,65},{2,98}... | collective-permute-start | bytes 1179656 | tf_op jit(solution)/shard_map/ppermute | solution.py:23
  174.4 11.1 %collective-permute-start.31 = (bf16[192,1024]{1,0:T(8,128)(2,1)}, bf16[192,1024]{1,0:T(8,128)(2,1)S(1)}, u32[]{:S(2)}, u32[]{:S(2)}) collective-permute-start(bf16[192,1024]{1,0:T(8,128)(2,1)} %get-tuple-element.110), channel_id=1, source_target_pairs={{0,64},{32,96},{64,0},{96,32},{1,65},{33,97},{65,1},{97,33},{2,66}... | collective-permute-start | bytes 1179656 | tf_op jit(solution)/shard_map/ppermute | solution.py:23
  174.4 45.0 %collective-permute-start.28 = (bf16[1024,512]{1,0:T(8,128)(2,1)}, bf16[1024,512]{1,0:T(8,128)(2,1)}, u32[]{:S(2)}, u32[]{:S(2)}) collective-permute-start(bf16[1024,512]{1,0:T(8,128)(2,1)} %gated_output.1.own), channel_id=1, source_target_pairs={{0,3},{1,0},{2,1},{3,2},{4,7},{5,4},{6,5},{7,6},{8,11},{9,8},{10,9... | collective-permute-start | bytes 3145736 | tf_op jit(solution)/shard_map/ppermute | solution.py:23
  184.1 18.4 %copy-start.27 = (bf16[192,1024]{1,0:T(8,128)(2,1)}, bf16[192,1024]{1,0:T(8,128)(2,1)S(1)}, u32[]{:S(2)}) copy-start(bf16[192,1024]{1,0:T(8,128)(2,1)S(1)} %collective-permute-done.30.refs_2_) | copy-start | bytes 1179652
  184.1 37.3 %collective-permute-start.14 = (bf16[1024,512]{1,0:T(8,128)(2,1)}, bf16[1024,512]{1,0:T(8,128)(2,1)}, u32[]{:S(2)}, u32[]{:S(2)}) collective-permute-start(bf16[1024,512]{1,0:T(8,128)(2,1)} %gated_output.1.own), channel_id=1, source_target_pairs={{0,1},{1,2},{2,3},{3,0},{4,5},{5,6},{6,7},{7,4},{8,9},{9,10},{10,1... | collective-permute-start | bytes 3145736 | tf_op jit(solution)/shard_map/ppermute | solution.py:23
  185.5 17.0 %copy-start.28 = (bf16[192,1024]{1,0:T(8,128)(2,1)}, bf16[192,1024]{1,0:T(8,128)(2,1)S(1)}, u32[]{:S(2)}) copy-start(bf16[192,1024]{1,0:T(8,128)(2,1)S(1)} %collective-permute-done.31.refs_3_) | copy-start | bytes 1179652
  185.5 17.0 %collective-permute-start.32 = (bf16[192,1024]{1,0:T(8,128)(2,1)}, bf16[192,1024]{1,0:T(8,128)(2,1)S(1)}, u32[]{:S(2)}, u32[]{:S(2)}) collective-permute-start(bf16[192,1024]{1,0:T(8,128)(2,1)} %get-tuple-element.111), channel_id=1, source_target_pairs={{0,32},{32,64},{64,96},{96,0},{1,33},{33,65},{65,97},{97,1},{2,34}... | collective-permute-start | bytes 1179656 | tf_op jit(solution)/shard_map/ppermute | solution.py:23
  203.3 4.5 %copy-start.2 = (bf16[192,3072]{1,0:T(8,128)(2,1)S(1)}, bf16[192,3072]{1,0:T(8,128)(2,1)}, u32[]{:S(2)}) copy-start(bf16[192,3072]{1,0:T(8,128)(2,1)} %get-tuple-element.116) | copy-start | bytes 3538948
  203.3 4.5 %copy-start.23 = (s32[192]{0:T(256)S(1)}, s32[192]{0:T(256)}, u32[]{:S(2)}) copy-start(s32[192]{0:T(256)} %copy-done.22) | copy-start | bytes 2308
  211.3 38.3 %all-to-all-start.1 = ((bf16[32,8,3072]{2,1,0:T(8,128)(2,1)}), bf16[32,8,3072]{2,1,0:T(8,128)(2,1)S(1)}, u32[]{:S(2)}, u32[]{:S(2)}) async-start(bf16[32,8,3072]{2,1,0:T(8,128)(2,1)} %bitcast.26), calls=%async_computation.1 | async-start | bytes 3145728 | tf_op jit(solution)/shard_map/all_to_all | solution.py:715
  219.5 5.5 %copy-start.4 = (f32[64,128]{1,0:T(8,128)S(1)}, f32[64,128]{1,0:T(8,128)}, u32[]{:S(2)}) copy-start(f32[64,128]{1,0:T(8,128)} %get-tuple-element.120) | copy-start | bytes 98308
  219.5 5.9 %copy-start.3 = (bf16[256,1024]{1,0:T(8,128)(2,1)S(1)}, bf16[256,1024]{1,0:T(8,128)(2,1)}, u32[]{:S(2)}) copy-start(bf16[256,1024]{1,0:T(8,128)(2,1)} %get-tuple-element.113) | copy-start | bytes 1572868
  223.3 2.1 collective-permute-start.33
  223.5 13.5 %collective-permute-start.29 = (bf16[512,512]{1,0:T(8,128)(2,1)}, bf16[512,512]{1,0:T(8,128)(2,1)}, u32[]{:S(2)}, u32[]{:S(2)}) collective-permute-start(bf16[512,512]{1,0:T(8,128)(2,1)} %slice.233), channel_id=1, source_target_pairs={{0,3},{1,0},{2,1},{3,2},{4,7},{5,4},{6,5},{7,6},{8,11},{9,8},{10,9... | collective-permute-start | bytes 1572872 | tf_op jit(solution)/shard_map/ppermute | solution.py:23
  224.7 14.5 %collective-permute-start.27 = (bf16[512,512]{1,0:T(8,128)(2,1)}, bf16[512,512]{1,0:T(8,128)(2,1)}, u32[]{:S(2)}, u32[]{:S(2)}) collective-permute-start(bf16[512,512]{1,0:T(8,128)(2,1)} %slice.230), channel_id=1, source_target_pairs={{0,1},{1,2},{2,3},{3,0},{4,5},{5,6},{6,7},{7,4},{8,9},{9,10},{10,1... | collective-permute-start | bytes 1572872 | tf_op jit(solution)/shard_map/ppermute | solution.py:23
  239.2 10.3 %collective-permute-start.36 = (bf16[64,1024]{1,0:T(8,128)(2,1)S(1)}, bf16[64,1024]{1,0:T(8,128)(2,1)S(1)}, u32[]{:S(2)}, u32[]{:S(2)}) collective-permute-start(bf16[64,1024]{1,0:T(8,128)(2,1)S(1)} %get-tuple-element.139), channel_id=1, source_target_pairs={{0,3},{1,0},{2,1},{3,2},{4,7},{5,4},{6,5},{7,6},{8,11},{9,8},{10,9... | collective-permute-start | bytes 393224 | tf_op jit(solution)/shard_map/ppermute | solution.py:23
  239.6 10.0 %collective-permute-start.37 = (bf16[64,1024]{1,0:T(8,128)(2,1)S(1)}, bf16[64,1024]{1,0:T(8,128)(2,1)S(1)}, u32[]{:S(2)}, u32[]{:S(2)}) collective-permute-start(bf16[64,1024]{1,0:T(8,128)(2,1)S(1)} %get-tuple-element.141), channel_id=1, source_target_pairs={{0,2},{1,3},{2,0},{3,1},{4,6},{5,7},{6,4},{7,5},{8,10},{9,11},{10,... | collective-permute-start | bytes 393224 | tf_op jit(solution)/shard_map/ppermute | solution.py:23
  240.1 9.4 %collective-permute-start.38 = (bf16[64,1024]{1,0:T(8,128)(2,1)S(1)}, bf16[64,1024]{1,0:T(8,128)(2,1)S(1)}, u32[]{:S(2)}, u32[]{:S(2)}) collective-permute-start(bf16[64,1024]{1,0:T(8,128)(2,1)S(1)} %get-tuple-element.140), channel_id=1, source_target_pairs={{0,1},{1,2},{2,3},{3,0},{4,5},{5,6},{6,7},{7,4},{8,9},{9,10},{10,1... | collective-permute-start | bytes 393224 | tf_op jit(solution)/shard_map/ppermute | solution.py:23
  (7 other events, 9.0 us)
where the time goes:
time: 254 us; the launch traced here: 251 us
  waiting for transfers between devices  71.2 us (28%)
  starting transfers between devices  66.4 us (26%)
  Pallas kernels  62.7 us (25%)
  local copies, waits for them, and re-layouts  20.2 us (8%)
  other arithmetic  14.7 us (6%)
  matrix products  14.6 us (6%)
    ppermute x39, waiting for transfers between devices, send(): return lax.ppermute(value, axis, [(i, (i + step) % n) for i in range(n)])  71.2 us
    ppermute x39, starting transfers between devices, send(): return lax.ppermute(value, axis, [(i, (i + step) % n) for i in range(n)])  49.7 us
    pallas_call x1, Pallas kernels, gated_output(): pl.pallas_call(output_kernel, name='gated_output', grid=(grid,), in_specs...  14 us
    pallas_call x2, Pallas kernels, back_a_rows(): pl.pallas_call(kernel, grid=(width // 512,), in_specs=[pl.BlockSpec((rows...  11.6 us
    dot_general x6, matrix products, mm(): return jnp.dot(a, b, preferred_element_type=F32)  10.8 us
    pallas_call x1, Pallas kernels, projected(): pl.pallas_call(project_kernel, name='projected', grid=(4,), in_specs=[pl....  8.76 us
    all_to_all x1, starting transfers between devices, per_device(): lax.all_to_all(placed_a.reshape(32, ROW, a_width), EP, 0, 0, tiled=False)  8.59 us
    all_to_all x1, starting transfers between devices, per_device(): lax.all_to_all(spread_a.reshape(32, ROW, ra), EP, 0, 0, tiled=False)  8.13 us
  transfers between devices with their start and end apart: 41, of which 13 were waited for; matrix products, arithmetic and copies ran while one was open for 13% of the time, Pallas kernels for 18%

commit v1 on v0

--- a/solution.py
+++ b/solution.py
@@ -12,8 +12,8 @@
 CHUNK = 256
 META = 128
 ROW = 8
-D_B = 1280
-R_B = 1024
+D_B = 768
+R_B = 1152
 F32 = jnp.float32
 BF16 = jnp.bfloat16
 
@@ -268,19 +268,30 @@
     return [top, bottom]
 
 
-def project_kernel(place_ref, own, left, top, bottom, right, w_ref, out_ref):
+def weight_rows(w_ref, place_ref, d, height):
+    start = pl.multiple_of(((place_ref[0] - d) & 3) * height, height)
+    return w_ref[pl.ds(start, height), :]
+
+
+def project_kernel(place_ref, own, left, right, w_ref, out_ref):
     height = own.shape[1]
+    total = None
+    for d, piece in ((0, own), (1, left), (3, right)):
+        product = mm(piece[...], weight_rows(w_ref, place_ref, d, height))
+        total = product if total is None else total + product
+    out_ref[...] = total
+
+
+def finish_kernel(place_ref, part_ref, top, bottom, w_ref, out_ref):
+    height = top.shape[1]
     step = pl.program_id(0)
     cross = jnp.where(step < pl.num_programs(0) // 2, top[...], bottom[...])
-    total = None
-    for d, piece in enumerate((own[...], left[...], cross, right[...])):
-        start = pl.multiple_of(((place_ref[0] - d) & 3) * height, height)
-        product = mm(piece, w_ref[pl.ds(start, height), :])
-        total = product if total is None else total + product
-    out_ref[...] = total.astype(BF16)
-
-
-def projected(place, own, left, top, bottom, right, out_weight):
+    out_ref[...] = (
+        part_ref[...] + mm(cross, weight_rows(w_ref, place_ref, 2, height))
+    ).astype(BF16)
+
+
+def projected(place, own, left, right, out_weight):
     rows, width = own.shape
     cols = out_weight.shape[1]
     step = rows // 4
@@ -289,21 +300,38 @@
         project_kernel,
         name="projected",
         grid=(4,),
+        in_specs=[pl.BlockSpec(memory_space=pltpu.SMEM)]
+        + [whole] * 3
+        + [pl.BlockSpec(memory_space=pltpu.VMEM)],
+        out_specs=pl.BlockSpec((step, cols), lambda i: (i, 0)),
+        out_shape=jax.ShapeDtypeStruct((rows, cols), F32),
+        cost_estimate=pl.CostEstimate(
+            flops=6 * rows * width * cols, bytes_accessed=10 << 20, transcendentals=0
+        ),
+    )(place, own, left, right, out_weight)
+
+
+def finished(place, part, top, bottom, out_weight):
+    rows, cols = part.shape
+    width = top.shape[1]
+    step = rows // 4
+    return pl.pallas_call(
+        finish_kernel,
+        name="finished",
+        grid=(4,),
         in_specs=[
             pl.BlockSpec(memory_space=pltpu.SMEM),
-            whole,
-            whole,
+            pl.BlockSpec((step, cols), lambda i: (i, 0)),
             pl.BlockSpec((step, width), lambda i: (jnp.minimum(i, 1), 0)),
             pl.BlockSpec((step, width), lambda i: (jnp.maximum(i - 2, 0), 0)),
-            whole,
-            pl.BlockSpec(out_weight.shape, lambda i: (0, 0)),
+            pl.BlockSpec(memory_space=pltpu.VMEM),
         ],
         out_specs=pl.BlockSpec((step, cols), lambda i: (i, 0)),
         out_shape=jax.ShapeDtypeStruct((rows, cols), BF16),
         cost_estimate=pl.CostEstimate(
-            flops=8 * rows * width * cols, bytes_accessed=10 << 20, transcendentals=0
-        ),
-    )(place, own, left, top, bottom, right, out_weight)
+            flops=2 * rows * width * cols, bytes_accessed=10 << 20, transcendentals=0
+        ),
+    )(place, part, top, bottom, out_weight)
 
 
 def token_kernel(x_ref, gain_ref, routes_ref, weights_ref, a_ref, b_ref, meta_ref, *, capacity):
@@ -490,63 +518,124 @@
     )(*pieces)
 
 
-def back_b_kernel(hidden_ref, w_ref, o0, o1, o2, o3, swapped_ref, *, unit):
-    side = hidden_ref.shape[0] // 4
+def near_kernel(first, second, third, gate_ref, up_ref, gate_out, up_out, rows_ref):
+    side, width = first.shape
+    for place, piece in enumerate((first, second, third)):
+        rows_ref[side * place : side * place + side, :] = piece[...]
+    rows = rows_ref[...]
+    gate_out[...] = mm(rows, gate_ref[:width, :])
+    up_out[...] = mm(rows, up_ref[:width, :])
+
+
+def near_sums(pieces, gate_w, up_w):
+    side, width = pieces[0].shape
+    inner = gate_w.shape[1]
+    vmem = pl.BlockSpec(memory_space=pltpu.VMEM)
+    return pl.pallas_call(
+        near_kernel,
+        name="near_sums",
+        in_specs=[vmem] * 5,
+        out_specs=(vmem, vmem),
+        out_shape=(jax.ShapeDtypeStruct((3 * side, inner), F32),) * 2,
+        scratch_shapes=[pltpu.VMEM((3 * side, width), BF16)],
+        cost_estimate=pl.CostEstimate(
+            flops=12 * side * width * inner, bytes_accessed=12 << 20, transcendentals=0
+        ),
+    )(*pieces, gate_w, up_w)
+
+
+def hidden_kernel(top, bottom, b_ref, gate_sum, up_sum, gate_ref, up_ref, near_ref, far_ref):
+    half, width = top.shape
+    side = 2 * half
+    far = jnp.concatenate([top[...], bottom[...]], axis=0)
+    b_rows = b_ref[...]
+    gate_b = mm(b_rows, gate_ref[width:, :])
+    up_b = mm(b_rows, up_ref[width:, :])
+    gate_far = mm(far, gate_ref[:width, :]) + gate_b[2 * side : 3 * side]
+    up_far = mm(far, up_ref[:width, :]) + up_b[2 * side : 3 * side]
+    far_ref[...] = (gate_far * jax.nn.sigmoid(gate_far) * up_far).astype(BF16)
+    for place, x in enumerate((0, 1, 3)):
+        low = side * place
+        gate = gate_sum[low : low + side, :] + gate_b[side * x : side * x + side]
+        up = up_sum[low : low + side, :] + up_b[side * x : side * x + side]
+        near_ref[low : low + side, :] = (gate * jax.nn.sigmoid(gate) * up).astype(BF16)
+
+
+def hidden_rows(cross, b_rows, sums, gate_w, up_w):
+    half = cross[0].shape[0]
+    width, inner = gate_w.shape
+    vmem = pl.BlockSpec(memory_space=pltpu.VMEM)
+    return pl.pallas_call(
+        hidden_kernel,
+        name="hidden_rows",
+        in_specs=[vmem] * 7,
+        out_specs=(vmem, vmem),
+        out_shape=(
+            jax.ShapeDtypeStruct((6 * half, inner), BF16),
+            jax.ShapeDtypeStruct((2 * half, inner), BF16),
+        ),
+        cost_estimate=pl.CostEstimate(
+            flops=16 * half * width * inner, bytes_accessed=12 << 20, transcendentals=8 * half * inner
+        ),
+    )(*cross, b_rows, *sums, gate_w, up_w)
+
+
+def back_b_kernel(near_ref, far_ref, w_ref, o0, o1, o2, o3, swapped_ref, *, unit):
+    side = far_ref.shape[0]
     block = 4 * unit
     swap = swap_matrix(side, unit)
     for z in range(4):
+        low = block * z
         part = jnp.concatenate(
-            [hidden_ref[side * x + block * z : side * x + block * z + block, :] for x in range(4)],
+            [
+                near_ref[low : low + block, :],
+                near_ref[side + low : side + low + block, :],
+                far_ref[low : low + block, :],
+                near_ref[2 * side + low : 2 * side + low + block, :],
+            ],
             axis=0,
         )
         turned_part = mm(swap, part).astype(BF16)
         for y in range(4):
-            swapped_ref[side * y + block * z : side * y + block * z + block, :] = turned_part[
+            swapped_ref[side * y + low : side * y + low + block, :] = turned_part[
                 block * y : block * y + block, :
             ]
+    result = mm(swapped_ref[...], w_ref[:, w_ref.shape[1] - o0.shape[1] :]).astype(BF16)
     for y, out in enumerate((o0, o1, o2, o3)):
-        out[...] = mm(swapped_ref[side * y : side * y + side, :], w_ref[...]).astype(BF16)
-
-
-def back_b_rows(hidden, weight, unit):
-    rows, inner = hidden.shape
+        out[...] = result[side * y : side * y + side, :]
+
+
+def back_b_rows(near, far, weight, unit):
+    side, inner = far.shape
     vmem = pl.BlockSpec(memory_space=pltpu.VMEM)
-    shape = jax.ShapeDtypeStruct((rows // 4, R_B), BF16)
-    first = (weight.shape[1] - R_B) // R_B
+    shape = jax.ShapeDtypeStruct((side, R_B), BF16)
     return list(
         pl.pallas_call(
             lambda *refs: back_b_kernel(*refs, unit=unit),
             name="back_b_rows",
-            grid=(1,),
-            in_specs=[
-                pl.BlockSpec((rows, inner), lambda i: (0, 0)),
-                pl.BlockSpec((inner, R_B), lambda i: (0, first)),
-            ],
-            out_specs=(pl.BlockSpec((rows // 4, R_B), lambda i: (0, 0)),) * 4,
+            in_specs=[vmem] * 3,
+            out_specs=(vmem,) * 4,
             out_shape=(shape,) * 4,
-            scratch_shapes=[pltpu.VMEM((rows, inner), BF16)],
+            scratch_shapes=[pltpu.VMEM((4 * side, inner), BF16)],
             cost_estimate=pl.CostEstimate(
                 flops=1 << 30, bytes_accessed=3 << 20, transcendentals=0
             ),
-        )(hidden, weight)
+        )(near, far, weight)
     )
 
 
 def back_a_rows(hidden, weight, width, spans):
-    rows, inner = hidden.shape
+    vmem = pl.BlockSpec(memory_space=pltpu.VMEM)
 
     def kernel(hidden_ref, w_ref, *out_refs):
+        result = mm(hidden_ref[...], w_ref[:, :width]).astype(BF16)
         for (low, high), out in zip(spans, out_refs):
-            out[...] = mm(hidden_ref[low:high, :], w_ref[...]).astype(BF16)
+            out[...] = result[low:high, :]
 
     return pl.pallas_call(
         kernel,
-        grid=(width // 512,),
-        in_specs=[
-            pl.BlockSpec((rows, inner), lambda i: (0, 0)),
-            pl.BlockSpec((inner, 512), lambda i: (0, i)),
-        ],
-        out_specs=tuple(pl.BlockSpec((h - l, 512), lambda i: (0, i)) for l, h in spans),
+        in_specs=[vmem] * 2,
+        out_specs=(vmem,) * len(spans),
         out_shape=tuple(jax.ShapeDtypeStruct((h - l, width), BF16) for l, h in spans),
         cost_estimate=pl.CostEstimate(flops=2 << 30, bytes_accessed=6 << 20, transcendentals=0),
     )(hidden, weight)
@@ -659,74 +748,70 @@
     decay = after(log_decay, placed_a)
     cosine, sine = tables(query.shape[0])
     cum_c, cum_t = running(decay)
-    blocks_b, meta_b = placed_rows(here, got_b, after(other_b, sine), D_B, capacity)
-    got_b = exchange(blocks_b, "ep_0", 1)
-
-    state = local_state(after(keys, blocks_b[0]), values, cosine, sine, cum_t)
+
+    state = local_state(after(keys, sine), values, cosine, sine, cum_t)
     inside, group = core_prefix(state, jnp.sum(decay, axis=1))
     inside, group_z = ring_prefix(inside, group, "ep_1", heads)
+    blocks_b, meta_b = placed_rows(here, got_b, after(other_b, group), D_B, capacity)
 
     compact = compaction(capacity)
-    slots_a = mm(compact, after(got_a, group).reshape(32 * ROW, a_width)).astype(BF16)
+    slots_a = mm(
+        compact, after(got_a, blocks_b[0]).reshape(32 * ROW, a_width)
+    ).astype(BF16)
     left_a, right_a = ring_first(slots_a)
     inside, _ = ring_prefix(inside, after(group_z, slots_a), "ep_0", heads)
-
-    turn_b = regrouped(after(got_b, slots_a))
+    got_b = exchange(blocks_b, "ep_0", 1)
+
+    gated = gated_output(
+        query, keys, values, gate_pre, cosine, sine, cum_c, cum_t, inside[0]
+    )
+    turn_b = regrouped(after(got_b, gated))
     got_b = exchange(turn_b, "ep_1", 1)
-    gated = gated_output(
-        query, keys, values, gate_pre, cosine, sine, cum_c, cum_t, after(inside[0], turn_b[0])
-    )
-    cross_a = ring_second(left_a, right_a, gated)
+    cross_a = ring_second(left_a, right_a, turn_b[0])
     left_g, right_g = ring_first(gated)
 
-    turned_b = turned_rows(after(got_b, gated), unit)
-    gate_h = mm(turned_b, gate_w[a_width:])
-    up_h = mm(turned_b, up_w[a_width:])
-    all_a = jnp.concatenate(after([slots_a, left_a, *cross_a, right_a], gate_h), axis=0)
-    gate_h = gate_h + mm(all_a, gate_w[:a_width])
-    up_h = up_h + mm(all_a, up_w[:a_width])
-    hidden = lax.optimization_barrier((jax.nn.silu(gate_h) * up_h).astype(BF16))
+    side = 4 * block
+    sums = near_sums([slots_a, left_a, right_a], gate_w, up_w)
+    turned_b = turned_rows(after(got_b, sums), unit)
+    near, far = hidden_rows(after(cross_a, turned_b), turned_b, sums, gate_w, up_w)
 
     ra = width - R_B
     half = 2 * block
-    upper, lower = back_a_rows(
-        hidden, down_w, ra, ((8 * block, 10 * block), (10 * block, 12 * block))
-    )
+    upper, lower = back_a_rows(far, down_w, ra, ((0, half), (half, side)))
     upper = send(upper, "tp", -1)
     lower = send(lower, "tp", 1)
-    back_b = back_b_rows(hidden, down_w, unit)
+    back_b = back_b_rows(near, far, down_w, unit)
     got_b = exchange(back_b, "ep_1", -1)
     b0, b1, b3 = back_a_rows(
-        after(hidden, back_b[0]),
-        down_w,
-        ra,
-        ((0, 4 * block), (4 * block, 8 * block), (12 * block, 16 * block)),
+        after(near, back_b[0]), down_w, ra, ((0, side), (side, 2 * side), (2 * side, 3 * side))
     )
     b1 = jnp.concatenate([b1[:half] + upper, b1[half:]], axis=0)
     b3 = jnp.concatenate([b3[:half], b3[half:] + lower], axis=0)
     up_a, down_a = send(b1, "tp", -1), send(b3, "tp", 1)
-    turn_b = regrouped(after(got_b, b1, b3))
+    place = lax.axis_index("tp").astype(jnp.int32)[None]
+    part = projected(place, after(gated, b1, b3), left_g, right_g, out_weight)
+    turn_b = regrouped(after(got_b, part))
     home_b = exchange(turn_b, "ep_0", -1)
     cross_g = ring_second(left_g, right_g, turn_b[0])
-    own_b, other_b = combined_rows(here, home_b, meta_b, capacity)
-    other_b = send(other_b, "ep_2", 1)
-    summed_a = (after(b0, own_b).astype(F32) + up_a.astype(F32) + down_a.astype(F32)).astype(BF16)
+    summed_a = (
+        after(b0, turn_b[0]).astype(F32) + up_a.astype(F32) + down_a.astype(F32)
+    ).astype(BF16)
     spread_a = mm_t(compact, summed_a).astype(BF16)
     home_a = lax.all_to_all(
         spread_a.reshape(32, ROW, ra), EP, 0, 0, tiled=False
     ).reshape(32 * ROW, ra)
-    mixed_b = own_b + after(other_b, spread_a)
-    got_b = exchange(rows_of(mixed_b, 4), "tp", -1)
-    place = lax.axis_index("tp").astype(jnp.int32)[None]
-    mixed = projected(
-        place, gated, left_g, *after(cross_g, mixed_b), right_g, out_weight
-    )
-    final_b = sum(p.astype(F32) for p in got_b)
+    facts_a = after(meta_a, spread_a)
     slot_lane = jnp.arange(32 * ROW, dtype=jnp.int32)[None, :]
     shares = sum(
-        jnp.where(meta_a[:, 4 + r : 5 + r].astype(jnp.int32) == slot_lane, meta_a[:, 2 + r : 3 + r], 0.0)
+        jnp.where(facts_a[:, 4 + r : 5 + r].astype(jnp.int32) == slot_lane, facts_a[:, 2 + r : 3 + r], 0.0)
         for r in range(top)
     ).astype(BF16)
+    own_b, other_b = combined_rows(here, after(home_b, spread_a), meta_b, capacity)
+    other_b = send(other_b, "ep_2", 1)
+    mixed_b = own_b + other_b
+    got_b = exchange(rows_of(mixed_b, 4), "tp", -1)
+    mixed = finished(place, part, *after(cross_g, mixed_b), out_weight)
+    final_b = sum(p.astype(F32) for p in got_b)
     final_a = mm(shares, after(home_a, mixed))
     moe_out = jnp.concatenate([final_a, final_b], axis=1).astype(BF16)
     return (mixed, moe_out)

time: 254 us -> 267 us (1.051)
  Pallas kernels: 62.7 us -> 82.7 us
  matrix products: 14.6 us -> 4.3 us
  waiting for transfers between devices: 71.2 us -> 80.1 us
  local copies, waits for them, and re-layouts: 20.2 us -> 13.1 us
    pallas_call x2 -> x5, Pallas kernels: 11.6 us -> 32.5 us  [the longest x2 9.45 us: back_a_rows(): pl.pallas_call(kernel, in_specs=[vmem] * 2, out_specs=(vmem,) * len(spans...]
    dot_general x6 -> x2, matrix products: 10.8 us -> 0.96 us  [mm(): return jnp.dot(a, b, preferred_element_type=F32)]
    ppermute x39, waiting for transfers between devices: 71.2 us -> 80.1 us  [send(): return lax.ppermute(value, axis, [(i, (i + step) % n) for i in range(n)])]
    ppermute x39, starting transfers between devices: 49.7 us -> 53.8 us  [send(): return lax.ppermute(value, axis, [(i, (i + step) % n) for i in range(n)])]
    all_to_all x1, starting transfers between devices: 8.13 us -> 4.55 us  [per_device(): lax.all_to_all(spread_a.reshape(32, ROW, ra), EP, 0, 0, tiled=False)]
    unnamed x64 -> x42, local copies, waits for them, and re-layouts: 7.48 us -> 4.46 us
  transfers between devices with their start and end apart: 41 -> 41, of which waited for: 13 -> 12; matrix products, arithmetic and copies ran while one was open for 13% -> 10% of each run, Pallas kernels for 18% -> 24%
where the time goes in v1:
time: 267 us; the launch traced here: 262 us
  Pallas kernels  82.7 us (31%)
  waiting for transfers between devices  80.1 us (30%)
  starting transfers between devices  66.7 us (25%)
  other arithmetic  14.5 us (5%)
  local copies, waits for them, and re-layouts  13.1 us (5%)
  matrix products  4.3 us (2%)
    ppermute x39, waiting for transfers between devices, send(): return lax.ppermute(value, axis, [(i, (i + step) % n) for i in range(n)])  80.1 us
    ppermute x39, starting transfers between devices, send(): return lax.ppermute(value, axis, [(i, (i + step) % n) for i in range(n)])  53.8 us
    pallas_call x1, Pallas kernels, gated_output(): pl.pallas_call(output_kernel, name='gated_output', grid=(grid,), in_specs...  14 us
    pallas_call x2, Pallas kernels, back_a_rows(): pl.pallas_call(kernel, in_specs=[vmem] * 2, out_specs=(vmem,) * len(spans...  9.45 us
    pallas_call x1, Pallas kernels, near_sums(): pl.pallas_call(near_kernel, name='near_sums', in_specs=[vmem] * 5, out_sp...  9.02 us
    all_to_all x1, starting transfers between devices, per_device(): lax.all_to_all(placed_a.reshape(32, ROW, a_width), EP, 0, 0, tiled=False)  8.35 us
    pallas_call x1, Pallas kernels, projected(): pl.pallas_call(project_kernel, name='projected', grid=(4,), in_specs=[pl....  8.1 us
    pallas_call x1, Pallas kernels, hidden_rows(): pl.pallas_call(hidden_kernel, name='hidden_rows', in_specs=[vmem] * 7, ou...  7.49 us
  transfers between devices with their start and end apart: 41, of which 12 were waited for; matrix products, arithmetic and copies ran while one was open for 10% of the time, Pallas kernels for 24%

profile of v1, /device:TPU:1, one launch (start us, length us, event | category | flops | bytes accessed | tf_op | source)
XLA Modules:
  0.0 262.5 jit_solution(10400667767295495664)
XLA Ops:
  0.6 3.2 %token_rows.1 = (bf16[256,3328]{1,0:T(8,128)(2,1)}, bf16[64,896]{1,0:T(8,128)(2,1)}, f32[64,128]{1,0:T(8,128)}) custom-call(bf16[64,4096]{1,0:T(8,128)(2,1)} %refs_0_.1, f32[1,4096]{1,0:T(1,128)} %bitcast.56, s32[2,64]{1,0:T(2,128)} %bitcast.58, f32[2,64]{1,0:T(2,128)} %bitcast.59), custom_call_target="tpu_custom_call" | custom-call | flops 16777216 | bytes 1048576 | tf_op jit(solution)/shard_map/token_rows/pallas_call | solution.py:389
  3.8 2.0 collective-permute-start.4
  5.9 2.5 collective-permute-start.5
  8.3 1.2 collective-permute-start.6
  11.4 1.1 copy.18
  12.5 3.0 %fusion.1 = (f32[1024,128]{1,0:T(8,128)}, f32[1024,128]{1,0:T(8,128)}) fusion(f32[128]{0:T(128)S(1)} %compare_select_fusion.6, f32[128]{0:T(128)S(1)} %mul.194, f32[1024]{0:T(1024)S(1)} %add_convert_fusion.5), kind=kLoop, calls=%fused_computation.11 | loop fusion | flops 262144 | bytes 1053696 | tf_op jit(solution)/shard_map/mul | solution.py:246
  15.5 4.8 %local_state.1 = f32[256,128]{1,0:T(8,128)} custom-call(bf16[1024,256]{1,0:T(8,128)(2,1)} %k_ref.2, bf16[1024,512]{1,0:T(8,128)(2,1)} %v_ref.3, f32[1024,128]{1,0:T(8,128)} %get-tuple-element.153.cos_ref, f32[1024,128]{1,0:T(8,128)} %get-tuple-element.152.sin_ref, f32[1024,4]{1,0:T(8,128)} %bitcast.53), custom_call_target="tpu_custom_call" | custom-call | flops 134217728 | bytes 3145728 | tf_op jit(solution)/shard_map/local_state/pallas_call | solution.py:135
  20.4 0.9 convert_element_type.165
  21.5 1.6 collective-permute-start
  23.1 8.3 %all-to-all-start = ((bf16[32,8,3328]{2,1,0:T(8,128)(2,1)}), bf16[32,8,3328]{2,1,0:T(8,128)(2,1)S(1)}, u32[]{:S(2)}, u32[]{:S(2)}) async-start(bf16[32,8,3328]{2,1,0:T(8,128)(2,1)} %bitcast.16), calls=%async_computation | async-start | bytes 3407872 | tf_op jit(solution)/shard_map/all_to_all | solution.py:744
  32.8 2.6 %collective-permute-start.3 = (bf16[264,128]{1,0:T(8,128)(2,1)S(1)}, bf16[264,128]{1,0:T(8,128)(2,1)S(1)}, u32[]{:S(2)}, u32[]{:S(2)}) collective-permute-start(bf16[264,128]{1,0:T(8,128)(2,1)S(1)} %pad_maximum_fusion.5), channel_id=1, source_target_pairs={{0,24},{8,0},{16,8},{24,16},{1,25},{9,1},{17,9},{25,17},{2,26},{10... | collective-permute-start | bytes 202760 | tf_op jit(solution)/shard_map/ppermute | solution.py:23
  36.6 1.3 collective-permute-start.7
  38.0 15.8 %collective-permute-done.3 = bf16[264,128]{1,0:T(8,128)(2,1)S(1)} collective-permute-done((bf16[264,128]{1,0:T(8,128)(2,1)S(1)}, bf16[264,128]{1,0:T(8,128)(2,1)S(1)}, u32[]{:S(2)}, u32[]{:S(2)}) %collective-permute-start.3) | collective-permute-done | bytes 67616 | tf_op jit(solution)/shard_map/ppermute | solution.py:23
  53.9 2.0 collective-permute-done.2
  57.9 3.0 %placed_rows.1 = (bf16[192,768]{1,0:T(8,128)(2,1)}, bf16[192,768]{1,0:T(8,128)(2,1)}, bf16[192,768]{1,0:T(8,128)(2,1)}, bf16[192,768]{1,0:T(8,128)(2,1)}, bf16[512,128]{1,0:T(8,128)(2,1)}) custom-call(s32[3]{0:T(128)} %pad_add_fusion.refs_0_, bf16[64,896]{1,0:T(8,128)(2,1)} %get-tuple-element.70.refs_1_, bf16[64,896]{1,0:T(8,128)(2,1)} %copy-done.15, ...), custom_call_target="tpu_custom_call" | custom-call | flops 1073741824 | bytes 4194304 | tf_op jit(solution)/shard_map/placed_rows/pallas_call | solution.py:448
  61.4 1.8 collective-permute-start.8
  65.2 1.6 collective-permute-start.13
  66.8 1.7 collective-permute-start.10
  68.5 0.9 collective-permute-start.9
  69.8 11.9 %collective-permute-done.9 = bf16[264,128]{1,0:T(8,128)(2,1)} collective-permute-done((bf16[264,128]{1,0:T(8,128)(2,1)}, bf16[264,128]{1,0:T(8,128)(2,1)}, u32[]{:S(2)}, u32[]{:S(2)}) %collective-permute-start.9) | collective-permute-done | bytes 67616 | tf_op jit(solution)/shard_map/ppermute | solution.py:23
  83.1 1.8 fusion.13.inc_ref
  84.9 14.0 %gated_output.1.own = bf16[1024,512]{1,0:T(8,128)(2,1)} custom-call(bf16[1024,256]{1,0:T(8,128)(2,1)} %q_ref.1, bf16[1024,256]{1,0:T(8,128)(2,1)} %k_ref.2, bf16[1024,512]{1,0:T(8,128)(2,1)} %v_ref.3, bf16[1024,512]{1,0:T(8,128)(2,1)} %g_ref.1, f32[1024,128]{1,0:T(8,128)} %get-tuple-element.153.cos_ref, f32[1024,128]{1,0:T(8,128)} %get-tuple-element.152.sin_ref, ...), custom_call_target="tpu_custom_call" | custom-call | flops 10000000000 | bytes 5242880 | tf_op jit(solution)/shard_map/gated_output/pallas_call | solution.py:160
  99.8 2.3 regrouped.2
  102.1 0.9 slice.198
  103.4 1.5 collective-permute-start.15
  104.8 4.8 %collective-permute-done.16.third = bf16[192,3328]{1,0:T(8,128)(2,1)} collective-permute-done((bf16[192,3328]{1,0:T(8,128)(2,1)S(1)}, bf16[192,3328]{1,0:T(8,128)(2,1)}, u32[]{:S(2)}, u32[]{:S(2)}) %collective-permute-start.16) | collective-permute-done | bytes 1277984 | tf_op jit(solution)/shard_map/ppermute | solution.py:23
  109.6 1.1 slice.199
  110.8 1.6 collective-permute-start.17
  112.3 2.0 collective-permute-start.18
  114.3 1.7 collective-permute-start.19
  116.7 9.0 %near_sums.1 = (f32[576,384]{1,0:T(8,128)}, f32[576,384]{1,0:T(8,128)}) custom-call(bf16[192,3328]{1,0:T(8,128)(2,1)} %copy-done, bf16[192,3328]{1,0:T(8,128)(2,1)} %copy-done.8, bf16[192,3328]{1,0:T(8,128)(2,1)} %collective-permute-done.16.third, bf16[4096,384]{1,0:T(8,128)(2,1)} %bitcast.49, bf16[4096,384]{1,0:T(8,128)(2,1)} %bitcast.51), custom_call_target="tpu_custom_call" | custom-call | flops 2944401408 | bytes 12582912 | tf_op jit(solution)/shard_map/near_sums/pallas_call | solution.py:534
  125.7 1.7 collective-permute-done.19.refs_2_
  128.7 2.8 %turned_rows.1.b_ref = bf16[768,768]{1,0:T(8,128)(2,1)} custom-call(bf16[192,768]{1,0:T(8,128)(2,1)} %get-tuple-element.90.refs_0_, bf16[192,768]{1,0:T(8,128)(2,1)} %copy-done.9, bf16[192,768]{1,0:T(8,128)(2,1)} %copy-done.10, bf16[192,768]{1,0:T(8,128)(2,1)} %copy-done.11), custom_call_target="tpu_custom_call" | custom-call | flops 536870912 | bytes 4194304 | tf_op jit(solution)/shard_map/turned_rows/pallas_call | solution.py:511
  132.4 0.9 copy-done.4
  133.2 7.5 %hidden_rows.1 = (bf16[576,384]{1,0:T(8,128)(2,1)}, bf16[192,384]{1,0:T(8,128)(2,1)}) custom-call(bf16[96,3328]{1,0:T(8,128)(2,1)} %copy-done.3, bf16[96,3328]{1,0:T(8,128)(2,1)} %copy-done.4, bf16[768,768]{1,0:T(8,128)(2,1)} %turned_rows.1.b_ref, f32[576,384]{1,0:T(8,128)} %get-tuple-element.88.gate_sum, f32[576,384]{1,0:T(8,128)} %get-tuple-element.89.up_sum, ...), custom_call_target="tpu_custom_call" | custom-call | flops 2415919104 | bytes 12582912 | tf_op jit(solution)/shard_map/hidden_rows/pallas_call | solution.py:568
  140.7 3.7 %shard_map.141 = (bf16[96,2944]{1,0:T(8,128)(2,1)}, bf16[96,2944]{1,0:T(8,128)(2,1)}) custom-call(bf16[192,384]{1,0:T(8,128)(2,1)} %get-tuple-element.97.refs_1_.hidden_ref, bf16[384,4096]{1,0:T(8,128)(2,1)} %bitcast.60), custom_call_target="tpu_custom_call" | custom-call | flops 2147483648 | bytes 6291456 | tf_op jit(solution)/shard_map/pallas_call | solution.py:635
  144.8 1.1 collective-permute-start.22
  145.9 2.7 %collective-permute-start.24 = (bf16[1024,512]{1,0:T(8,128)(2,1)}, bf16[1024,512]{1,0:T(8,128)(2,1)}, u32[]{:S(2)}, u32[]{:S(2)}) collective-permute-start(bf16[1024,512]{1,0:T(8,128)(2,1)} %gated_output.1.own), channel_id=1, source_target_pairs={{0,3},{1,0},{2,1},{3,2},{4,7},{5,4},{6,5},{7,6},{8,11},{9,8},{10,9... | collective-permute-start | bytes 3145736 | tf_op jit(solution)/shard_map/ppermute | solution.py:23
  148.6 4.6 %back_b_rows.1 = (bf16[192,1152]{1,0:T(8,128)(2,1)}, bf16[192,1152]{1,0:T(8,128)(2,1)}, bf16[192,1152]{1,0:T(8,128)(2,1)}, bf16[192,1152]{1,0:T(8,128)(2,1)}) custom-call(bf16[576,384]{1,0:T(8,128)(2,1)} %get-tuple-element.99.refs_0_.hidden_ref, bf16[192,384]{1,0:T(8,128)(2,1)} %get-tuple-element.97.refs_1_.hidden_ref, bf16[384,4096]{1,0:T(8,128)(2,1)} %bitcast.61), custom_call_target="tpu_custom_call" | custom-call | flops 1073741824 | bytes 3145728 | tf_op jit(solution)/shard_map/back_b_rows/pallas_call | solution.py:613
  153.2 5.7 %shard_map.140 = (bf16[192,2944]{1,0:T(8,128)(2,1)}, bf16[192,2944]{1,0:T(8,128)(2,1)}, bf16[192,2944]{1,0:T(8,128)(2,1)}) custom-call(bf16[576,384]{1,0:T(8,128)(2,1)} %get-tuple-element.99.refs_0_.hidden_ref, bf16[384,4096]{1,0:T(8,128)(2,1)} %bitcast.62), custom_call_target="tpu_custom_call" | custom-call | flops 2147483648 | bytes 6291456 | tf_op jit(solution)/shard_map/pallas_call | solution.py:635
  158.9 1.8 slice_add_fusion.1
  160.9 1.1 pad_maximum_fusion
  162.0 2.7 %collective-permute-start.33 = (bf16[192,2944]{1,0:T(8,128)(2,1)}, bf16[192,2944]{1,0:T(8,128)(2,1)}, u32[]{:S(2)}, u32[]{:S(2)}) collective-permute-start(bf16[192,2944]{1,0:T(8,128)(2,1)} %pad_maximum_fusion), channel_id=1, source_target_pairs={{0,3},{1,0},{2,1},{3,2},{4,7},{5,4},{6,5},{7,6},{8,11},{9,8},{10,9... | collective-permute-start | bytes 3391496 | tf_op jit(solution)/shard_map/ppermute | solution.py:23
  164.7 4.0 %collective-permute-start.25 = (bf16[192,1152]{1,0:T(8,128)(2,1)}, bf16[192,1152]{1,0:T(8,128)(2,1)}, u32[]{:S(2)}, u32[]{:S(2)}) collective-permute-start(bf16[192,1152]{1,0:T(8,128)(2,1)} %get-tuple-element.105), channel_id=1, source_target_pairs={{0,24},{8,0},{16,8},{24,16},{1,25},{9,1},{17,9},{25,17},{2,26},{10... | collective-permute-start | bytes 1327112 | tf_op jit(solution)/shard_map/ppermute | solution.py:23
  168.6 11.9 %collective-permute-done.23.left = bf16[1024,512]{1,0:T(8,128)(2,1)} collective-permute-done((bf16[1024,512]{1,0:T(8,128)(2,1)}, bf16[1024,512]{1,0:T(8,128)(2,1)}, u32[]{:S(2)}, u32[]{:S(2)}) %collective-permute-start.23) | collective-permute-done | bytes 1048608 | tf_op jit(solution)/shard_map/ppermute | solution.py:23
  180.5 1.4 collective-permute-start.26
  181.8 4.2 %collective-permute-start.27 = (bf16[192,1152]{1,0:T(8,128)(2,1)}, bf16[192,1152]{1,0:T(8,128)(2,1)}, u32[]{:S(2)}, u32[]{:S(2)}) collective-permute-start(bf16[192,1152]{1,0:T(8,128)(2,1)} %get-tuple-element.107), channel_id=1, source_target_pairs={{0,8},{8,16},{16,24},{24,0},{1,9},{9,17},{17,25},{25,1},{2,10},{10... | collective-permute-start | bytes 1327112 | tf_op jit(solution)/shard_map/ppermute | solution.py:23
  186.0 8.1 %projected.1.part_ref = f32[1024,1024]{1,0:T(8,128)} custom-call(s32[1]{0:T(128)} %bitcast.place_ref, bf16[1024,512]{1,0:T(8,128)(2,1)} %gated_output.1.own, bf16[1024,512]{1,0:T(8,128)(2,1)} %collective-permute-done.23.left, bf16[1024,512]{1,0:T(8,128)(2,1)} %collective-permute-done.24.right, bf16[2048,1024]{1,0:T(8,128)(2,1)} %w_ref.3), custom_call_target="tpu_custom_call" | custom-call | flops 3221225472 | bytes 10485760 | tf_op jit(solution)/shard_map/projected/pallas_call | solution.py:299
  194.2 6.5 %collective-permute-done.27.i3 = bf16[192,1152]{1,0:T(8,128)(2,1)} collective-permute-done((bf16[192,1152]{1,0:T(8,128)(2,1)}, bf16[192,1152]{1,0:T(8,128)(2,1)}, u32[]{:S(2)}, u32[]{:S(2)}) %collective-permute-start.27) | collective-permute-done | bytes 442400 | tf_op jit(solution)/shard_map/ppermute | solution.py:23
  200.7 2.7 %regrouped.3 = (bf16[192,1152]{1,0:T(8,128)(2,1)}, bf16[192,1152]{1,0:T(8,128)(2,1)}, bf16[192,1152]{1,0:T(8,128)(2,1)}, bf16[192,1152]{1,0:T(8,128)(2,1)}) custom-call(bf16[192,1152]{1,0:T(8,128)(2,1)} %get-tuple-element.108.i0, bf16[192,1152]{1,0:T(8,128)(2,1)} %collective-permute-done.25.i1, bf16[192,1152]{1,0:T(8,128)(2,1)} %collective-permute-done.26.i2, ...), custom_call_target="tpu_custom_call" | custom-call | flops 1048576 | bytes 4194304 | tf_op jit(solution)/shard_map/regrouped/pallas_call | solution.py:472
  203.4 3.5 %collective-permute-start.31 = (bf16[192,1152]{1,0:T(8,128)(2,1)}, bf16[192,1152]{1,0:T(8,128)(2,1)}, u32[]{:S(2)}, u32[]{:S(2)}) collective-permute-start(bf16[192,1152]{1,0:T(8,128)(2,1)} %get-tuple-element.116), channel_id=1, source_target_pairs={{0,64},{32,96},{64,0},{96,32},{1,65},{33,97},{65,1},{97,33},{2,66}... | collective-permute-start | bytes 1327112 | tf_op jit(solution)/shard_map/ppermute | solution.py:23
  206.9 0.9 collective-permute-start.32
  207.8 3.2 %convolution_convert_fusion.1 = bf16[256,2944]{1,0:T(8,128)(2,1)} fusion(bf16[192,2944]{1,0:T(8,128)(2,1)S(1)} %collective-permute-done.34, bf16[192,2944]{1,0:T(8,128)(2,1)} %collective-permute-done.33, bf16[192,2944]{1,0:T(8,128)(2,1)S(1)} %copy-done.2, s32[192]{0:T(256)S(1)} %copy-done.19), kind=kOutput, calls=%fused_computation.1 | convolution fusion | flops 293601280 | bytes 4899584 | tf_op jit(solution)/shard_map/dot_general | solution.py:35
  211.7 3.1 %collective-permute-done.31.refs_3_ = bf16[192,1152]{1,0:T(8,128)(2,1)} collective-permute-done((bf16[192,1152]{1,0:T(8,128)(2,1)}, bf16[192,1152]{1,0:T(8,128)(2,1)}, u32[]{:S(2)}, u32[]{:S(2)}) %collective-permute-start.31) | collective-permute-done | bytes 442400 | tf_op jit(solution)/shard_map/ppermute | solution.py:23
  214.9 12.4 %collective-permute-done.32.refs_4_ = bf16[192,1152]{1,0:T(8,128)(2,1)} collective-permute-done((bf16[192,1152]{1,0:T(8,128)(2,1)}, bf16[192,1152]{1,0:T(8,128)(2,1)}, u32[]{:S(2)}, u32[]{:S(2)}) %collective-permute-start.32) | collective-permute-done | bytes 442400 | tf_op jit(solution)/shard_map/ppermute | solution.py:23
  227.3 4.6 %combined_rows.1 = (bf16[256,1152]{1,0:T(8,128)(2,1)}, bf16[256,1152]{1,0:T(8,128)(2,1)}) custom-call(s32[3]{0:T(128)} %pad_add_fusion.refs_0_, bf16[192,1152]{1,0:T(8,128)(2,1)} %get-tuple-element.120.refs_1_, bf16[192,1152]{1,0:T(8,128)(2,1)} %collective-permute-done.30.refs_2_, bf16[192,1152]{1,0:T(8,128)(2,1)} %collective-permute-done.31.refs_3_, ...), custom_call_target="tpu_custom_call" | custom-call | flops 1073741824 | bytes 4194304 | tf_op jit(solution)/shard_map/combined_rows/pallas_call | solution.py:680
  232.4 4.5 %all-to-all-start.1 = ((bf16[32,8,2944]{2,1,0:T(8,128)(2,1)}), bf16[32,8,2944]{2,1,0:T(8,128)(2,1)S(1)}, u32[]{:S(2)}, u32[]{:S(2)}) async-start(bf16[32,8,2944]{2,1,0:T(8,128)(2,1)} %bitcast.24), calls=%async_computation.1 | async-start | bytes 3014656 | tf_op jit(solution)/shard_map/all_to_all | solution.py:800
  237.0 1.1 slice.200
  238.1 1.1 slice.201
  239.5 2.4 collective-permute-start.29
  242.4 1.2 collective-permute-start.37
  243.6 1.5 collective-permute-start.36
  245.3 8.5 %collective-permute-done.28.top = bf16[512,512]{1,0:T(8,128)(2,1)S(1)} collective-permute-done((bf16[512,512]{1,0:T(8,128)(2,1)S(1)}, bf16[512,512]{1,0:T(8,128)(2,1)S(1)}, u32[]{:S(2)}, u32[]{:S(2)}) %collective-permute-start.28) | collective-permute-done | bytes 524320 | tf_op jit(solution)/shard_map/ppermute | solution.py:23
  254.5 6.6 %finished.1 = bf16[1024,1024]{1,0:T(8,128)(2,1)} custom-call(s32[1]{0:T(128)} %bitcast.place_ref, f32[1024,1024]{1,0:T(8,128)} %projected.1.part_ref, bf16[512,512]{1,0:T(8,128)(2,1)} %copy-done.6, bf16[512,512]{1,0:T(8,128)(2,1)} %collective-permute-done.29.bottom, bf16[2048,1024]{1,0:T(8,128)(2,1)} %w_ref.3), custom_call_target="tpu_custom_call" | custom-call | flops 1073741824 | bytes 10485760 | tf_op jit(solution)/shard_map/finished/pallas_call | solution.py:318
  (159 shorter events, 19.9 us)
Async XLA Ops:
  3.8 32.1 %collective-permute-start.4 = (bf16[64,896]{1,0:T(8,128)(2,1)}, bf16[64,896]{1,0:T(8,128)(2,1)S(1)}, u32[]{:S(2)}, u32[]{:S(2)}) collective-permute-start(bf16[64,896]{1,0:T(8,128)(2,1)} %get-tuple-element.70.refs_1_), channel_id=1, source_target_pairs={{0,1},{1,2},{2,3},{3,0},{4,5},{5,6},{6,7},{7,4},{8,9},{9,10},{10,1... | collective-permute-start | bytes 344072 | tf_op jit(solution)/shard_map/ppermute | solution.py:23
  5.9 30.7 %collective-permute-start.5 = (bf16[64,896]{1,0:T(8,128)(2,1)}, bf16[64,896]{1,0:T(8,128)(2,1)S(1)}, u32[]{:S(2)}, u32[]{:S(2)}) collective-permute-start(bf16[64,896]{1,0:T(8,128)(2,1)} %get-tuple-element.70.refs_1_), channel_id=1, source_target_pairs={{0,2},{1,3},{2,0},{3,1},{4,6},{5,7},{6,4},{7,5},{8,10},{9,11},{10,... | collective-permute-start | bytes 344072 | tf_op jit(solution)/shard_map/ppermute | solution.py:23
  8.3 28.3 %collective-permute-start.6 = (bf16[64,896]{1,0:T(8,128)(2,1)}, bf16[64,896]{1,0:T(8,128)(2,1)S(1)}, u32[]{:S(2)}, u32[]{:S(2)}) collective-permute-start(bf16[64,896]{1,0:T(8,128)(2,1)} %get-tuple-element.70.refs_1_), channel_id=1, source_target_pairs={{0,3},{1,0},{2,1},{3,2},{4,7},{5,4},{6,5},{7,6},{8,11},{9,8},{10,9... | collective-permute-start | bytes 344072 | tf_op jit(solution)/shard_map/ppermute | solution.py:23
  21.5 10.7 %collective-permute-start = (bf16[264,128]{1,0:T(8,128)(2,1)S(1)}, bf16[264,128]{1,0:T(8,128)(2,1)S(1)}, u32[]{:S(2)}, u32[]{:S(2)}) collective-permute-start(bf16[264,128]{1,0:T(8,128)(2,1)S(1)} %pad_maximum_fusion.4), channel_id=1, source_target_pairs={{0,4},{4,0},{1,5},{5,1},{2,6},{6,2},{3,7},{7,3},{8,12},{12,8},{9,1... | collective-permute-start | bytes 202760 | tf_op jit(solution)/shard_map/ppermute | solution.py:23
  23.1 9.5 %copy-start.1 = (f32[256,128]{1,0:T(8,128)S(1)}, f32[256,128]{1,0:T(8,128)}, u32[]{:S(2)}) copy-start(f32[256,128]{1,0:T(8,128)} %local_state.1) | copy-start | bytes 393220
  23.1 13.5 %copy-start.14 = (bf16[64,896]{1,0:T(8,128)(2,1)S(1)}, bf16[64,896]{1,0:T(8,128)(2,1)}, u32[]{:S(2)}) copy-start(bf16[64,896]{1,0:T(8,128)(2,1)} %get-tuple-element.70.refs_1_) | copy-start | bytes 344068
  23.1 37.8 %all-to-all-start = ((bf16[32,8,3328]{2,1,0:T(8,128)(2,1)}), bf16[32,8,3328]{2,1,0:T(8,128)(2,1)S(1)}, u32[]{:S(2)}, u32[]{:S(2)}) async-start(bf16[32,8,3328]{2,1,0:T(8,128)(2,1)} %bitcast.16), calls=%async_computation | async-start | bytes 3407872 | tf_op jit(solution)/shard_map/all_to_all | solution.py:744
  31.6 29.3 %copy-start.18 = (s32[192]{0:T(256)}, s32[192]{0:T(256)S(1)}, u32[]{:S(2)}) copy-start(s32[192]{0:T(256)S(1)} %fusion.28) | copy-start | bytes 2308
  32.8 21.0 %collective-permute-start.3 = (bf16[264,128]{1,0:T(8,128)(2,1)S(1)}, bf16[264,128]{1,0:T(8,128)(2,1)S(1)}, u32[]{:S(2)}, u32[]{:S(2)}) collective-permute-start(bf16[264,128]{1,0:T(8,128)(2,1)S(1)} %pad_maximum_fusion.5), channel_id=1, source_target_pairs={{0,24},{8,0},{16,8},{24,16},{1,25},{9,1},{17,9},{25,17},{2,26},{10... | collective-permute-start | bytes 202760 | tf_op jit(solution)/shard_map/ppermute | solution.py:23
  35.4 20.4 %collective-permute-start.2 = (bf16[264,128]{1,0:T(8,128)(2,1)S(1)}, bf16[264,128]{1,0:T(8,128)(2,1)S(1)}, u32[]{:S(2)}, u32[]{:S(2)}) collective-permute-start(bf16[264,128]{1,0:T(8,128)(2,1)S(1)} %pad_maximum_fusion.5), channel_id=1, source_target_pairs={{0,16},{8,24},{16,0},{24,8},{1,17},{9,25},{17,1},{25,9},{2,18},{10... | collective-permute-start | bytes 202760 | tf_op jit(solution)/shard_map/ppermute | solution.py:23
  36.0 21.9 %copy-start.15 = (bf16[64,896]{1,0:T(8,128)(2,1)}, bf16[64,896]{1,0:T(8,128)(2,1)S(1)}, u32[]{:S(2)}) copy-start(bf16[64,896]{1,0:T(8,128)(2,1)S(1)} %collective-permute-done.4.refs_2_) | copy-start | bytes 344068
  36.0 20.0 %collective-permute-start.1 = (bf16[264,128]{1,0:T(8,128)(2,1)S(1)}, bf16[264,128]{1,0:T(8,128)(2,1)S(1)}, u32[]{:S(2)}, u32[]{:S(2)}) collective-permute-start(bf16[264,128]{1,0:T(8,128)(2,1)S(1)} %pad_maximum_fusion.5), channel_id=1, source_target_pairs={{0,8},{8,16},{16,24},{24,0},{1,9},{9,17},{17,25},{25,1},{2,10},{10... | collective-permute-start | bytes 202760 | tf_op jit(solution)/shard_map/ppermute | solution.py:23
  36.6 21.3 %copy-start.16 = (bf16[64,896]{1,0:T(8,128)(2,1)}, bf16[64,896]{1,0:T(8,128)(2,1)S(1)}, u32[]{:S(2)}) copy-start(bf16[64,896]{1,0:T(8,128)(2,1)S(1)} %collective-permute-done.5.refs_3_) | copy-start | bytes 344068
  36.6 21.3 %copy-start.17 = (bf16[64,896]{1,0:T(8,128)(2,1)}, bf16[64,896]{1,0:T(8,128)(2,1)S(1)}, u32[]{:S(2)}) copy-start(bf16[64,896]{1,0:T(8,128)(2,1)S(1)} %collective-permute-done.6.refs_4_) | copy-start | bytes 344068
  36.6 21.2 %collective-permute-start.7 = (bf16[256,896]{1,0:T(8,128)(2,1)S(1)}, bf16[256,896]{1,0:T(8,128)(2,1)}, u32[]{:S(2)}, u32[]{:S(2)}) collective-permute-start(bf16[256,896]{1,0:T(8,128)(2,1)S(1)} %pad_maximum_fusion.3), channel_id=1, source_target_pairs={{0,4},{4,0},{1,5},{5,1},{2,6},{6,2},{3,7},{7,3},{8,12},{12,8},{9,1... | collective-permute-start | bytes 1376264 | tf_op jit(solution)/shard_map/ppermute | solution.py:23
  61.4 37.5 %copy-start = (bf16[192,3328]{1,0:T(8,128)(2,1)}, bf16[192,3328]{1,0:T(8,128)(2,1)S(1)}, u32[]{:S(2)}) copy-start(bf16[192,3328]{1,0:T(8,128)(2,1)S(1)} %convolution_convert_fusion.first) | copy-start | bytes 3833860
  61.4 8.0 %collective-permute-start.8 = (bf16[264,128]{1,0:T(8,128)(2,1)}, bf16[264,128]{1,0:T(8,128)(2,1)S(1)}, u32[]{:S(2)}, u32[]{:S(2)}) collective-permute-start(bf16[264,128]{1,0:T(8,128)(2,1)} %pad_maximum_fusion.6), channel_id=1, source_target_pairs={{0,32},{32,64},{64,96},{96,0},{1,33},{33,65},{65,97},{97,1},{2,34}... | collective-permute-start | bytes 202760 | tf_op jit(solution)/shard_map/ppermute | solution.py:23
  64.4 34.5 %collective-permute-start.12 = (bf16[192,768]{1,0:T(8,128)(2,1)}, bf16[192,768]{1,0:T(8,128)(2,1)S(1)}, u32[]{:S(2)}, u32[]{:S(2)}) collective-permute-start(bf16[192,768]{1,0:T(8,128)(2,1)} %get-tuple-element.75), channel_id=1, source_target_pairs={{0,32},{32,64},{64,96},{96,0},{1,33},{33,65},{65,97},{97,1},{2,34}... | collective-permute-start | bytes 884744 | tf_op jit(solution)/shard_map/ppermute | solution.py:23
  65.2 33.8 %collective-permute-start.13 = (bf16[192,768]{1,0:T(8,128)(2,1)}, bf16[192,768]{1,0:T(8,128)(2,1)S(1)}, u32[]{:S(2)}, u32[]{:S(2)}) collective-permute-start(bf16[192,768]{1,0:T(8,128)(2,1)} %get-tuple-element.76), channel_id=1, source_target_pairs={{0,64},{32,96},{64,0},{96,32},{1,65},{33,97},{65,1},{97,33},{2,66}... | collective-permute-start | bytes 884744 | tf_op jit(solution)/shard_map/ppermute | solution.py:23
  66.8 16.1 %collective-permute-start.10 = (bf16[264,128]{1,0:T(8,128)(2,1)}, bf16[264,128]{1,0:T(8,128)(2,1)}, u32[]{:S(2)}, u32[]{:S(2)}) collective-permute-start(bf16[264,128]{1,0:T(8,128)(2,1)} %pad_maximum_fusion.6), channel_id=1, source_target_pairs={{0,96},{32,0},{64,32},{96,64},{1,97},{33,1},{65,33},{97,65},{2,98}... | collective-permute-start | bytes 202760 | tf_op jit(solution)/shard_map/ppermute | solution.py:23
  68.5 13.2 %collective-permute-start.9 = (bf16[264,128]{1,0:T(8,128)(2,1)}, bf16[264,128]{1,0:T(8,128)(2,1)}, u32[]{:S(2)}, u32[]{:S(2)}) collective-permute-start(bf16[264,128]{1,0:T(8,128)(2,1)} %pad_maximum_fusion.6), channel_id=1, source_target_pairs={{0,64},{32,96},{64,0},{96,32},{1,65},{33,97},{65,1},{97,33},{2,66}... | collective-permute-start | bytes 202760 | tf_op jit(solution)/shard_map/ppermute | solution.py:23
  69.5 32.6 %collective-permute-start.11 = (bf16[192,3328]{1,0:T(8,128)(2,1)S(1)}, bf16[192,3328]{1,0:T(8,128)(2,1)S(1)}, u32[]{:S(2)}, u32[]{:S(2)}) collective-permute-start(bf16[192,3328]{1,0:T(8,128)(2,1)S(1)} %convolution_convert_fusion.first), channel_id=1, source_target_pairs={{0,1},{1,2},{2,3},{3,0},{4,5},{5,6},{6,7},{7,4},{8,9},{9,10},{10,1... | collective-permute-start | bytes 3833864 | tf_op jit(solution)/shard_map/ppermute | solution.py:23
  81.7 27.9 %collective-permute-start.16 = (bf16[192,3328]{1,0:T(8,128)(2,1)S(1)}, bf16[192,3328]{1,0:T(8,128)(2,1)}, u32[]{:S(2)}, u32[]{:S(2)}) collective-permute-start(bf16[192,3328]{1,0:T(8,128)(2,1)S(1)} %convolution_convert_fusion.first), channel_id=1, source_target_pairs={{0,3},{1,0},{2,1},{3,2},{4,7},{5,4},{6,5},{7,6},{8,11},{9,8},{10,9... | collective-permute-start | bytes 3833864 | tf_op jit(solution)/shard_map/ppermute | solution.py:23
  82.9 16.1 %collective-permute-start.14 = (bf16[192,768]{1,0:T(8,128)(2,1)}, bf16[192,768]{1,0:T(8,128)(2,1)}, u32[]{:S(2)}, u32[]{:S(2)}) collective-permute-start(bf16[192,768]{1,0:T(8,128)(2,1)} %get-tuple-element.77), channel_id=1, source_target_pairs={{0,96},{32,0},{64,32},{96,64},{1,97},{33,1},{65,33},{97,65},{2,98}... | collective-permute-start | bytes 884744 | tf_op jit(solution)/shard_map/ppermute | solution.py:23
  99.0 0.7 copy-start.12
  99.0 0.8 copy-start.13
  102.0 14.0 %copy-start.20 = (bf16[192,768]{1,0:T(8,128)(2,1)S(1)}, bf16[192,768]{1,0:T(8,128)(2,1)}, u32[]{:S(2)}) copy-start(bf16[192,768]{1,0:T(8,128)(2,1)} %get-tuple-element.87) | copy-start | bytes 884740
  102.0 1.3 copy-start.8
  103.4 28.1 %collective-permute-start.15 = (bf16[96,3328]{1,0:T(8,128)(2,1)}, bf16[96,3328]{1,0:T(8,128)(2,1)S(1)}, u32[]{:S(2)}, u32[]{:S(2)}) collective-permute-start(bf16[96,3328]{1,0:T(8,128)(2,1)} %slice.198), channel_id=1, source_target_pairs={{0,1},{1,2},{2,3},{3,0},{4,5},{5,6},{6,7},{7,4},{8,9},{9,10},{10,1... | collective-permute-start | bytes 1916936 | tf_op jit(solution)/shard_map/ppermute | solution.py:23
  110.8 20.7 %collective-permute-start.17 = (bf16[96,3328]{1,0:T(8,128)(2,1)S(1)}, bf16[96,3328]{1,0:T(8,128)(2,1)S(1)}, u32[]{:S(2)}, u32[]{:S(2)}) collective-permute-start(bf16[96,3328]{1,0:T(8,128)(2,1)S(1)} %slice.199), channel_id=1, source_target_pairs={{0,3},{1,0},{2,1},{3,2},{4,7},{5,4},{6,5},{7,6},{8,11},{9,8},{10,9... | collective-permute-start | bytes 1916936 | tf_op jit(solution)/shard_map/ppermute | solution.py:23
  112.3 13.4 %collective-permute-start.18 = (bf16[192,768]{1,0:T(8,128)(2,1)}, bf16[192,768]{1,0:T(8,128)(2,1)S(1)}, u32[]{:S(2)}, u32[]{:S(2)}) collective-permute-start(bf16[192,768]{1,0:T(8,128)(2,1)} %get-tuple-element.85), channel_id=1, source_target_pairs={{0,8},{8,16},{16,24},{24,0},{1,9},{9,17},{17,25},{25,1},{2,10},{10... | collective-permute-start | bytes 884744 | tf_op jit(solution)/shard_map/ppermute | solution.py:23
  114.3 13.1 %collective-permute-start.19 = (bf16[192,768]{1,0:T(8,128)(2,1)}, bf16[192,768]{1,0:T(8,128)(2,1)S(1)}, u32[]{:S(2)}, u32[]{:S(2)}) collective-permute-start(bf16[192,768]{1,0:T(8,128)(2,1)} %get-tuple-element.86), channel_id=1, source_target_pairs={{0,16},{8,24},{16,0},{24,8},{1,17},{9,25},{17,1},{25,9},{2,18},{10... | collective-permute-start | bytes 884744 | tf_op jit(solution)/shard_map/ppermute | solution.py:23
  116.0 12.0 %collective-permute-start.20 = (bf16[192,768]{1,0:T(8,128)(2,1)S(1)}, bf16[192,768]{1,0:T(8,128)(2,1)S(1)}, u32[]{:S(2)}, u32[]{:S(2)}) collective-permute-start(bf16[192,768]{1,0:T(8,128)(2,1)S(1)} %copy-done.20), channel_id=1, source_target_pairs={{0,24},{8,0},{16,8},{24,16},{1,25},{9,1},{17,9},{25,17},{2,26},{10... | collective-permute-start | bytes 884744 | tf_op jit(solution)/shard_map/ppermute | solution.py:23
  125.7 2.3 copy-start.9
  127.4 0.7 copy-start.10
  128.0 0.7 copy-start.11
  131.5 0.8 copy-start.3
  132.4 0.9 copy-start.4
  144.4 14.5 %collective-permute-start.21 = (bf16[96,2944]{1,0:T(8,128)(2,1)}, bf16[96,2944]{1,0:T(8,128)(2,1)S(1)}, u32[]{:S(2)}, u32[]{:S(2)}) collective-permute-start(bf16[96,2944]{1,0:T(8,128)(2,1)} %get-tuple-element.101), channel_id=1, source_target_pairs={{0,3},{1,0},{2,1},{3,2},{4,7},{5,4},{6,5},{7,6},{8,11},{9,8},{10,9... | collective-permute-start | bytes 1695752 | tf_op jit(solution)/shard_map/ppermute | solution.py:23
  144.8 14.1 %collective-permute-start.22 = (bf16[96,2944]{1,0:T(8,128)(2,1)}, bf16[96,2944]{1,0:T(8,128)(2,1)S(1)}, u32[]{:S(2)}, u32[]{:S(2)}) collective-permute-start(bf16[96,2944]{1,0:T(8,128)(2,1)} %get-tuple-element.103), channel_id=1, source_target_pairs={{0,1},{1,2},{2,3},{3,0},{4,5},{5,6},{6,7},{7,4},{8,9},{9,10},{10,1... | collective-permute-start | bytes 1695752 | tf_op jit(solution)/shard_map/ppermute | solution.py:23
  145.9 34.6 %collective-permute-start.23 = (bf16[1024,512]{1,0:T(8,128)(2,1)}, bf16[1024,512]{1,0:T(8,128)(2,1)}, u32[]{:S(2)}, u32[]{:S(2)}) collective-permute-start(bf16[1024,512]{1,0:T(8,128)(2,1)} %gated_output.1.own), channel_id=1, source_target_pairs={{0,1},{1,2},{2,3},{3,0},{4,5},{5,6},{6,7},{7,4},{8,9},{9,10},{10,1... | collective-permute-start | bytes 3145736 | tf_op jit(solution)/shard_map/ppermute | solution.py:23
  145.9 35.9 %collective-permute-start.24 = (bf16[1024,512]{1,0:T(8,128)(2,1)}, bf16[1024,512]{1,0:T(8,128)(2,1)}, u32[]{:S(2)}, u32[]{:S(2)}) collective-permute-start(bf16[1024,512]{1,0:T(8,128)(2,1)} %gated_output.1.own), channel_id=1, source_target_pairs={{0,3},{1,0},{2,1},{3,2},{4,7},{5,4},{6,5},{7,6},{8,11},{9,8},{10,9... | collective-permute-start | bytes 3145736 | tf_op jit(solution)/shard_map/ppermute | solution.py:23
  160.8 46.9 %collective-permute-start.34 = (bf16[192,2944]{1,0:T(8,128)(2,1)S(1)}, bf16[192,2944]{1,0:T(8,128)(2,1)S(1)}, u32[]{:S(2)}, u32[]{:S(2)}) collective-permute-start(bf16[192,2944]{1,0:T(8,128)(2,1)S(1)} %pad_maximum_fusion.1), channel_id=1, source_target_pairs={{0,1},{1,2},{2,3},{3,0},{4,5},{5,6},{6,7},{7,4},{8,9},{9,10},{10,1... | collective-permute-start | bytes 3391496 | tf_op jit(solution)/shard_map/ppermute | solution.py:23
  162.0 45.7 %collective-permute-start.33 = (bf16[192,2944]{1,0:T(8,128)(2,1)}, bf16[192,2944]{1,0:T(8,128)(2,1)}, u32[]{:S(2)}, u32[]{:S(2)}) collective-permute-start(bf16[192,2944]{1,0:T(8,128)(2,1)} %pad_maximum_fusion), channel_id=1, source_target_pairs={{0,3},{1,0},{2,1},{3,2},{4,7},{5,4},{6,5},{7,6},{8,11},{9,8},{10,9... | collective-permute-start | bytes 3391496 | tf_op jit(solution)/shard_map/ppermute | solution.py:23
  164.7 29.5 %collective-permute-start.25 = (bf16[192,1152]{1,0:T(8,128)(2,1)}, bf16[192,1152]{1,0:T(8,128)(2,1)}, u32[]{:S(2)}, u32[]{:S(2)}) collective-permute-start(bf16[192,1152]{1,0:T(8,128)(2,1)} %get-tuple-element.105), channel_id=1, source_target_pairs={{0,24},{8,0},{16,8},{24,16},{1,25},{9,1},{17,9},{25,17},{2,26},{10... | collective-permute-start | bytes 1327112 | tf_op jit(solution)/shard_map/ppermute | solution.py:23
  180.5 13.7 %collective-permute-start.26 = (bf16[192,1152]{1,0:T(8,128)(2,1)}, bf16[192,1152]{1,0:T(8,128)(2,1)}, u32[]{:S(2)}, u32[]{:S(2)}) collective-permute-start(bf16[192,1152]{1,0:T(8,128)(2,1)} %get-tuple-element.106), channel_id=1, source_target_pairs={{0,16},{8,24},{16,0},{24,8},{1,17},{9,25},{17,1},{25,9},{2,18},{10... | collective-permute-start | bytes 1327112 | tf_op jit(solution)/shard_map/ppermute | solution.py:23
  181.8 18.8 %collective-permute-start.27 = (bf16[192,1152]{1,0:T(8,128)(2,1)}, bf16[192,1152]{1,0:T(8,128)(2,1)}, u32[]{:S(2)}, u32[]{:S(2)}) collective-permute-start(bf16[192,1152]{1,0:T(8,128)(2,1)} %get-tuple-element.107), channel_id=1, source_target_pairs={{0,8},{8,16},{16,24},{24,0},{1,9},{9,17},{17,25},{25,1},{2,10},{10... | collective-permute-start | bytes 1327112 | tf_op jit(solution)/shard_map/ppermute | solution.py:23
  194.1 13.6 %copy-start.2 = (bf16[192,2944]{1,0:T(8,128)(2,1)S(1)}, bf16[192,2944]{1,0:T(8,128)(2,1)}, u32[]{:S(2)}) copy-start(bf16[192,2944]{1,0:T(8,128)(2,1)} %get-tuple-element.119) | copy-start | bytes 3391492
  194.1 13.6 %copy-start.19 = (s32[192]{0:T(256)S(1)}, s32[192]{0:T(256)}, u32[]{:S(2)}) copy-start(s32[192]{0:T(256)} %copy-done.18) | copy-start | bytes 2308
  203.4 8.4 %collective-permute-start.30 = (bf16[192,1152]{1,0:T(8,128)(2,1)}, bf16[192,1152]{1,0:T(8,128)(2,1)}, u32[]{:S(2)}, u32[]{:S(2)}) collective-permute-start(bf16[192,1152]{1,0:T(8,128)(2,1)} %get-tuple-element.115), channel_id=1, source_target_pairs={{0,96},{32,0},{64,32},{96,64},{1,97},{33,1},{65,33},{97,65},{2,98}... | collective-permute-start | bytes 1327112 | tf_op jit(solution)/shard_map/ppermute | solution.py:23
  203.4 11.5 %collective-permute-start.31 = (bf16[192,1152]{1,0:T(8,128)(2,1)}, bf16[192,1152]{1,0:T(8,128)(2,1)}, u32[]{:S(2)}, u32[]{:S(2)}) collective-permute-start(bf16[192,1152]{1,0:T(8,128)(2,1)} %get-tuple-element.116), channel_id=1, source_target_pairs={{0,64},{32,96},{64,0},{96,32},{1,65},{33,97},{65,1},{97,33},{2,66}... | collective-permute-start | bytes 1327112 | tf_op jit(solution)/shard_map/ppermute | solution.py:23
  206.9 20.4 %collective-permute-start.32 = (bf16[192,1152]{1,0:T(8,128)(2,1)}, bf16[192,1152]{1,0:T(8,128)(2,1)}, u32[]{:S(2)}, u32[]{:S(2)}) collective-permute-start(bf16[192,1152]{1,0:T(8,128)(2,1)} %get-tuple-element.117), channel_id=1, source_target_pairs={{0,32},{32,64},{64,96},{96,0},{1,33},{33,65},{65,97},{97,1},{2,34}... | collective-permute-start | bytes 1327112 | tf_op jit(solution)/shard_map/ppermute | solution.py:23
  231.9 10.2 %collective-permute-start.35 = (bf16[256,1152]{1,0:T(8,128)(2,1)}, bf16[256,1152]{1,0:T(8,128)(2,1)S(1)}, u32[]{:S(2)}, u32[]{:S(2)}) collective-permute-start(bf16[256,1152]{1,0:T(8,128)(2,1)} %get-tuple-element.126), channel_id=1, source_target_pairs={{0,4},{4,0},{1,5},{5,1},{2,6},{6,2},{3,7},{7,3},{8,12},{12,8},{9,1... | collective-permute-start | bytes 1769480 | tf_op jit(solution)/shard_map/ppermute | solution.py:23
  232.4 28.8 %all-to-all-start.1 = ((bf16[32,8,2944]{2,1,0:T(8,128)(2,1)}), bf16[32,8,2944]{2,1,0:T(8,128)(2,1)S(1)}, u32[]{:S(2)}, u32[]{:S(2)}) async-start(bf16[32,8,2944]{2,1,0:T(8,128)(2,1)} %bitcast.24), calls=%async_computation.1 | async-start | bytes 3014656 | tf_op jit(solution)/shard_map/all_to_all | solution.py:800
  237.0 5.0 %copy-start.7 = (f32[64,128]{1,0:T(8,128)S(1)}, f32[64,128]{1,0:T(8,128)}, u32[]{:S(2)}) copy-start(f32[64,128]{1,0:T(8,128)} %get-tuple-element.130) | copy-start | bytes 98308
  237.0 5.2 %copy-start.5 = (bf16[256,1152]{1,0:T(8,128)(2,1)S(1)}, bf16[256,1152]{1,0:T(8,128)(2,1)}, u32[]{:S(2)}) copy-start(bf16[256,1152]{1,0:T(8,128)(2,1)} %get-tuple-element.125) | copy-start | bytes 1769476
  239.2 14.5 %collective-permute-start.28 = (bf16[512,512]{1,0:T(8,128)(2,1)S(1)}, bf16[512,512]{1,0:T(8,128)(2,1)S(1)}, u32[]{:S(2)}, u32[]{:S(2)}) collective-permute-start(bf16[512,512]{1,0:T(8,128)(2,1)S(1)} %slice.200), channel_id=1, source_target_pairs={{0,1},{1,2},{2,3},{3,0},{4,5},{5,6},{6,7},{7,4},{8,9},{9,10},{10,1... | collective-permute-start | bytes 1572872 | tf_op jit(solution)/shard_map/ppermute | solution.py:23
  239.5 14.2 %collective-permute-start.29 = (bf16[512,512]{1,0:T(8,128)(2,1)S(1)}, bf16[512,512]{1,0:T(8,128)(2,1)}, u32[]{:S(2)}, u32[]{:S(2)}) collective-permute-start(bf16[512,512]{1,0:T(8,128)(2,1)S(1)} %slice.201), channel_id=1, source_target_pairs={{0,3},{1,0},{2,1},{3,2},{4,7},{5,4},{6,5},{7,6},{8,11},{9,8},{10,9... | collective-permute-start | bytes 1572872 | tf_op jit(solution)/shard_map/ppermute | solution.py:23
  242.4 18.8 %collective-permute-start.38 = (bf16[64,1152]{1,0:T(8,128)(2,1)S(1)}, bf16[64,1152]{1,0:T(8,128)(2,1)S(1)}, u32[]{:S(2)}, u32[]{:S(2)}) collective-permute-start(bf16[64,1152]{1,0:T(8,128)(2,1)S(1)} %get-tuple-element.150), channel_id=1, source_target_pairs={{0,1},{1,2},{2,3},{3,0},{4,5},{5,6},{6,7},{7,4},{8,9},{9,10},{10,1... | collective-permute-start | bytes 442376 | tf_op jit(solution)/shard_map/ppermute | solution.py:23
  242.4 18.7 %collective-permute-start.37 = (bf16[64,1152]{1,0:T(8,128)(2,1)S(1)}, bf16[64,1152]{1,0:T(8,128)(2,1)S(1)}, u32[]{:S(2)}, u32[]{:S(2)}) collective-permute-start(bf16[64,1152]{1,0:T(8,128)(2,1)S(1)} %get-tuple-element.151), channel_id=1, source_target_pairs={{0,2},{1,3},{2,0},{3,1},{4,6},{5,7},{6,4},{7,5},{8,10},{9,11},{10,... | collective-permute-start | bytes 442376 | tf_op jit(solution)/shard_map/ppermute | solution.py:23
  243.6 17.5 %collective-permute-start.36 = (bf16[64,1152]{1,0:T(8,128)(2,1)S(1)}, bf16[64,1152]{1,0:T(8,128)(2,1)S(1)}, u32[]{:S(2)}, u32[]{:S(2)}) collective-permute-start(bf16[64,1152]{1,0:T(8,128)(2,1)S(1)} %get-tuple-element.149), channel_id=1, source_target_pairs={{0,3},{1,0},{2,1},{3,2},{4,7},{5,4},{6,5},{7,6},{8,11},{9,8},{10,9... | collective-permute-start | bytes 442376 | tf_op jit(solution)/shard_map/ppermute | solution.py:23
  253.7 0.8 copy-start.6

commit v2 on v1

--- a/solution.py
+++ b/solution.py
@@ -7,8 +7,9 @@
 from jax.sharding import PartitionSpec as P
 
 
-EP = ("ep_0", "ep_1", "ep_2")
-EP_TP = ("ep_0", "ep_1", "ep_2", "tp")
+Z, Y, C, X = "ep_0", "ep_1", "ep_2", "tp"
+EP = (Z, Y, C)
+EP_TP = (Z, Y, C, X)
 CHUNK = 256
 META = 128
 ROW = 8
@@ -201,9 +202,9 @@
 
 def core_prefix(state, log_total):
     heads = log_total.shape[0]
-    second = lax.axis_index("ep_2") == 1
+    second = lax.axis_index(C) == 1
     mine = pack_state(state, log_total)
-    other_state, other_log = unpack_state(send(mine, "ep_2", 1), heads)
+    other_state, other_log = unpack_state(send(mine, C, 1), heads)
     state = unpack_state(mine, heads)[0]
     inside = (jnp.where(second, other_state, 0.0), jnp.where(second, other_log, 0.0))
     first_s = jnp.where(second, other_state, state)
@@ -257,14 +258,14 @@
 
 
 def ring_first(value):
-    return send(value, "tp", 1), send(value, "tp", -1)
+    return send(value, X, 1), send(value, X, -1)
 
 
 def ring_second(left, right, *earlier):
     half = left.shape[0] // 2
     top, bottom = after(left[:half], *earlier), after(right[half:], *earlier)
-    top = send(top, "tp", 1)
-    bottom = send(bottom, "tp", -1)
+    top = send(top, X, 1)
+    bottom = send(bottom, X, -1)
     return [top, bottom]
 
 
@@ -740,18 +741,18 @@
         expert_input, norm_gain, routes, route_weights, capacity, D_B
     )
     here = jnp.stack([lax.axis_index(name) for name in EP]).astype(jnp.int32)
-    got_b = exchange([payload_b] * 4, "tp", 1)
+    got_b = exchange([payload_b] * 4, X, 1)
     got_a = lax.all_to_all(placed_a.reshape(32, ROW, a_width), EP, 0, 0, tiled=False)
 
     held_b = jnp.concatenate(got_b, axis=0)
-    other_b = send(held_b, "ep_2", 1)
+    other_b = send(held_b, C, 1)
     decay = after(log_decay, placed_a)
     cosine, sine = tables(query.shape[0])
     cum_c, cum_t = running(decay)
 
     state = local_state(after(keys, sine), values, cosine, sine, cum_t)
     inside, group = core_prefix(state, jnp.sum(decay, axis=1))
-    inside, group_z = ring_prefix(inside, group, "ep_1", heads)
+    inside, group_z = ring_prefix(inside, group, Y, heads)
     blocks_b, meta_b = placed_rows(here, got_b, after(other_b, group), D_B, capacity)
 
     compact = compaction(capacity)
@@ -759,14 +760,14 @@
         compact, after(got_a, blocks_b[0]).reshape(32 * ROW, a_width)
     ).astype(BF16)
     left_a, right_a = ring_first(slots_a)
-    inside, _ = ring_prefix(inside, after(group_z, slots_a), "ep_0", heads)
-    got_b = exchange(blocks_b, "ep_0", 1)
+    inside, _ = ring_prefix(inside, after(group_z, slots_a), Z, heads)
+    got_b = exchange(blocks_b, Z, 1)
 
     gated = gated_output(
         query, keys, values, gate_pre, cosine, sine, cum_c, cum_t, inside[0]
     )
     turn_b = regrouped(after(got_b, gated))
-    got_b = exchange(turn_b, "ep_1", 1)
+    got_b = exchange(turn_b, Y, 1)
     cross_a = ring_second(left_a, right_a, turn_b[0])
     left_g, right_g = ring_first(gated)
 
@@ -778,20 +779,20 @@
     ra = width - R_B
     half = 2 * block
     upper, lower = back_a_rows(far, down_w, ra, ((0, half), (half, side)))
-    upper = send(upper, "tp", -1)
-    lower = send(lower, "tp", 1)
+    upper = send(upper, X, -1)
+    lower = send(lower, X, 1)
     back_b = back_b_rows(near, far, down_w, unit)
-    got_b = exchange(back_b, "ep_1", -1)
+    got_b = exchange(back_b, Y, -1)
     b0, b1, b3 = back_a_rows(
         after(near, back_b[0]), down_w, ra, ((0, side), (side, 2 * side), (2 * side, 3 * side))
     )
     b1 = jnp.concatenate([b1[:half] + upper, b1[half:]], axis=0)
     b3 = jnp.concatenate([b3[:half], b3[half:] + lower], axis=0)
-    up_a, down_a = send(b1, "tp", -1), send(b3, "tp", 1)
-    place = lax.axis_index("tp").astype(jnp.int32)[None]
+    up_a, down_a = send(b1, X, -1), send(b3, X, 1)
+    place = lax.axis_index(X).astype(jnp.int32)[None]
     part = projected(place, after(gated, b1, b3), left_g, right_g, out_weight)
     turn_b = regrouped(after(got_b, part))
-    home_b = exchange(turn_b, "ep_0", -1)
+    home_b = exchange(turn_b, Z, -1)
     cross_g = ring_second(left_g, right_g, turn_b[0])
     summed_a = (
         after(b0, turn_b[0]).astype(F32) + up_a.astype(F32) + down_a.astype(F32)
@@ -807,9 +808,9 @@
         for r in range(top)
     ).astype(BF16)
     own_b, other_b = combined_rows(here, after(home_b, spread_a), meta_b, capacity)
-    other_b = send(other_b, "ep_2", 1)
+    other_b = send(other_b, C, 1)
     mixed_b = own_b + other_b
-    got_b = exchange(rows_of(mixed_b, 4), "tp", -1)
+    got_b = exchange(rows_of(mixed_b, 4), X, -1)
     mixed = finished(place, part, *after(cross_g, mixed_b), out_weight)
     final_b = sum(p.astype(F32) for p in got_b)
     final_a = mm(shares, after(home_a, mixed))
@@ -818,25 +819,25 @@
 
 
 def solution(mesh):
-    torus = Mesh(mesh.devices.reshape(4, 4, 2, mesh.shape["tp"]), ("ep_0", "ep_1", "ep_2", "tp"))
+    torus = Mesh(mesh.devices.reshape(4, 4, 2, mesh.shape[X]), EP_TP)
     return jax.shard_map(
         per_device,
         mesh=torus,
         in_specs=(
-            P(EP, "tp"),
-            P(EP, "tp"),
-            P(EP, "tp"),
-            P(EP, "tp"),
-            P("tp", EP),
-            P(None, "tp"),
+            P(EP, X),
+            P(EP, X),
+            P(EP, X),
+            P(EP, X),
+            P(X, EP),
+            P(None, X),
             P(EP_TP, None),
             P(),
             P(EP_TP, None),
             P(EP_TP, None),
-            P(EP, None, "tp"),
-            P(EP, None, "tp"),
-            P(EP, "tp", None),
-        ),
-        out_specs=(P(EP, "tp"), P(EP_TP, None)),
+            P(EP, None, X),
+            P(EP, None, X),
+            P(EP, X, None),
+        ),
+        out_specs=(P(EP, X), P(EP_TP, None)),
         check_vma=False,
     )

time: 267 us -> 267 us (level)
  no operation moved by 1% of the time
where the time goes in v2:
time: 267 us; the launch traced here: 262 us
  Pallas kernels  82.7 us (31%)
  waiting for transfers between devices  80.1 us (30%)
  starting transfers between devices  66.7 us (25%)
  other arithmetic  14.5 us (5%)
  local copies, waits for them, and re-layouts  13.1 us (5%)
  matrix products  4.3 us (2%)
    ppermute x39, waiting for transfers between devices, send(): return lax.ppermute(value, axis, [(i, (i + step) % n) for i in range(n)])  80.1 us
    ppermute x39, starting transfers between devices, send(): return lax.ppermute(value, axis, [(i, (i + step) % n) for i in range(n)])  53.8 us
    pallas_call x1, Pallas kernels, gated_output(): pl.pallas_call(output_kernel, name='gated_output', grid=(grid,), in_specs...  14 us
    pallas_call x2, Pallas kernels, back_a_rows(): pl.pallas_call(kernel, in_specs=[vmem] * 2, out_specs=(vmem,) * len(spans...  9.45 us
    pallas_call x1, Pallas kernels, near_sums(): pl.pallas_call(near_kernel, name='near_sums', in_specs=[vmem] * 5, out_sp...  9.02 us
    all_to_all x1, starting transfers between devices, per_device(): lax.all_to_all(placed_a.reshape(32, ROW, a_width), EP, 0, 0, tiled=False)  8.35 us
    pallas_call x1, Pallas kernels, projected(): pl.pallas_call(project_kernel, name='projected', grid=(4,), in_specs=[pl....  8.1 us
    pallas_call x1, Pallas kernels, hidden_rows(): pl.pallas_call(hidden_kernel, name='hidden_rows', in_specs=[vmem] * 7, ou...  7.49 us
  transfers between devices with their start and end apart: 41, of which 12 were waited for; matrix products, arithmetic and copies ran while one was open for 10% of the time, Pallas kernels for 24%

profile of v2, /device:TPU:1, one launch (start us, length us, event | category | flops | bytes accessed | tf_op | source)
XLA Modules:
  0.0 262.5 jit_solution(10400667767295495664)
XLA Ops:
  0.6 3.2 %token_rows.1 = (bf16[256,3328]{1,0:T(8,128)(2,1)}, bf16[64,896]{1,0:T(8,128)(2,1)}, f32[64,128]{1,0:T(8,128)}) custom-call(bf16[64,4096]{1,0:T(8,128)(2,1)} %refs_0_.1, f32[1,4096]{1,0:T(1,128)} %bitcast.56, s32[2,64]{1,0:T(2,128)} %bitcast.58, f32[2,64]{1,0:T(2,128)} %bitcast.59), custom_call_target="tpu_custom_call" | custom-call | flops 16777216 | bytes 1048576 | tf_op jit(solution)/shard_map/token_rows/pallas_call | solution.py:390
  3.8 2.0 collective-permute-start.4
  5.9 2.5 collective-permute-start.5
  8.3 1.2 collective-permute-start.6
  11.4 1.1 copy.18
  12.5 3.0 %fusion.1 = (f32[1024,128]{1,0:T(8,128)}, f32[1024,128]{1,0:T(8,128)}) fusion(f32[128]{0:T(128)S(1)} %compare_select_fusion.6, f32[128]{0:T(128)S(1)} %mul.194, f32[1024]{0:T(1024)S(1)} %add_convert_fusion.5), kind=kLoop, calls=%fused_computation.11 | loop fusion | flops 262144 | bytes 1053696 | tf_op jit(solution)/shard_map/mul | solution.py:247
  15.5 4.8 %local_state.1 = f32[256,128]{1,0:T(8,128)} custom-call(bf16[1024,256]{1,0:T(8,128)(2,1)} %k_ref.2, bf16[1024,512]{1,0:T(8,128)(2,1)} %v_ref.3, f32[1024,128]{1,0:T(8,128)} %get-tuple-element.153.cos_ref, f32[1024,128]{1,0:T(8,128)} %get-tuple-element.152.sin_ref, f32[1024,4]{1,0:T(8,128)} %bitcast.53), custom_call_target="tpu_custom_call" | custom-call | flops 134217728 | bytes 3145728 | tf_op jit(solution)/shard_map/local_state/pallas_call | solution.py:136
  20.4 0.9 convert_element_type.165
  21.5 1.6 collective-permute-start
  23.1 8.3 %all-to-all-start = ((bf16[32,8,3328]{2,1,0:T(8,128)(2,1)}), bf16[32,8,3328]{2,1,0:T(8,128)(2,1)S(1)}, u32[]{:S(2)}, u32[]{:S(2)}) async-start(bf16[32,8,3328]{2,1,0:T(8,128)(2,1)} %bitcast.16), calls=%async_computation | async-start | bytes 3407872 | tf_op jit(solution)/shard_map/all_to_all | solution.py:745
  32.8 2.6 %collective-permute-start.3 = (bf16[264,128]{1,0:T(8,128)(2,1)S(1)}, bf16[264,128]{1,0:T(8,128)(2,1)S(1)}, u32[]{:S(2)}, u32[]{:S(2)}) collective-permute-start(bf16[264,128]{1,0:T(8,128)(2,1)S(1)} %pad_maximum_fusion.5), channel_id=1, source_target_pairs={{0,24},{8,0},{16,8},{24,16},{1,25},{9,1},{17,9},{25,17},{2,26},{10... | collective-permute-start | bytes 202760 | tf_op jit(solution)/shard_map/ppermute | solution.py:24
  36.6 1.3 collective-permute-start.7
  38.0 15.8 %collective-permute-done.3 = bf16[264,128]{1,0:T(8,128)(2,1)S(1)} collective-permute-done((bf16[264,128]{1,0:T(8,128)(2,1)S(1)}, bf16[264,128]{1,0:T(8,128)(2,1)S(1)}, u32[]{:S(2)}, u32[]{:S(2)}) %collective-permute-start.3) | collective-permute-done | bytes 67616 | tf_op jit(solution)/shard_map/ppermute | solution.py:24
  53.9 2.0 collective-permute-done.2
  57.9 3.0 %placed_rows.1 = (bf16[192,768]{1,0:T(8,128)(2,1)}, bf16[192,768]{1,0:T(8,128)(2,1)}, bf16[192,768]{1,0:T(8,128)(2,1)}, bf16[192,768]{1,0:T(8,128)(2,1)}, bf16[512,128]{1,0:T(8,128)(2,1)}) custom-call(s32[3]{0:T(128)} %pad_add_fusion.refs_0_, bf16[64,896]{1,0:T(8,128)(2,1)} %get-tuple-element.70.refs_1_, bf16[64,896]{1,0:T(8,128)(2,1)} %copy-done.15, ...), custom_call_target="tpu_custom_call" | custom-call | flops 1073741824 | bytes 4194304 | tf_op jit(solution)/shard_map/placed_rows/pallas_call | solution.py:449
  61.4 1.8 collective-permute-start.8
  65.2 1.6 collective-permute-start.13
  66.8 1.7 collective-permute-start.10
  68.5 0.9 collective-permute-start.9
  69.8 11.9 %collective-permute-done.9 = bf16[264,128]{1,0:T(8,128)(2,1)} collective-permute-done((bf16[264,128]{1,0:T(8,128)(2,1)}, bf16[264,128]{1,0:T(8,128)(2,1)}, u32[]{:S(2)}, u32[]{:S(2)}) %collective-permute-start.9) | collective-permute-done | bytes 67616 | tf_op jit(solution)/shard_map/ppermute | solution.py:24
  83.1 1.8 fusion.13.inc_ref
  84.9 14.0 %gated_output.1.own = bf16[1024,512]{1,0:T(8,128)(2,1)} custom-call(bf16[1024,256]{1,0:T(8,128)(2,1)} %q_ref.1, bf16[1024,256]{1,0:T(8,128)(2,1)} %k_ref.2, bf16[1024,512]{1,0:T(8,128)(2,1)} %v_ref.3, bf16[1024,512]{1,0:T(8,128)(2,1)} %g_ref.1, f32[1024,128]{1,0:T(8,128)} %get-tuple-element.153.cos_ref, f32[1024,128]{1,0:T(8,128)} %get-tuple-element.152.sin_ref, ...), custom_call_target="tpu_custom_call" | custom-call | flops 10000000000 | bytes 5242880 | tf_op jit(solution)/shard_map/gated_output/pallas_call | solution.py:161
  99.8 2.3 regrouped.2
  102.1 0.9 slice.198
  103.4 1.5 collective-permute-start.15
  104.8 4.8 %collective-permute-done.16.third = bf16[192,3328]{1,0:T(8,128)(2,1)} collective-permute-done((bf16[192,3328]{1,0:T(8,128)(2,1)S(1)}, bf16[192,3328]{1,0:T(8,128)(2,1)}, u32[]{:S(2)}, u32[]{:S(2)}) %collective-permute-start.16) | collective-permute-done | bytes 1277984 | tf_op jit(solution)/shard_map/ppermute | solution.py:24
  109.6 1.1 slice.199
  110.8 1.6 collective-permute-start.17
  112.3 2.0 collective-permute-start.18
  114.3 1.7 collective-permute-start.19
  116.7 9.0 %near_sums.1 = (f32[576,384]{1,0:T(8,128)}, f32[576,384]{1,0:T(8,128)}) custom-call(bf16[192,3328]{1,0:T(8,128)(2,1)} %copy-done, bf16[192,3328]{1,0:T(8,128)(2,1)} %copy-done.8, bf16[192,3328]{1,0:T(8,128)(2,1)} %collective-permute-done.16.third, bf16[4096,384]{1,0:T(8,128)(2,1)} %bitcast.49, bf16[4096,384]{1,0:T(8,128)(2,1)} %bitcast.51), custom_call_target="tpu_custom_call" | custom-call | flops 2944401408 | bytes 12582912 | tf_op jit(solution)/shard_map/near_sums/pallas_call | solution.py:535
  125.7 1.7 collective-permute-done.19.refs_2_
  128.7 2.8 %turned_rows.1.b_ref = bf16[768,768]{1,0:T(8,128)(2,1)} custom-call(bf16[192,768]{1,0:T(8,128)(2,1)} %get-tuple-element.90.refs_0_, bf16[192,768]{1,0:T(8,128)(2,1)} %copy-done.9, bf16[192,768]{1,0:T(8,128)(2,1)} %copy-done.10, bf16[192,768]{1,0:T(8,128)(2,1)} %copy-done.11), custom_call_target="tpu_custom_call" | custom-call | flops 536870912 | bytes 4194304 | tf_op jit(solution)/shard_map/turned_rows/pallas_call | solution.py:512
  132.4 0.9 copy-done.4
  133.2 7.5 %hidden_rows.1 = (bf16[576,384]{1,0:T(8,128)(2,1)}, bf16[192,384]{1,0:T(8,128)(2,1)}) custom-call(bf16[96,3328]{1,0:T(8,128)(2,1)} %copy-done.3, bf16[96,3328]{1,0:T(8,128)(2,1)} %copy-done.4, bf16[768,768]{1,0:T(8,128)(2,1)} %turned_rows.1.b_ref, f32[576,384]{1,0:T(8,128)} %get-tuple-element.88.gate_sum, f32[576,384]{1,0:T(8,128)} %get-tuple-element.89.up_sum, ...), custom_call_target="tpu_custom_call" | custom-call | flops 2415919104 | bytes 12582912 | tf_op jit(solution)/shard_map/hidden_rows/pallas_call | solution.py:569
  140.7 3.7 %shard_map.141 = (bf16[96,2944]{1,0:T(8,128)(2,1)}, bf16[96,2944]{1,0:T(8,128)(2,1)}) custom-call(bf16[192,384]{1,0:T(8,128)(2,1)} %get-tuple-element.97.refs_1_.hidden_ref, bf16[384,4096]{1,0:T(8,128)(2,1)} %bitcast.60), custom_call_target="tpu_custom_call" | custom-call | flops 2147483648 | bytes 6291456 | tf_op jit(solution)/shard_map/pallas_call | solution.py:636
  144.8 1.1 collective-permute-start.22
  145.9 2.7 %collective-permute-start.24 = (bf16[1024,512]{1,0:T(8,128)(2,1)}, bf16[1024,512]{1,0:T(8,128)(2,1)}, u32[]{:S(2)}, u32[]{:S(2)}) collective-permute-start(bf16[1024,512]{1,0:T(8,128)(2,1)} %gated_output.1.own), channel_id=1, source_target_pairs={{0,3},{1,0},{2,1},{3,2},{4,7},{5,4},{6,5},{7,6},{8,11},{9,8},{10,9... | collective-permute-start | bytes 3145736 | tf_op jit(solution)/shard_map/ppermute | solution.py:24
  148.6 4.6 %back_b_rows.1 = (bf16[192,1152]{1,0:T(8,128)(2,1)}, bf16[192,1152]{1,0:T(8,128)(2,1)}, bf16[192,1152]{1,0:T(8,128)(2,1)}, bf16[192,1152]{1,0:T(8,128)(2,1)}) custom-call(bf16[576,384]{1,0:T(8,128)(2,1)} %get-tuple-element.99.refs_0_.hidden_ref, bf16[192,384]{1,0:T(8,128)(2,1)} %get-tuple-element.97.refs_1_.hidden_ref, bf16[384,4096]{1,0:T(8,128)(2,1)} %bitcast.61), custom_call_target="tpu_custom_call" | custom-call | flops 1073741824 | bytes 3145728 | tf_op jit(solution)/shard_map/back_b_rows/pallas_call | solution.py:614
  153.2 5.7 %shard_map.140 = (bf16[192,2944]{1,0:T(8,128)(2,1)}, bf16[192,2944]{1,0:T(8,128)(2,1)}, bf16[192,2944]{1,0:T(8,128)(2,1)}) custom-call(bf16[576,384]{1,0:T(8,128)(2,1)} %get-tuple-element.99.refs_0_.hidden_ref, bf16[384,4096]{1,0:T(8,128)(2,1)} %bitcast.62), custom_call_target="tpu_custom_call" | custom-call | flops 2147483648 | bytes 6291456 | tf_op jit(solution)/shard_map/pallas_call | solution.py:636
  158.9 1.8 slice_add_fusion.1
  160.9 1.1 pad_maximum_fusion
  162.0 2.7 %collective-permute-start.33 = (bf16[192,2944]{1,0:T(8,128)(2,1)}, bf16[192,2944]{1,0:T(8,128)(2,1)}, u32[]{:S(2)}, u32[]{:S(2)}) collective-permute-start(bf16[192,2944]{1,0:T(8,128)(2,1)} %pad_maximum_fusion), channel_id=1, source_target_pairs={{0,3},{1,0},{2,1},{3,2},{4,7},{5,4},{6,5},{7,6},{8,11},{9,8},{10,9... | collective-permute-start | bytes 3391496 | tf_op jit(solution)/shard_map/ppermute | solution.py:24
  164.7 4.0 %collective-permute-start.25 = (bf16[192,1152]{1,0:T(8,128)(2,1)}, bf16[192,1152]{1,0:T(8,128)(2,1)}, u32[]{:S(2)}, u32[]{:S(2)}) collective-permute-start(bf16[192,1152]{1,0:T(8,128)(2,1)} %get-tuple-element.105), channel_id=1, source_target_pairs={{0,24},{8,0},{16,8},{24,16},{1,25},{9,1},{17,9},{25,17},{2,26},{10... | collective-permute-start | bytes 1327112 | tf_op jit(solution)/shard_map/ppermute | solution.py:24
  168.6 11.9 %collective-permute-done.23.left = bf16[1024,512]{1,0:T(8,128)(2,1)} collective-permute-done((bf16[1024,512]{1,0:T(8,128)(2,1)}, bf16[1024,512]{1,0:T(8,128)(2,1)}, u32[]{:S(2)}, u32[]{:S(2)}) %collective-permute-start.23) | collective-permute-done | bytes 1048608 | tf_op jit(solution)/shard_map/ppermute | solution.py:24
  180.5 1.4 collective-permute-start.26
  181.8 4.2 %collective-permute-start.27 = (bf16[192,1152]{1,0:T(8,128)(2,1)}, bf16[192,1152]{1,0:T(8,128)(2,1)}, u32[]{:S(2)}, u32[]{:S(2)}) collective-permute-start(bf16[192,1152]{1,0:T(8,128)(2,1)} %get-tuple-element.107), channel_id=1, source_target_pairs={{0,8},{8,16},{16,24},{24,0},{1,9},{9,17},{17,25},{25,1},{2,10},{10... | collective-permute-start | bytes 1327112 | tf_op jit(solution)/shard_map/ppermute | solution.py:24
  186.0 8.1 %projected.1.part_ref = f32[1024,1024]{1,0:T(8,128)} custom-call(s32[1]{0:T(128)} %bitcast.place_ref, bf16[1024,512]{1,0:T(8,128)(2,1)} %gated_output.1.own, bf16[1024,512]{1,0:T(8,128)(2,1)} %collective-permute-done.23.left, bf16[1024,512]{1,0:T(8,128)(2,1)} %collective-permute-done.24.right, bf16[2048,1024]{1,0:T(8,128)(2,1)} %w_ref.3), custom_call_target="tpu_custom_call" | custom-call | flops 3221225472 | bytes 10485760 | tf_op jit(solution)/shard_map/projected/pallas_call | solution.py:300
  194.2 6.5 %collective-permute-done.27.i3 = bf16[192,1152]{1,0:T(8,128)(2,1)} collective-permute-done((bf16[192,1152]{1,0:T(8,128)(2,1)}, bf16[192,1152]{1,0:T(8,128)(2,1)}, u32[]{:S(2)}, u32[]{:S(2)}) %collective-permute-start.27) | collective-permute-done | bytes 442400 | tf_op jit(solution)/shard_map/ppermute | solution.py:24
  200.7 2.7 %regrouped.3 = (bf16[192,1152]{1,0:T(8,128)(2,1)}, bf16[192,1152]{1,0:T(8,128)(2,1)}, bf16[192,1152]{1,0:T(8,128)(2,1)}, bf16[192,1152]{1,0:T(8,128)(2,1)}) custom-call(bf16[192,1152]{1,0:T(8,128)(2,1)} %get-tuple-element.108.i0, bf16[192,1152]{1,0:T(8,128)(2,1)} %collective-permute-done.25.i1, bf16[192,1152]{1,0:T(8,128)(2,1)} %collective-permute-done.26.i2, ...), custom_call_target="tpu_custom_call" | custom-call | flops 1048576 | bytes 4194304 | tf_op jit(solution)/shard_map/regrouped/pallas_call | solution.py:473
  203.4 3.5 %collective-permute-start.31 = (bf16[192,1152]{1,0:T(8,128)(2,1)}, bf16[192,1152]{1,0:T(8,128)(2,1)}, u32[]{:S(2)}, u32[]{:S(2)}) collective-permute-start(bf16[192,1152]{1,0:T(8,128)(2,1)} %get-tuple-element.116), channel_id=1, source_target_pairs={{0,64},{32,96},{64,0},{96,32},{1,65},{33,97},{65,1},{97,33},{2,66}... | collective-permute-start | bytes 1327112 | tf_op jit(solution)/shard_map/ppermute | solution.py:24
  206.9 0.9 collective-permute-start.32
  207.8 3.2 %convolution_convert_fusion.1 = bf16[256,2944]{1,0:T(8,128)(2,1)} fusion(bf16[192,2944]{1,0:T(8,128)(2,1)S(1)} %collective-permute-done.34, bf16[192,2944]{1,0:T(8,128)(2,1)} %collective-permute-done.33, bf16[192,2944]{1,0:T(8,128)(2,1)S(1)} %copy-done.2, s32[192]{0:T(256)S(1)} %copy-done.19), kind=kOutput, calls=%fused_computation.1 | convolution fusion | flops 293601280 | bytes 4899584 | tf_op jit(solution)/shard_map/dot_general | solution.py:36
  211.7 3.1 %collective-permute-done.31.refs_3_ = bf16[192,1152]{1,0:T(8,128)(2,1)} collective-permute-done((bf16[192,1152]{1,0:T(8,128)(2,1)}, bf16[192,1152]{1,0:T(8,128)(2,1)}, u32[]{:S(2)}, u32[]{:S(2)}) %collective-permute-start.31) | collective-permute-done | bytes 442400 | tf_op jit(solution)/shard_map/ppermute | solution.py:24
  214.9 12.4 %collective-permute-done.32.refs_4_ = bf16[192,1152]{1,0:T(8,128)(2,1)} collective-permute-done((bf16[192,1152]{1,0:T(8,128)(2,1)}, bf16[192,1152]{1,0:T(8,128)(2,1)}, u32[]{:S(2)}, u32[]{:S(2)}) %collective-permute-start.32) | collective-permute-done | bytes 442400 | tf_op jit(solution)/shard_map/ppermute | solution.py:24
  227.3 4.6 %combined_rows.1 = (bf16[256,1152]{1,0:T(8,128)(2,1)}, bf16[256,1152]{1,0:T(8,128)(2,1)}) custom-call(s32[3]{0:T(128)} %pad_add_fusion.refs_0_, bf16[192,1152]{1,0:T(8,128)(2,1)} %get-tuple-element.120.refs_1_, bf16[192,1152]{1,0:T(8,128)(2,1)} %collective-permute-done.30.refs_2_, bf16[192,1152]{1,0:T(8,128)(2,1)} %collective-permute-done.31.refs_3_, ...), custom_call_target="tpu_custom_call" | custom-call | flops 1073741824 | bytes 4194304 | tf_op jit(solution)/shard_map/combined_rows/pallas_call | solution.py:681
  232.4 4.5 %all-to-all-start.1 = ((bf16[32,8,2944]{2,1,0:T(8,128)(2,1)}), bf16[32,8,2944]{2,1,0:T(8,128)(2,1)S(1)}, u32[]{:S(2)}, u32[]{:S(2)}) async-start(bf16[32,8,2944]{2,1,0:T(8,128)(2,1)} %bitcast.24), calls=%async_computation.1 | async-start | bytes 3014656 | tf_op jit(solution)/shard_map/all_to_all | solution.py:801
  237.0 1.1 slice.200
  238.1 1.1 slice.201
  239.5 2.4 collective-permute-start.29
  242.4 1.2 collective-permute-start.37
  243.6 1.5 collective-permute-start.36
  245.3 8.5 %collective-permute-done.28.top = bf16[512,512]{1,0:T(8,128)(2,1)S(1)} collective-permute-done((bf16[512,512]{1,0:T(8,128)(2,1)S(1)}, bf16[512,512]{1,0:T(8,128)(2,1)S(1)}, u32[]{:S(2)}, u32[]{:S(2)}) %collective-permute-start.28) | collective-permute-done | bytes 524320 | tf_op jit(solution)/shard_map/ppermute | solution.py:24
  254.5 6.6 %finished.1 = bf16[1024,1024]{1,0:T(8,128)(2,1)} custom-call(s32[1]{0:T(128)} %bitcast.place_ref, f32[1024,1024]{1,0:T(8,128)} %projected.1.part_ref, bf16[512,512]{1,0:T(8,128)(2,1)} %copy-done.6, bf16[512,512]{1,0:T(8,128)(2,1)} %collective-permute-done.29.bottom, bf16[2048,1024]{1,0:T(8,128)(2,1)} %w_ref.3), custom_call_target="tpu_custom_call" | custom-call | flops 1073741824 | bytes 10485760 | tf_op jit(solution)/shard_map/finished/pallas_call | solution.py:319
  (159 shorter events, 19.9 us)
Async XLA Ops:
  3.8 32.1 %collective-permute-start.4 = (bf16[64,896]{1,0:T(8,128)(2,1)}, bf16[64,896]{1,0:T(8,128)(2,1)S(1)}, u32[]{:S(2)}, u32[]{:S(2)}) collective-permute-start(bf16[64,896]{1,0:T(8,128)(2,1)} %get-tuple-element.70.refs_1_), channel_id=1, source_target_pairs={{0,1},{1,2},{2,3},{3,0},{4,5},{5,6},{6,7},{7,4},{8,9},{9,10},{10,1... | collective-permute-start | bytes 344072 | tf_op jit(solution)/shard_map/ppermute | solution.py:24
  5.9 30.7 %collective-permute-start.5 = (bf16[64,896]{1,0:T(8,128)(2,1)}, bf16[64,896]{1,0:T(8,128)(2,1)S(1)}, u32[]{:S(2)}, u32[]{:S(2)}) collective-permute-start(bf16[64,896]{1,0:T(8,128)(2,1)} %get-tuple-element.70.refs_1_), channel_id=1, source_target_pairs={{0,2},{1,3},{2,0},{3,1},{4,6},{5,7},{6,4},{7,5},{8,10},{9,11},{10,... | collective-permute-start | bytes 344072 | tf_op jit(solution)/shard_map/ppermute | solution.py:24
  8.3 28.3 %collective-permute-start.6 = (bf16[64,896]{1,0:T(8,128)(2,1)}, bf16[64,896]{1,0:T(8,128)(2,1)S(1)}, u32[]{:S(2)}, u32[]{:S(2)}) collective-permute-start(bf16[64,896]{1,0:T(8,128)(2,1)} %get-tuple-element.70.refs_1_), channel_id=1, source_target_pairs={{0,3},{1,0},{2,1},{3,2},{4,7},{5,4},{6,5},{7,6},{8,11},{9,8},{10,9... | collective-permute-start | bytes 344072 | tf_op jit(solution)/shard_map/ppermute | solution.py:24
  21.5 10.7 %collective-permute-start = (bf16[264,128]{1,0:T(8,128)(2,1)S(1)}, bf16[264,128]{1,0:T(8,128)(2,1)S(1)}, u32[]{:S(2)}, u32[]{:S(2)}) collective-permute-start(bf16[264,128]{1,0:T(8,128)(2,1)S(1)} %pad_maximum_fusion.4), channel_id=1, source_target_pairs={{0,4},{4,0},{1,5},{5,1},{2,6},{6,2},{3,7},{7,3},{8,12},{12,8},{9,1... | collective-permute-start | bytes 202760 | tf_op jit(solution)/shard_map/ppermute | solution.py:24
  23.1 9.5 %copy-start.1 = (f32[256,128]{1,0:T(8,128)S(1)}, f32[256,128]{1,0:T(8,128)}, u32[]{:S(2)}) copy-start(f32[256,128]{1,0:T(8,128)} %local_state.1) | copy-start | bytes 393220
  23.1 13.5 %copy-start.14 = (bf16[64,896]{1,0:T(8,128)(2,1)S(1)}, bf16[64,896]{1,0:T(8,128)(2,1)}, u32[]{:S(2)}) copy-start(bf16[64,896]{1,0:T(8,128)(2,1)} %get-tuple-element.70.refs_1_) | copy-start | bytes 344068
  23.1 37.8 %all-to-all-start = ((bf16[32,8,3328]{2,1,0:T(8,128)(2,1)}), bf16[32,8,3328]{2,1,0:T(8,128)(2,1)S(1)}, u32[]{:S(2)}, u32[]{:S(2)}) async-start(bf16[32,8,3328]{2,1,0:T(8,128)(2,1)} %bitcast.16), calls=%async_computation | async-start | bytes 3407872 | tf_op jit(solution)/shard_map/all_to_all | solution.py:745
  31.6 29.3 %copy-start.18 = (s32[192]{0:T(256)}, s32[192]{0:T(256)S(1)}, u32[]{:S(2)}) copy-start(s32[192]{0:T(256)S(1)} %fusion.28) | copy-start | bytes 2308
  32.8 21.0 %collective-permute-start.3 = (bf16[264,128]{1,0:T(8,128)(2,1)S(1)}, bf16[264,128]{1,0:T(8,128)(2,1)S(1)}, u32[]{:S(2)}, u32[]{:S(2)}) collective-permute-start(bf16[264,128]{1,0:T(8,128)(2,1)S(1)} %pad_maximum_fusion.5), channel_id=1, source_target_pairs={{0,24},{8,0},{16,8},{24,16},{1,25},{9,1},{17,9},{25,17},{2,26},{10... | collective-permute-start | bytes 202760 | tf_op jit(solution)/shard_map/ppermute | solution.py:24
  35.4 20.4 %collective-permute-start.2 = (bf16[264,128]{1,0:T(8,128)(2,1)S(1)}, bf16[264,128]{1,0:T(8,128)(2,1)S(1)}, u32[]{:S(2)}, u32[]{:S(2)}) collective-permute-start(bf16[264,128]{1,0:T(8,128)(2,1)S(1)} %pad_maximum_fusion.5), channel_id=1, source_target_pairs={{0,16},{8,24},{16,0},{24,8},{1,17},{9,25},{17,1},{25,9},{2,18},{10... | collective-permute-start | bytes 202760 | tf_op jit(solution)/shard_map/ppermute | solution.py:24
  36.0 21.9 %copy-start.15 = (bf16[64,896]{1,0:T(8,128)(2,1)}, bf16[64,896]{1,0:T(8,128)(2,1)S(1)}, u32[]{:S(2)}) copy-start(bf16[64,896]{1,0:T(8,128)(2,1)S(1)} %collective-permute-done.4.refs_2_) | copy-start | bytes 344068
  36.0 20.0 %collective-permute-start.1 = (bf16[264,128]{1,0:T(8,128)(2,1)S(1)}, bf16[264,128]{1,0:T(8,128)(2,1)S(1)}, u32[]{:S(2)}, u32[]{:S(2)}) collective-permute-start(bf16[264,128]{1,0:T(8,128)(2,1)S(1)} %pad_maximum_fusion.5), channel_id=1, source_target_pairs={{0,8},{8,16},{16,24},{24,0},{1,9},{9,17},{17,25},{25,1},{2,10},{10... | collective-permute-start | bytes 202760 | tf_op jit(solution)/shard_map/ppermute | solution.py:24
  36.6 21.3 %copy-start.16 = (bf16[64,896]{1,0:T(8,128)(2,1)}, bf16[64,896]{1,0:T(8,128)(2,1)S(1)}, u32[]{:S(2)}) copy-start(bf16[64,896]{1,0:T(8,128)(2,1)S(1)} %collective-permute-done.5.refs_3_) | copy-start | bytes 344068
  36.6 21.3 %copy-start.17 = (bf16[64,896]{1,0:T(8,128)(2,1)}, bf16[64,896]{1,0:T(8,128)(2,1)S(1)}, u32[]{:S(2)}) copy-start(bf16[64,896]{1,0:T(8,128)(2,1)S(1)} %collective-permute-done.6.refs_4_) | copy-start | bytes 344068
  36.6 21.2 %collective-permute-start.7 = (bf16[256,896]{1,0:T(8,128)(2,1)S(1)}, bf16[256,896]{1,0:T(8,128)(2,1)}, u32[]{:S(2)}, u32[]{:S(2)}) collective-permute-start(bf16[256,896]{1,0:T(8,128)(2,1)S(1)} %pad_maximum_fusion.3), channel_id=1, source_target_pairs={{0,4},{4,0},{1,5},{5,1},{2,6},{6,2},{3,7},{7,3},{8,12},{12,8},{9,1... | collective-permute-start | bytes 1376264 | tf_op jit(solution)/shard_map/ppermute | solution.py:24
  61.4 37.5 %copy-start = (bf16[192,3328]{1,0:T(8,128)(2,1)}, bf16[192,3328]{1,0:T(8,128)(2,1)S(1)}, u32[]{:S(2)}) copy-start(bf16[192,3328]{1,0:T(8,128)(2,1)S(1)} %convolution_convert_fusion.first) | copy-start | bytes 3833860
  61.4 8.0 %collective-permute-start.8 = (bf16[264,128]{1,0:T(8,128)(2,1)}, bf16[264,128]{1,0:T(8,128)(2,1)S(1)}, u32[]{:S(2)}, u32[]{:S(2)}) collective-permute-start(bf16[264,128]{1,0:T(8,128)(2,1)} %pad_maximum_fusion.6), channel_id=1, source_target_pairs={{0,32},{32,64},{64,96},{96,0},{1,33},{33,65},{65,97},{97,1},{2,34}... | collective-permute-start | bytes 202760 | tf_op jit(solution)/shard_map/ppermute | solution.py:24
  64.4 34.5 %collective-permute-start.12 = (bf16[192,768]{1,0:T(8,128)(2,1)}, bf16[192,768]{1,0:T(8,128)(2,1)S(1)}, u32[]{:S(2)}, u32[]{:S(2)}) collective-permute-start(bf16[192,768]{1,0:T(8,128)(2,1)} %get-tuple-element.75), channel_id=1, source_target_pairs={{0,32},{32,64},{64,96},{96,0},{1,33},{33,65},{65,97},{97,1},{2,34}... | collective-permute-start | bytes 884744 | tf_op jit(solution)/shard_map/ppermute | solution.py:24
  65.2 33.8 %collective-permute-start.13 = (bf16[192,768]{1,0:T(8,128)(2,1)}, bf16[192,768]{1,0:T(8,128)(2,1)S(1)}, u32[]{:S(2)}, u32[]{:S(2)}) collective-permute-start(bf16[192,768]{1,0:T(8,128)(2,1)} %get-tuple-element.76), channel_id=1, source_target_pairs={{0,64},{32,96},{64,0},{96,32},{1,65},{33,97},{65,1},{97,33},{2,66}... | collective-permute-start | bytes 884744 | tf_op jit(solution)/shard_map/ppermute | solution.py:24
  66.8 16.1 %collective-permute-start.10 = (bf16[264,128]{1,0:T(8,128)(2,1)}, bf16[264,128]{1,0:T(8,128)(2,1)}, u32[]{:S(2)}, u32[]{:S(2)}) collective-permute-start(bf16[264,128]{1,0:T(8,128)(2,1)} %pad_maximum_fusion.6), channel_id=1, source_target_pairs={{0,96},{32,0},{64,32},{96,64},{1,97},{33,1},{65,33},{97,65},{2,98}... | collective-permute-start | bytes 202760 | tf_op jit(solution)/shard_map/ppermute | solution.py:24
  68.5 13.2 %collective-permute-start.9 = (bf16[264,128]{1,0:T(8,128)(2,1)}, bf16[264,128]{1,0:T(8,128)(2,1)}, u32[]{:S(2)}, u32[]{:S(2)}) collective-permute-start(bf16[264,128]{1,0:T(8,128)(2,1)} %pad_maximum_fusion.6), channel_id=1, source_target_pairs={{0,64},{32,96},{64,0},{96,32},{1,65},{33,97},{65,1},{97,33},{2,66}... | collective-permute-start | bytes 202760 | tf_op jit(solution)/shard_map/ppermute | solution.py:24
  69.5 32.6 %collective-permute-start.11 = (bf16[192,3328]{1,0:T(8,128)(2,1)S(1)}, bf16[192,3328]{1,0:T(8,128)(2,1)S(1)}, u32[]{:S(2)}, u32[]{:S(2)}) collective-permute-start(bf16[192,3328]{1,0:T(8,128)(2,1)S(1)} %convolution_convert_fusion.first), channel_id=1, source_target_pairs={{0,1},{1,2},{2,3},{3,0},{4,5},{5,6},{6,7},{7,4},{8,9},{9,10},{10,1... | collective-permute-start | bytes 3833864 | tf_op jit(solution)/shard_map/ppermute | solution.py:24
  81.7 27.9 %collective-permute-start.16 = (bf16[192,3328]{1,0:T(8,128)(2,1)S(1)}, bf16[192,3328]{1,0:T(8,128)(2,1)}, u32[]{:S(2)}, u32[]{:S(2)}) collective-permute-start(bf16[192,3328]{1,0:T(8,128)(2,1)S(1)} %convolution_convert_fusion.first), channel_id=1, source_target_pairs={{0,3},{1,0},{2,1},{3,2},{4,7},{5,4},{6,5},{7,6},{8,11},{9,8},{10,9... | collective-permute-start | bytes 3833864 | tf_op jit(solution)/shard_map/ppermute | solution.py:24
  82.9 16.1 %collective-permute-start.14 = (bf16[192,768]{1,0:T(8,128)(2,1)}, bf16[192,768]{1,0:T(8,128)(2,1)}, u32[]{:S(2)}, u32[]{:S(2)}) collective-permute-start(bf16[192,768]{1,0:T(8,128)(2,1)} %get-tuple-element.77), channel_id=1, source_target_pairs={{0,96},{32,0},{64,32},{96,64},{1,97},{33,1},{65,33},{97,65},{2,98}... | collective-permute-start | bytes 884744 | tf_op jit(solution)/shard_map/ppermute | solution.py:24
  99.0 0.7 copy-start.12
  99.0 0.8 copy-start.13
  102.0 14.0 %copy-start.20 = (bf16[192,768]{1,0:T(8,128)(2,1)S(1)}, bf16[192,768]{1,0:T(8,128)(2,1)}, u32[]{:S(2)}) copy-start(bf16[192,768]{1,0:T(8,128)(2,1)} %get-tuple-element.87) | copy-start | bytes 884740
  102.0 1.3 copy-start.8
  103.4 28.1 %collective-permute-start.15 = (bf16[96,3328]{1,0:T(8,128)(2,1)}, bf16[96,3328]{1,0:T(8,128)(2,1)S(1)}, u32[]{:S(2)}, u32[]{:S(2)}) collective-permute-start(bf16[96,3328]{1,0:T(8,128)(2,1)} %slice.198), channel_id=1, source_target_pairs={{0,1},{1,2},{2,3},{3,0},{4,5},{5,6},{6,7},{7,4},{8,9},{9,10},{10,1... | collective-permute-start | bytes 1916936 | tf_op jit(solution)/shard_map/ppermute | solution.py:24
  110.8 20.7 %collective-permute-start.17 = (bf16[96,3328]{1,0:T(8,128)(2,1)S(1)}, bf16[96,3328]{1,0:T(8,128)(2,1)S(1)}, u32[]{:S(2)}, u32[]{:S(2)}) collective-permute-start(bf16[96,3328]{1,0:T(8,128)(2,1)S(1)} %slice.199), channel_id=1, source_target_pairs={{0,3},{1,0},{2,1},{3,2},{4,7},{5,4},{6,5},{7,6},{8,11},{9,8},{10,9... | collective-permute-start | bytes 1916936 | tf_op jit(solution)/shard_map/ppermute | solution.py:24
  112.3 13.4 %collective-permute-start.18 = (bf16[192,768]{1,0:T(8,128)(2,1)}, bf16[192,768]{1,0:T(8,128)(2,1)S(1)}, u32[]{:S(2)}, u32[]{:S(2)}) collective-permute-start(bf16[192,768]{1,0:T(8,128)(2,1)} %get-tuple-element.85), channel_id=1, source_target_pairs={{0,8},{8,16},{16,24},{24,0},{1,9},{9,17},{17,25},{25,1},{2,10},{10... | collective-permute-start | bytes 884744 | tf_op jit(solution)/shard_map/ppermute | solution.py:24
  114.3 13.1 %collective-permute-start.19 = (bf16[192,768]{1,0:T(8,128)(2,1)}, bf16[192,768]{1,0:T(8,128)(2,1)S(1)}, u32[]{:S(2)}, u32[]{:S(2)}) collective-permute-start(bf16[192,768]{1,0:T(8,128)(2,1)} %get-tuple-element.86), channel_id=1, source_target_pairs={{0,16},{8,24},{16,0},{24,8},{1,17},{9,25},{17,1},{25,9},{2,18},{10... | collective-permute-start | bytes 884744 | tf_op jit(solution)/shard_map/ppermute | solution.py:24
  116.0 12.0 %collective-permute-start.20 = (bf16[192,768]{1,0:T(8,128)(2,1)S(1)}, bf16[192,768]{1,0:T(8,128)(2,1)S(1)}, u32[]{:S(2)}, u32[]{:S(2)}) collective-permute-start(bf16[192,768]{1,0:T(8,128)(2,1)S(1)} %copy-done.20), channel_id=1, source_target_pairs={{0,24},{8,0},{16,8},{24,16},{1,25},{9,1},{17,9},{25,17},{2,26},{10... | collective-permute-start | bytes 884744 | tf_op jit(solution)/shard_map/ppermute | solution.py:24
  125.7 2.3 copy-start.9
  127.4 0.7 copy-start.10
  128.0 0.7 copy-start.11
  131.5 0.8 copy-start.3
  132.4 0.9 copy-start.4
  144.4 14.5 %collective-permute-start.21 = (bf16[96,2944]{1,0:T(8,128)(2,1)}, bf16[96,2944]{1,0:T(8,128)(2,1)S(1)}, u32[]{:S(2)}, u32[]{:S(2)}) collective-permute-start(bf16[96,2944]{1,0:T(8,128)(2,1)} %get-tuple-element.101), channel_id=1, source_target_pairs={{0,3},{1,0},{2,1},{3,2},{4,7},{5,4},{6,5},{7,6},{8,11},{9,8},{10,9... | collective-permute-start | bytes 1695752 | tf_op jit(solution)/shard_map/ppermute | solution.py:24
  144.8 14.1 %collective-permute-start.22 = (bf16[96,2944]{1,0:T(8,128)(2,1)}, bf16[96,2944]{1,0:T(8,128)(2,1)S(1)}, u32[]{:S(2)}, u32[]{:S(2)}) collective-permute-start(bf16[96,2944]{1,0:T(8,128)(2,1)} %get-tuple-element.103), channel_id=1, source_target_pairs={{0,1},{1,2},{2,3},{3,0},{4,5},{5,6},{6,7},{7,4},{8,9},{9,10},{10,1... | collective-permute-start | bytes 1695752 | tf_op jit(solution)/shard_map/ppermute | solution.py:24
  145.9 34.6 %collective-permute-start.23 = (bf16[1024,512]{1,0:T(8,128)(2,1)}, bf16[1024,512]{1,0:T(8,128)(2,1)}, u32[]{:S(2)}, u32[]{:S(2)}) collective-permute-start(bf16[1024,512]{1,0:T(8,128)(2,1)} %gated_output.1.own), channel_id=1, source_target_pairs={{0,1},{1,2},{2,3},{3,0},{4,5},{5,6},{6,7},{7,4},{8,9},{9,10},{10,1... | collective-permute-start | bytes 3145736 | tf_op jit(solution)/shard_map/ppermute | solution.py:24
  145.9 35.9 %collective-permute-start.24 = (bf16[1024,512]{1,0:T(8,128)(2,1)}, bf16[1024,512]{1,0:T(8,128)(2,1)}, u32[]{:S(2)}, u32[]{:S(2)}) collective-permute-start(bf16[1024,512]{1,0:T(8,128)(2,1)} %gated_output.1.own), channel_id=1, source_target_pairs={{0,3},{1,0},{2,1},{3,2},{4,7},{5,4},{6,5},{7,6},{8,11},{9,8},{10,9... | collective-permute-start | bytes 3145736 | tf_op jit(solution)/shard_map/ppermute | solution.py:24
  160.8 46.9 %collective-permute-start.34 = (bf16[192,2944]{1,0:T(8,128)(2,1)S(1)}, bf16[192,2944]{1,0:T(8,128)(2,1)S(1)}, u32[]{:S(2)}, u32[]{:S(2)}) collective-permute-start(bf16[192,2944]{1,0:T(8,128)(2,1)S(1)} %pad_maximum_fusion.1), channel_id=1, source_target_pairs={{0,1},{1,2},{2,3},{3,0},{4,5},{5,6},{6,7},{7,4},{8,9},{9,10},{10,1... | collective-permute-start | bytes 3391496 | tf_op jit(solution)/shard_map/ppermute | solution.py:24
  162.0 45.7 %collective-permute-start.33 = (bf16[192,2944]{1,0:T(8,128)(2,1)}, bf16[192,2944]{1,0:T(8,128)(2,1)}, u32[]{:S(2)}, u32[]{:S(2)}) collective-permute-start(bf16[192,2944]{1,0:T(8,128)(2,1)} %pad_maximum_fusion), channel_id=1, source_target_pairs={{0,3},{1,0},{2,1},{3,2},{4,7},{5,4},{6,5},{7,6},{8,11},{9,8},{10,9... | collective-permute-start | bytes 3391496 | tf_op jit(solution)/shard_map/ppermute | solution.py:24
  164.7 29.5 %collective-permute-start.25 = (bf16[192,1152]{1,0:T(8,128)(2,1)}, bf16[192,1152]{1,0:T(8,128)(2,1)}, u32[]{:S(2)}, u32[]{:S(2)}) collective-permute-start(bf16[192,1152]{1,0:T(8,128)(2,1)} %get-tuple-element.105), channel_id=1, source_target_pairs={{0,24},{8,0},{16,8},{24,16},{1,25},{9,1},{17,9},{25,17},{2,26},{10... | collective-permute-start | bytes 1327112 | tf_op jit(solution)/shard_map/ppermute | solution.py:24
  180.5 13.7 %collective-permute-start.26 = (bf16[192,1152]{1,0:T(8,128)(2,1)}, bf16[192,1152]{1,0:T(8,128)(2,1)}, u32[]{:S(2)}, u32[]{:S(2)}) collective-permute-start(bf16[192,1152]{1,0:T(8,128)(2,1)} %get-tuple-element.106), channel_id=1, source_target_pairs={{0,16},{8,24},{16,0},{24,8},{1,17},{9,25},{17,1},{25,9},{2,18},{10... | collective-permute-start | bytes 1327112 | tf_op jit(solution)/shard_map/ppermute | solution.py:24
  181.8 18.8 %collective-permute-start.27 = (bf16[192,1152]{1,0:T(8,128)(2,1)}, bf16[192,1152]{1,0:T(8,128)(2,1)}, u32[]{:S(2)}, u32[]{:S(2)}) collective-permute-start(bf16[192,1152]{1,0:T(8,128)(2,1)} %get-tuple-element.107), channel_id=1, source_target_pairs={{0,8},{8,16},{16,24},{24,0},{1,9},{9,17},{17,25},{25,1},{2,10},{10... | collective-permute-start | bytes 1327112 | tf_op jit(solution)/shard_map/ppermute | solution.py:24
  194.1 13.6 %copy-start.2 = (bf16[192,2944]{1,0:T(8,128)(2,1)S(1)}, bf16[192,2944]{1,0:T(8,128)(2,1)}, u32[]{:S(2)}) copy-start(bf16[192,2944]{1,0:T(8,128)(2,1)} %get-tuple-element.119) | copy-start | bytes 3391492
  194.1 13.6 %copy-start.19 = (s32[192]{0:T(256)S(1)}, s32[192]{0:T(256)}, u32[]{:S(2)}) copy-start(s32[192]{0:T(256)} %copy-done.18) | copy-start | bytes 2308
  203.4 8.4 %collective-permute-start.30 = (bf16[192,1152]{1,0:T(8,128)(2,1)}, bf16[192,1152]{1,0:T(8,128)(2,1)}, u32[]{:S(2)}, u32[]{:S(2)}) collective-permute-start(bf16[192,1152]{1,0:T(8,128)(2,1)} %get-tuple-element.115), channel_id=1, source_target_pairs={{0,96},{32,0},{64,32},{96,64},{1,97},{33,1},{65,33},{97,65},{2,98}... | collective-permute-start | bytes 1327112 | tf_op jit(solution)/shard_map/ppermute | solution.py:24
  203.4 11.5 %collective-permute-start.31 = (bf16[192,1152]{1,0:T(8,128)(2,1)}, bf16[192,1152]{1,0:T(8,128)(2,1)}, u32[]{:S(2)}, u32[]{:S(2)}) collective-permute-start(bf16[192,1152]{1,0:T(8,128)(2,1)} %get-tuple-element.116), channel_id=1, source_target_pairs={{0,64},{32,96},{64,0},{96,32},{1,65},{33,97},{65,1},{97,33},{2,66}... | collective-permute-start | bytes 1327112 | tf_op jit(solution)/shard_map/ppermute | solution.py:24
  206.9 20.4 %collective-permute-start.32 = (bf16[192,1152]{1,0:T(8,128)(2,1)}, bf16[192,1152]{1,0:T(8,128)(2,1)}, u32[]{:S(2)}, u32[]{:S(2)}) collective-permute-start(bf16[192,1152]{1,0:T(8,128)(2,1)} %get-tuple-element.117), channel_id=1, source_target_pairs={{0,32},{32,64},{64,96},{96,0},{1,33},{33,65},{65,97},{97,1},{2,34}... | collective-permute-start | bytes 1327112 | tf_op jit(solution)/shard_map/ppermute | solution.py:24
  231.9 10.2 %collective-permute-start.35 = (bf16[256,1152]{1,0:T(8,128)(2,1)}, bf16[256,1152]{1,0:T(8,128)(2,1)S(1)}, u32[]{:S(2)}, u32[]{:S(2)}) collective-permute-start(bf16[256,1152]{1,0:T(8,128)(2,1)} %get-tuple-element.126), channel_id=1, source_target_pairs={{0,4},{4,0},{1,5},{5,1},{2,6},{6,2},{3,7},{7,3},{8,12},{12,8},{9,1... | collective-permute-start | bytes 1769480 | tf_op jit(solution)/shard_map/ppermute | solution.py:24
  232.4 28.8 %all-to-all-start.1 = ((bf16[32,8,2944]{2,1,0:T(8,128)(2,1)}), bf16[32,8,2944]{2,1,0:T(8,128)(2,1)S(1)}, u32[]{:S(2)}, u32[]{:S(2)}) async-start(bf16[32,8,2944]{2,1,0:T(8,128)(2,1)} %bitcast.24), calls=%async_computation.1 | async-start | bytes 3014656 | tf_op jit(solution)/shard_map/all_to_all | solution.py:801
  237.0 5.0 %copy-start.7 = (f32[64,128]{1,0:T(8,128)S(1)}, f32[64,128]{1,0:T(8,128)}, u32[]{:S(2)}) copy-start(f32[64,128]{1,0:T(8,128)} %get-tuple-element.130) | copy-start | bytes 98308
  237.0 5.2 %copy-start.5 = (bf16[256,1152]{1,0:T(8,128)(2,1)S(1)}, bf16[256,1152]{1,0:T(8,128)(2,1)}, u32[]{:S(2)}) copy-start(bf16[256,1152]{1,0:T(8,128)(2,1)} %get-tuple-element.125) | copy-start | bytes 1769476
  239.2 14.5 %collective-permute-start.28 = (bf16[512,512]{1,0:T(8,128)(2,1)S(1)}, bf16[512,512]{1,0:T(8,128)(2,1)S(1)}, u32[]{:S(2)}, u32[]{:S(2)}) collective-permute-start(bf16[512,512]{1,0:T(8,128)(2,1)S(1)} %slice.200), channel_id=1, source_target_pairs={{0,1},{1,2},{2,3},{3,0},{4,5},{5,6},{6,7},{7,4},{8,9},{9,10},{10,1... | collective-permute-start | bytes 1572872 | tf_op jit(solution)/shard_map/ppermute | solution.py:24
  239.5 14.2 %collective-permute-start.29 = (bf16[512,512]{1,0:T(8,128)(2,1)S(1)}, bf16[512,512]{1,0:T(8,128)(2,1)}, u32[]{:S(2)}, u32[]{:S(2)}) collective-permute-start(bf16[512,512]{1,0:T(8,128)(2,1)S(1)} %slice.201), channel_id=1, source_target_pairs={{0,3},{1,0},{2,1},{3,2},{4,7},{5,4},{6,5},{7,6},{8,11},{9,8},{10,9... | collective-permute-start | bytes 1572872 | tf_op jit(solution)/shard_map/ppermute | solution.py:24
  242.4 18.8 %collective-permute-start.38 = (bf16[64,1152]{1,0:T(8,128)(2,1)S(1)}, bf16[64,1152]{1,0:T(8,128)(2,1)S(1)}, u32[]{:S(2)}, u32[]{:S(2)}) collective-permute-start(bf16[64,1152]{1,0:T(8,128)(2,1)S(1)} %get-tuple-element.150), channel_id=1, source_target_pairs={{0,1},{1,2},{2,3},{3,0},{4,5},{5,6},{6,7},{7,4},{8,9},{9,10},{10,1... | collective-permute-start | bytes 442376 | tf_op jit(solution)/shard_map/ppermute | solution.py:24
  242.4 18.7 %collective-permute-start.37 = (bf16[64,1152]{1,0:T(8,128)(2,1)S(1)}, bf16[64,1152]{1,0:T(8,128)(2,1)S(1)}, u32[]{:S(2)}, u32[]{:S(2)}) collective-permute-start(bf16[64,1152]{1,0:T(8,128)(2,1)S(1)} %get-tuple-element.151), channel_id=1, source_target_pairs={{0,2},{1,3},{2,0},{3,1},{4,6},{5,7},{6,4},{7,5},{8,10},{9,11},{10,... | collective-permute-start | bytes 442376 | tf_op jit(solution)/shard_map/ppermute | solution.py:24
  243.6 17.5 %collective-permute-start.36 = (bf16[64,1152]{1,0:T(8,128)(2,1)S(1)}, bf16[64,1152]{1,0:T(8,128)(2,1)S(1)}, u32[]{:S(2)}, u32[]{:S(2)}) collective-permute-start(bf16[64,1152]{1,0:T(8,128)(2,1)S(1)} %get-tuple-element.149), channel_id=1, source_target_pairs={{0,3},{1,0},{2,1},{3,2},{4,7},{5,4},{6,5},{7,6},{8,11},{9,8},{10,9... | collective-permute-start | bytes 442376 | tf_op jit(solution)/shard_map/ppermute | solution.py:24
  253.7 0.8 copy-start.6
